TPU v7x, 32 devices: a whole 2x2x4 slice. The times are simulated.
32 devices in a mesh: ep: 4 (over y, x), tp: 8 (over z, core).
Axes of the slice: x: 2, y: 2, z: 4, core: 2. Of those that a mesh axis runs over, the one named last changes fastest.
Arguments:
- query_preactivation: bfloat16 [8192, 2048], P('ep', 'tp'), may hold values from -6 to 6
- forget_preactivation: bfloat16 [8192, 2048], P('ep', 'tp'), may hold values from -6 to 6
- value_input_rows: bfloat16 [8192, 1024], P('ep', 'tp'), may hold values from -8 to 8
- output_gate_preactivation: bfloat16 [8192, 1024], P('ep', 'tp'), may hold values from -6 to 6
- forget_floor_gap: float32 [2048], P('tp'), may hold values from 0 to 0.2, as said below
- extra_log_forget: float32 [8192, 16], P('ep', 'tp'), may hold values from -2 to 0
- head_output_gain: float32 [1024], P('tp'), may hold values from 0.1 to 1.9
- mixer_output_weight: bfloat16 [1024, 2048], P(None, 'tp'), may hold values from -0.1875 to 0.1875
- second_batch_tokens: bfloat16 [2048, 2048], P('ep'), may hold values from -6 to 6
- feedforward_norm_gain: float32 [2048], replicated, may hold values from 0.1 to 1.9
- chosen_expert_index: int32 [2048, 2], P('ep'), may hold values from 0 to 3, all different within a row; in each aligned block of 64 rows (0 to 63, 64 to 127, ...) at most 40 rows name the same one
- chosen_expert_weight: float32 [2048, 2], P('ep'), may hold values from 0.1 to 1
- expert_gate_weight: bfloat16 [4, 2048, 7168], P('ep', None, 'tp'), may hold values from -0.125 to 0.125
- expert_up_weight: bfloat16 [4, 2048, 7168], P('ep', None, 'tp'), may hold values from -0.125 to 0.125
- expert_down_weight: bfloat16 [4, 7168, 2048], P('ep', 'tp'), may hold values from -0.0625 to 0.0625
Outputs:
- mixer_output_first: bfloat16 [8192, 2048], P('ep', 'tp')
- moe_out: bfloat16 [2048, 2048], P(('ep', 'tp'))
Inputs may be any that keep to these rules, and one draw needn't show every extreme that they name: `chosen_expert_index`: each row names 2 different experts. In each aligned block of 64 rows (the rows of one device's share) no expert is named by more than 40 rows, and in every draw some expert is named by exactly 40 rows of some block. `forget_floor_gap`: every entry is positive.
All inputs are finite; a program needn't handle non-finite values.
Results may differ from a plain program's by a relative error of at most 0.019.
Values may be sent and summed in bfloat16 or wider, within the bound.
No kernel may reach another device: no remote copies, remote signals or barrier semaphores. Data moves between devices by JAX's collectives and lax.ppermute only.
A program may use at most 128 MiB of HBM per device.

v0:
```python
import functools
import jax
import jax.numpy as jnp
from jax import lax
from jax.experimental import pallas as pl
from jax.experimental.pallas import tpu as pltpu
from jax.sharding import PartitionSpec as P


KEY_DIM = 128
VAL_DIM = 64
BLOCK = 64
TOPK = 2
CORES = 2
PIECES = 2
epsilon = 1e-06
f32 = jnp.float32
bf16 = jnp.bfloat16


def mm(a, b, dims=((1,), (0,))):
    return lax.dot_general(a, b, (dims, ((), ())), preferred_element_type=f32)


def split2(x):
    hi = x.astype(bf16)
    return hi, (x - hi.astype(f32)).astype(bf16)


def sigmoid(x):
    return 1.0 / (1.0 + jnp.exp(-x))


def forget_log(heads, f_ref, gap_ref, extra_ref):
    key = gap_ref[...] * sigmoid(-f_ref[...].astype(f32))
    kw = heads * KEY_DIM
    pick = lax.broadcasted_iota(jnp.int32, (heads, kw), 1) // KEY_DIM
    pick = (pick == lax.broadcasted_iota(jnp.int32, (heads, kw), 0)).astype(bf16)
    hi, lo = split2(extra_ref[...])
    extra = mm(hi, pick, ((0,), (0,))) + mm(lo, pick, ((0,), (0,)))
    return key, jnp.log(1.0 - key) + extra


def same_head(heads):
    shape = (heads * VAL_DIM, heads * KEY_DIM)
    vh = lax.broadcasted_iota(jnp.int32, shape, 0) // VAL_DIM
    return vh == lax.broadcasted_iota(jnp.int32, shape, 1) // KEY_DIM


def state_body(heads, rows, f_ref, v_ref, gap_ref, extra_ref, st_ref, s_ref, l_ref):
    step = pl.program_id(0)
    vw = heads * VAL_DIM

    @pl.when(step == 0)
    def _():
        s_ref[...] = jnp.zeros_like(s_ref)
        l_ref[...] = jnp.zeros_like(l_ref)

    key, logf = forget_log(heads, f_ref, gap_ref, extra_ref)
    row = lax.broadcasted_iota(jnp.int32, (rows, rows), 0)
    later = (row < lax.broadcasted_iota(jnp.int32, (rows, rows), 1)).astype(bf16)
    hi, lo = split2(logf)
    rest = mm(later, hi) + mm(later, lo)
    whole = rest[0:1] + logf[0:1]
    ks = (key * jnp.exp(rest)).astype(bf16)
    s = s_ref[...] * jnp.exp(whole) + mm(v_ref[...], ks, ((0,), (0,)))
    l = l_ref[...] + whole
    s_ref[...] = s
    l_ref[...] = l

    @pl.when(step == pl.num_programs(0) - 1)
    def _():
        for h in range(heads):
            st_ref[h * VAL_DIM : (h + 1) * VAL_DIM, :] = s[
                h * VAL_DIM : (h + 1) * VAL_DIM, h * KEY_DIM : (h + 1) * KEY_DIM
            ]
            st_ref[vw + h : vw + h + 1, :] = l[:, h * KEY_DIM : (h + 1) * KEY_DIM]


def final_state(f, v, gap, extra):
    length, kw = f.shape
    heads = kw // KEY_DIM
    vw = heads * VAL_DIM
    rows = 4 * BLOCK
    rows_of = lambda w: pl.BlockSpec((rows, w), lambda i: (i, 0))
    whole = lambda r, w: pl.BlockSpec((r, w), lambda i: (0, 0))
    return pl.pallas_call(
        functools.partial(state_body, heads, rows),
        grid=(length // rows,),
        in_specs=[rows_of(kw), rows_of(vw), whole(1, kw), pl.BlockSpec((heads, rows), lambda i: (0, i))],
        out_specs=whole(vw + 8, KEY_DIM),
        out_shape=jax.ShapeDtypeStruct((vw + 8, KEY_DIM), f32),
        scratch_shapes=[pltpu.VMEM((vw, kw), f32), pltpu.VMEM((1, kw), f32)],
        cost_estimate=pl.CostEstimate(flops=4 * 10**9, bytes_accessed=2 * 10**6, transcendentals=10**6),
        name="final_state",
    )(f, v, gap.reshape(1, kw), extra)


def mixer_body(heads, ep, rows, sc_ref, *refs):
    others = refs[: ep - 1]
    q_ref, f_ref, v_ref, gate_ref, gap_ref, extra_ref, gain_ref, mixed_ref, s_ref = refs[ep - 1 :]
    kw = heads * KEY_DIM
    vw = heads * VAL_DIM
    blocks = rows // BLOCK
    me = sc_ref[0]

    @pl.when(pl.program_id(0) == 0)
    def _():
        carried = [jnp.zeros((VAL_DIM, KEY_DIM), f32) for _ in range(heads)]
        for j in range(ep):
            use = j < me
            for m in range(1, ep):
                flag = jnp.where(use & ((me ^ m) == j), 1.0, 0.0).astype(f32)
                o = others[m - 1]
                for h in range(heads):
                    decay = jnp.exp(o[vw + h : vw + h + 1, :] * flag)
                    carried[h] = carried[h] * decay + o[h * VAL_DIM : (h + 1) * VAL_DIM, :] * flag
        s_ref[...] = jnp.zeros_like(s_ref)
        for h in range(heads):
            s_ref[h * VAL_DIM : (h + 1) * VAL_DIM, h * KEY_DIM : (h + 1) * KEY_DIM] = carried[h]

    q = q_ref[...].astype(f32)
    q = q * sigmoid(q)
    key, logf = forget_log(heads, f_ref, gap_ref, extra_ref)
    row = lax.broadcasted_iota(jnp.int32, (rows, rows), 0)
    col = lax.broadcasted_iota(jnp.int32, (rows, rows), 1)
    causal = (row >= col) & (row // BLOCK == col // BLOCK)
    tri = causal.astype(bf16)
    hi, lo = split2(logf)
    cum = mm(tri, hi) + mm(tri, lo)
    v = v_ref[...]
    finals = [cum[(b + 1) * BLOCK - 1 : (b + 1) * BLOCK] for b in range(blocks)]
    fin = jnp.concatenate([jnp.broadcast_to(x, (BLOCK, kw)) for x in finals], axis=0)
    qs = (q * jnp.exp(cum - fin)).astype(bf16)
    ks = (key * jnp.exp(fin - cum)).astype(bf16)
    qc = (q * jnp.exp(cum)).astype(bf16)
    within = []
    for h in range(heads):
        ksl = slice(h * KEY_DIM, (h + 1) * KEY_DIM)
        sc = mm(qs[:, ksl], ks[:, ksl], ((1,), (1,)))
        sc = jnp.where(causal, sc, 0.0).astype(bf16)
        within.append(mm(sc, v[:, h * VAL_DIM : (h + 1) * VAL_DIM]))
    within = jnp.concatenate(within, axis=1)
    same = same_head(heads)
    s = s_ref[...]
    across = []
    for b in range(blocks):
        rs = slice(b * BLOCK, (b + 1) * BLOCK)
        across.append(mm(qc[rs], s.astype(bf16), ((1,), (1,))))
        upd = jnp.where(same, mm(v[rs], ks[rs], ((0,), (0,))), 0.0)
        s = s * jnp.exp(finals[b]) + upd
    s_ref[...] = s
    rec = within + jnp.concatenate(across, axis=0)
    a = lax.broadcasted_iota(jnp.int32, (vw, vw), 0) // VAL_DIM
    b = lax.broadcasted_iota(jnp.int32, (vw, vw), 1) // VAL_DIM
    ones = (a == b).astype(bf16)
    hi, lo = split2(rec * rec)
    mean = (mm(hi, ones) + mm(lo, ones)) * (1.0 / VAL_DIM)
    g = gate_ref[...].astype(f32)
    mixed_ref[...] = (rec * lax.rsqrt(mean + epsilon) * gain_ref[...] * (g * sigmoid(g))).astype(bf16)


def mixer(scal, others, q, f, v, gate, gap, extra, gain):
    length, kw = q.shape
    heads = kw // KEY_DIM
    vw = heads * VAL_DIM
    ep = len(others) + 1
    rows = 4 * BLOCK
    rows_of = lambda w: pl.BlockSpec((rows, w), lambda i, s: (i, 0))
    whole = lambda r, w: pl.BlockSpec((r, w), lambda i, s: (0, 0))
    return pl.pallas_call(
        functools.partial(mixer_body, heads, ep, rows),
        grid_spec=pltpu.PrefetchScalarGridSpec(
            num_scalar_prefetch=1,
            grid=(length // rows,),
            in_specs=[whole(vw + 8, KEY_DIM)] * (ep - 1)
            + [rows_of(kw), rows_of(kw), rows_of(vw), rows_of(vw), whole(1, kw)]
            + [pl.BlockSpec((heads, rows), lambda i, s: (0, i)), whole(1, vw)],
            out_specs=rows_of(vw),
            scratch_shapes=[pltpu.VMEM((vw, kw), f32)],
        ),
        out_shape=jax.ShapeDtypeStruct((length, vw), bf16),
        cost_estimate=pl.CostEstimate(flops=12 * 10**9, bytes_accessed=4 * 10**6, transcendentals=10**6),
        name="mixer",
    )(scal, *others, q, f, v, gate, gap.reshape(1, kw), extra, gain.reshape(1, vw))


def project_body(zn, sc_ref, *refs):
    gs = refs[:zn]
    w_ref, wp_ref, own_ref, other_ref = refs[zn:]
    vw = gs[0].shape[1]
    own = other = None
    for m in range(zn):
        at = pl.multiple_of(((sc_ref[2] ^ m) * CORES + sc_ref[1]) * vw, vw)
        g = gs[m][...]
        a = mm(g, w_ref[pl.ds(at, vw), :])
        b = mm(g, wp_ref[pl.ds(at, vw), :])
        own = a if own is None else own + a
        other = b if other is None else other + b
    own_ref[...] = own
    other_ref[...] = other.astype(bf16)


def project(scal, gathered, w, wp):
    length, vw = gathered[0].shape
    zn = len(gathered)
    rows = min(length, 512)
    rows_of = lambda n: pl.BlockSpec((rows, n), lambda i, s: (i, 0))
    whole = pl.BlockSpec(w.shape, lambda i, s: (0, 0))
    width = w.shape[1]
    return pl.pallas_call(
        functools.partial(project_body, zn),
        grid_spec=pltpu.PrefetchScalarGridSpec(
            num_scalar_prefetch=1,
            grid=(length // rows,),
            in_specs=[rows_of(vw)] * zn + [whole, whole],
            out_specs=[rows_of(width), rows_of(width)],
        ),
        out_shape=[
            jax.ShapeDtypeStruct((length, width), f32),
            jax.ShapeDtypeStruct((length, width), bf16),
        ],
        cost_estimate=pl.CostEstimate(flops=2 * 10**9, bytes_accessed=6 * 10**6, transcendentals=0),
        name="project",
    )(scal, *gathered, w, wp)


def own_lanes(x, zn, sub, core):
    out = None
    for c in range(CORES):
        at = [(z * CORES + c) * sub for z in range(zn)]
        part = jnp.concatenate([x[:, a : a + sub] for a in at], axis=1)
        out = part if out is None else jnp.where(core == c, part, out)
    return out


def targets(idx, me, zn, experts, capacity):
    n = idx.shape[1]
    sub = n // zn
    lines = max(8, experts)
    line = lax.broadcasted_iota(jnp.int32, (lines, n), 0)
    picks = [line == idx[r : r + 1] for r in range(TOPK)]
    onehot = jnp.where(picks[0] | picks[1], 1.0, 0.0).astype(bf16)
    row = lax.broadcasted_iota(jnp.int32, (n, n), 0)
    col = lax.broadcasted_iota(jnp.int32, (n, n), 1)
    earlier = ((row < col) & (row // sub == col // sub)).astype(bf16)
    counts = mm(onehot, earlier)
    blk = lax.broadcasted_iota(jnp.int32, (1, n), 1) // sub
    out = []
    for r in range(TOPK):
        slot = jnp.sum(jnp.where(picks[r], counts, 0.0), axis=0, keepdims=True).astype(jnp.int32)
        out.append((idx[r : r + 1] ^ me) * (zn * capacity) + blk * capacity + slot)
    return out


def pack_body(experts, capacity, sc_ref, tok_ref, idx_ref, gain_ref, *outs):
    zn, _, sub, width = tok_ref.shape
    n = zn * sub
    x = tok_ref[...].reshape(n, width).astype(f32)
    x = (x * lax.rsqrt(jnp.mean(x * x, axis=1, keepdims=True) + epsilon) * gain_ref[...]).astype(bf16)
    t = targets(own_lanes(idx_ref[...], zn, sub, sc_ref[1]), sc_ref[0], zn, experts, capacity)
    per = zn * capacity
    line = lax.broadcasted_iota(jnp.int32, (per, n), 0)
    for m in range(experts):
        hit = (t[0] == line + m * per) | (t[1] == line + m * per)
        outs[m][...] = mm(jnp.where(hit, 1.0, 0.0).astype(bf16), x).astype(bf16)


def pack(scal, tokens, idx, gain, experts, capacity):
    zn, _, sub, width = tokens.shape
    shape = jax.ShapeDtypeStruct((zn * capacity, width), bf16)
    return pl.pallas_call(
        functools.partial(pack_body, experts, capacity),
        grid_spec=pltpu.PrefetchScalarGridSpec(
            num_scalar_prefetch=1,
            grid=(1,),
            in_specs=[
                pl.BlockSpec((zn, 1, sub, width), lambda i, s: (0, s[1], 0, 0)),
                pl.BlockSpec(idx.shape, lambda i, s: (0, 0)),
                pl.BlockSpec((1, width), lambda i, s: (0, 0)),
            ],
            out_specs=[pl.BlockSpec(shape.shape, lambda i, s: (0, 0))] * experts,
        ),
        out_shape=[shape] * experts,
        cost_estimate=pl.CostEstimate(flops=4 * 10**9, bytes_accessed=4 * 10**6, transcendentals=10**3),
        name="pack",
    )(scal, tokens, idx, gain.reshape(1, width))


def ffn_body(count, pieces, *refs):
    xs = refs[:count]
    wg, wgp, wu, wup, wd, wdp = refs[count : count + 6]
    outs = refs[count + 6 : -2]
    x_ref, acc_ref = refs[-2:]
    step = pl.program_id(0)
    per = xs[0].shape[0]

    @pl.when(step == 0)
    def _():
        x_ref[...] = jnp.concatenate([x[...] for x in xs], axis=0)
        acc_ref[...] = jnp.zeros_like(acc_ref)

    x = x_ref[...]
    g = mm(x, jnp.concatenate([wg[0], wgp[0]], axis=1))
    u = mm(x, jnp.concatenate([wu[0], wup[0]], axis=1))
    h = (g * sigmoid(g) * u).astype(bf16)
    acc_ref[...] += mm(h, jnp.concatenate([wd[0], wdp[0]], axis=0))

    @pl.when(step == pl.num_programs(0) - 1)
    def _():
        cols = x_ref.shape[1] // pieces
        for i in range(count):
            for p in range(pieces):
                outs[i * pieces + p][...] = acc_ref[
                    i * per : (i + 1) * per, p * cols : (p + 1) * cols
                ].astype(bf16)


def ffn(xs, weights, pieces):
    count = len(xs)
    per, width = xs[0].shape
    hidden = weights[0].shape[2]
    chunk = 128 if hidden % 128 == 0 else hidden
    whole = pl.BlockSpec((per, width), lambda i: (0, 0))
    out = pl.BlockSpec((per, width // pieces), lambda i: (0, 0))
    up = pl.BlockSpec((1, width, chunk), lambda i: (0, 0, i))
    down = pl.BlockSpec((1, chunk, width), lambda i: (0, i, 0))
    outs = pl.pallas_call(
        functools.partial(ffn_body, count, pieces),
        grid=(hidden // chunk,),
        in_specs=[whole] * count + [up] * 4 + [down] * 2,
        out_specs=[out] * (count * pieces),
        out_shape=[jax.ShapeDtypeStruct((per, width // pieces), bf16)] * (count * pieces),
        scratch_shapes=[pltpu.VMEM((count * per, width), bf16), pltpu.VMEM((count * per, width), f32)],
        cost_estimate=pl.CostEstimate(flops=8 * 10**9, bytes_accessed=25 * 10**6, transcendentals=10**6),
        name="ffn",
    )(*xs, *weights)
    return [outs[i * pieces : (i + 1) * pieces] for i in range(count)]


def combine_body(experts, capacity, zn, sc_ref, idx_ref, w_ref, *refs):
    ys = refs[:experts]
    outs = refs[experts : experts + zn]
    acc_ref = refs[-1]
    sub = outs[0].shape[0]
    n = zn * sub
    t = targets(own_lanes(idx_ref[...], zn, sub, sc_ref[1]), sc_ref[0], zn, experts, capacity)
    w = own_lanes(w_ref[...], zn, sub, sc_ref[1])
    per = zn * capacity
    line = lax.broadcasted_iota(jnp.int32, (per, n), 0)
    acc = None
    for m in range(experts):
        c = jnp.where(t[0] == line + m * per, w[0:1], 0.0)
        c = c + jnp.where(t[1] == line + m * per, w[1:2], 0.0)
        part = mm(c.astype(bf16), ys[m][...], ((0,), (0,)))
        acc = part if acc is None else acc + part
    acc_ref[...] = acc.reshape(zn, sub, acc.shape[1]).astype(bf16)
    for m in range(zn):
        outs[m][...] = acc_ref[sc_ref[2] ^ m]


def combine(scal, idx, w, ys, piece, pieces, zn, sub, capacity):
    experts = len(ys)
    per = zn * capacity
    cols = ys[0].shape[1] // pieces if ys[0].shape[1] == max(y.shape[1] for y in ys) else ys[0].shape[1]
    shape = jax.ShapeDtypeStruct((sub, cols), bf16)
    return pl.pallas_call(
        functools.partial(combine_body, experts, capacity, zn),
        grid_spec=pltpu.PrefetchScalarGridSpec(
            num_scalar_prefetch=1,
            grid=(1,),
            in_specs=[pl.BlockSpec(idx.shape, lambda i, s: (0, 0))] * 2
            + [
                pl.BlockSpec((per, cols), (lambda i, s: (0, piece)) if y.shape[1] != cols else (lambda i, s: (0, 0)))
                for y in ys
            ],
            out_specs=[pl.BlockSpec(shape.shape, lambda i, s: (0, 0))] * zn,
            scratch_shapes=[pltpu.VMEM((zn, sub, cols), bf16)],
        ),
        out_shape=[shape] * zn,
        cost_estimate=pl.CostEstimate(flops=10**9, bytes_accessed=2 * 10**6, transcendentals=10**3),
        name="combine",
    )(scal, idx, w, *ys)


def on_device(
    query_preactivation,
    forget_preactivation,
    value_input_rows,
    output_gate_preactivation,
    forget_floor_gap,
    extra_log_forget,
    head_output_gain,
    mixer_output_weight,
    second_batch_tokens,
    feedforward_norm_gain,
    chosen_expert_index,
    chosen_expert_weight,
    expert_gate_weight,
    expert_up_weight,
    expert_down_weight,
):
    ep = lax.axis_size("ep")
    tp = lax.axis_size("tp")
    zn = tp // CORES
    me = lax.axis_index("ep").astype(jnp.int32)
    place = lax.axis_index("tp").astype(jnp.int32)
    zi, core = place >> 1, place & 1
    scal = jnp.stack([me, core, zi])
    over_ep = lambda x, m: lax.ppermute(x, "ep", [(i, i ^ m) for i in range(ep)])
    over_core = lambda x: lax.ppermute(x, "tp", [(i, i ^ 1) for i in range(tp)])
    over_z = lambda x, m: lax.ppermute(x, "tp", [(i, i ^ (m * CORES)) for i in range(tp)])
    tie = lax.optimization_barrier
    assert expert_gate_weight.shape[0] == 1
    experts = ep
    rows, width = second_batch_tokens.shape
    sub = rows // tp
    capacity = max(2, sub * TOPK * 5 // (4 * experts))
    pieces = PIECES
    extra = extra_log_forget.T
    idx = chosen_expert_index.T
    wts = chosen_expert_weight.T

    weights = []
    for w in (expert_gate_weight, expert_up_weight, expert_down_weight):
        weights += [w, over_core(w)]
    wp = over_core(mixer_output_weight)

    st = final_state(forget_preactivation, value_input_rows, forget_floor_gap, extra)
    states = [over_ep(st, m) for m in range(1, ep)]

    tokens, _ = tie((second_batch_tokens, st))
    tokens = tokens.reshape(zn, CORES, sub, width)
    packed = pack(scal, tokens, idx, feedforward_norm_gain, experts, capacity)
    order = [ep - 1] + list(range(1, ep - 1))
    arrived = {0: packed[0]}
    for m in order:
        arrived[m] = over_ep(packed[m], m)

    q, _ = tie((query_preactivation, packed[1]))
    mixed = mixer(
        scal,
        states,
        q,
        forget_preactivation,
        value_input_rows,
        output_gate_preactivation,
        forget_floor_gap,
        extra,
        head_output_gain,
    )
    gathered = [mixed]
    for m in range(1, zn):
        chained = m % 2 == 1 and m > 1
        gathered.append(over_z(gathered[m - 1] if chained else mixed, 1 if chained else m))

    x0, _ = tie((arrived[0], mixed))
    (y1,), (y0,) = ffn([arrived[ep - 1], x0], weights, 1)
    late = ffn([arrived[m] for m in order[1:]], weights, pieces)
    first_back = over_ep(y1, ep - 1)
    back = [[over_ep(late[i][p], m) for i, m in enumerate(order[1:])] for p in range(pieces)]
    own, other = project(scal, gathered, mixer_output_weight, wp)
    other = over_core(other)
    mixer_output_first = (own + other.astype(f32)).astype(bf16)
    outs = []
    for p in range(pieces):
        ys = [y0] + back[p] + [first_back]
        parts = combine(scal, idx, wts, ys, p, pieces, zn, sub, capacity)
        total = parts[0].astype(f32)
        for m in range(1, zn):
            total = total + over_z(parts[m], m).astype(f32)
        outs.append(total.astype(bf16))
    return mixer_output_first, jnp.concatenate(outs, axis=1)


def solution(mesh):
    placed = (
        P("ep", "tp"),
        P("ep", "tp"),
        P("ep", "tp"),
        P("ep", "tp"),
        P("tp"),
        P("ep", "tp"),
        P("tp"),
        P(None, "tp"),
        P("ep", None),
        P(),
        P("ep", None),
        P("ep", None),
        P("ep", None, "tp"),
        P("ep", None, "tp"),
        P("ep", "tp", None),
    )

    return jax.shard_map(
        on_device,
        mesh=mesh,
        in_specs=placed,
        out_specs=(P("ep", "tp"), P(("ep", "tp"), None)),
        check_vma=False,
    )
```

profile of v0, /device:TPU:0, one launch (start us, length us, event | category | flops | bytes accessed | tf_op | source)
XLA Modules:
  0.0 162.7 jit_solution(16597704701495916755)
XLA Ops:
  0.6 0.6 collective-permute-start.10
  1.2 0.1 collective-permute-start.11
  1.3 0.4 collective-permute-start.9
  1.7 8.2 %final_state.1 = f32[136,128]{1,0:T(8,128)} custom-call(bf16[2048,256]{1,0:T(8,128)(2,1)} %refs_4_.4, bf16[2048,128]{1,0:T(8,128)(2,1)} %refs_5_.1, f32[1,256]{1,0:T(1,128)} %bitcast.19, f32[2,2048]{1,0:T(2,128)} %bitcast.11), custom_call_target="tpu_custom_call" | custom-call | flops 4000000000 | bytes 2000000 | tf_op jit(solution)/shard_map/final_state/pallas_call | solution.py:87
  9.9 2.6 %collective-permute-start = (f32[136,128]{1,0:T(8,128)}, f32[136,128]{1,0:T(8,128)S(1)}, u32[]{:S(2)}, u32[]{:S(2)}) collective-permute-start(f32[136,128]{1,0:T(8,128)} %final_state.1), channel_id=1, source_target_pairs={{0,8},{8,0},{16,24},{24,16},{1,9},{9,1},{17,25},{25,17},{2,10},{10... | collective-permute-start | bytes 208904 | tf_op jit(solution)/shard_map/ppermute | solution.py:410
  12.4 1.5 collective-permute-start.1
  14.0 0.6 pad_add_fusion.sc_ref
  14.6 0.9 collective-permute-done.refs_0_
  15.4 2.7 %collective-permute-start.2 = (f32[136,128]{1,0:T(8,128)}, f32[136,128]{1,0:T(8,128)S(1)}, u32[]{:S(2)}, u32[]{:S(2)}) collective-permute-start(f32[136,128]{1,0:T(8,128)} %final_state.1), channel_id=1, source_target_pairs={{0,24},{8,16},{16,8},{24,0},{1,25},{9,17},{17,9},{25,1},{2,26},{10... | collective-permute-start | bytes 208904 | tf_op jit(solution)/shard_map/ppermute | solution.py:410
  18.1 4.2 %pack.1 = (bf16[160,2048]{1,0:T(8,128)(2,1)}, bf16[160,2048]{1,0:T(8,128)(2,1)}, bf16[160,2048]{1,0:T(8,128)(2,1)}, bf16[160,2048]{1,0:T(8,128)(2,1)}) custom-call(s32[3]{0:T(128)} %pad_add_fusion.sc_ref, bf16[4,2,64,2048]{3,2,1,0:T(8,128)(2,1)} %bitcast.10, s32[2,512]{1,0:T(2,128)} %bitcast.14, f32[1,2048]{1,0:T(1,128)} %bitcast.13), custom_call_target="tpu_custom_call" | custom-call | flops 4000000000 | bytes 4000000 | tf_op jit(solution)/shard_map/pack/pallas_call | solution.py:272
  22.3 0.0 collective-permute-done.1.refs_1_
  22.3 0.1 collective-permute-start.6
  22.4 0.0 collective-permute-done.2.refs_2_
  22.4 0.0 copy-start.15
  22.4 0.5 copy-done.14
  23.0 0.1 copy-done.15
  23.1 15.6 %mixer.1.refs_0_ = bf16[2048,128]{1,0:T(8,128)(2,1)} custom-call(s32[3]{0:T(128)} %pad_add_fusion.sc_ref, f32[136,128]{1,0:T(8,128)} %copy-done.13, f32[136,128]{1,0:T(8,128)} %copy-done.14, f32[136,128]{1,0:T(8,128)} %copy-done.15, bf16[2048,256]{1,0:T(8,128)(2,1)} %refs_3_, bf16[2048,256]{1,0:T(8,128)(2,1)} %refs_4_.4, bf16[2048,128]{1,0:T(8,128)(2,1)} %refs_5_.1, ...), custom_call_target="tpu_custom_call" | custom-call | flops 12000000000 | bytes 4000000 | tf_op jit(solution)/shard_map/mixer/pallas_call | solution.py:171
  38.6 2.6 %collective-permute-start.4 = (bf16[2048,128]{1,0:T(8,128)(2,1)}, bf16[2048,128]{1,0:T(8,128)(2,1)S(1)}, u32[]{:S(2)}, u32[]{:S(2)}) collective-permute-start(bf16[2048,128]{1,0:T(8,128)(2,1)} %mixer.1.refs_0_), channel_id=1, source_target_pairs={{0,4},{1,5},{2,6},{3,7},{4,0},{5,1},{6,2},{7,3},{8,12},{9,13},{10,... | collective-permute-start | bytes 1572872 | tf_op jit(solution)/shard_map/ppermute | solution.py:412
  41.2 0.0 collective-permute-done.6.refs_5_
  41.2 1.6 collective-permute-start.3
  42.8 22.6 %collective-permute-done.4.refs_2_ = bf16[2048,128]{1,0:T(8,128)(2,1)S(1)} collective-permute-done((bf16[2048,128]{1,0:T(8,128)(2,1)}, bf16[2048,128]{1,0:T(8,128)(2,1)S(1)}, u32[]{:S(2)}, u32[]{:S(2)}) %collective-permute-start.4) | collective-permute-done | bytes 524320 | tf_op jit(solution)/shard_map/ppermute | solution.py:412
  65.4 0.7 collective-permute-start.5
  66.1 0.0 collective-permute-done.3.refs_1_
  66.1 0.5 collective-permute-start.8
  66.6 12.2 %collective-permute-done.5.refs_3_ = bf16[2048,128]{1,0:T(8,128)(2,1)S(1)} collective-permute-done((bf16[2048,128]{1,0:T(8,128)(2,1)S(1)}, bf16[2048,128]{1,0:T(8,128)(2,1)S(1)}, u32[]{:S(2)}, u32[]{:S(2)}) %collective-permute-start.5) | collective-permute-done | bytes 524320 | tf_op jit(solution)/shard_map/ppermute | solution.py:412
  78.8 0.8 copy-done.11
  79.6 0.5 collective-permute-start.12
  80.1 6.6 %project.1 = (f32[2048,256]{1,0:T(8,128)}, bf16[2048,256]{1,0:T(8,128)(2,1)}) custom-call(s32[3]{0:T(128)} %pad_add_fusion.sc_ref, bf16[2048,128]{1,0:T(8,128)(2,1)} %mixer.1.refs_0_, bf16[2048,128]{1,0:T(8,128)(2,1)} %copy-done.10, bf16[2048,128]{1,0:T(8,128)(2,1)} %copy-done.9, bf16[2048,128]{1,0:T(8,128)(2,1)} %copy-done.11, bf16[1024,256]{1,0:T(8,128)(2,1)} %refs_4_.5, ...), custom_call_target="tpu_custom_call" | custom-call | flops 2000000000 | bytes 6000000 | tf_op jit(solution)/shard_map/project/pallas_call | solution.py:211
  86.7 0.0 collective-permute-done.8.refs_0_
  86.7 0.1 collective-permute-start.13
  86.8 0.0 collective-permute-done.10.refs_5_
  86.8 0.7 copy-done.5
  87.5 0.0 collective-permute-start.7
  87.6 0.0 collective-permute-done.11.refs_7_
  87.6 0.0 collective-permute-done.9.refs_3_
  87.6 15.1 %ffn.2 = (bf16[160,2048]{1,0:T(8,128)(2,1)}, bf16[160,2048]{1,0:T(8,128)(2,1)}) custom-call(bf16[160,2048]{1,0:T(8,128)(2,1)} %copy-done.5, bf16[160,2048]{1,0:T(8,128)(2,1)} %get-tuple-element.32.refs_1_, bf16[1,2048,896]{2,1,0:T(8,128)(2,1)} %refs_2_.3, bf16[1,2048,896]{2,1,0:T(8,128)(2,1)} %collective-permute-done.9.refs_3_, ...), custom_call_target="tpu_custom_call" | custom-call | flops 8000000000 | bytes 25000000 | tf_op jit(solution)/shard_map/ffn/pallas_call | solution.py:328
  102.7 2.2 %collective-permute-start.16 = (bf16[160,2048]{1,0:T(8,128)(2,1)}, bf16[160,2048]{1,0:T(8,128)(2,1)}, u32[]{:S(2)}, u32[]{:S(2)}) collective-permute-start(bf16[160,2048]{1,0:T(8,128)(2,1)} %get-tuple-element.37), channel_id=1, source_target_pairs={{0,24},{8,16},{16,8},{24,0},{1,25},{9,17},{17,9},{25,1},{2,26},{10... | collective-permute-start | bytes 1966088 | tf_op jit(solution)/shard_map/ppermute | solution.py:410
  104.9 0.0 collective-permute-done.12.refs_0_
  104.9 0.0 collective-permute-done.13.refs_1_
  104.9 0.8 copy-done.6
  105.7 15.1 %ffn.3 = (bf16[160,1024]{1,0:T(8,128)(2,1)}, bf16[160,1024]{1,0:T(8,128)(2,1)}, bf16[160,1024]{1,0:T(8,128)(2,1)}, bf16[160,1024]{1,0:T(8,128)(2,1)}) custom-call(bf16[160,2048]{1,0:T(8,128)(2,1)} %collective-permute-done.12.refs_0_, bf16[160,2048]{1,0:T(8,128)(2,1)} %copy-done.6, bf16[1,2048,896]{2,1,0:T(8,128)(2,1)} %refs_2_.3, ...), custom_call_target="tpu_custom_call" | custom-call | flops 8000000000 | bytes 25000000 | tf_op jit(solution)/shard_map/ffn/pallas_call | solution.py:328
  120.8 0.6 collective-permute-start.14
  121.4 0.7 collective-permute-start.15
  122.1 1.5 collective-permute-start.20
  123.6 8.0 %collective-permute-done.14.refs_1_ = bf16[160,1024]{1,0:T(8,128)(2,1)S(1)} collective-permute-done((bf16[160,1024]{1,0:T(8,128)(2,1)}, bf16[160,1024]{1,0:T(8,128)(2,1)S(1)}, u32[]{:S(2)}, u32[]{:S(2)}) %collective-permute-start.14) | collective-permute-done | bytes 327712 | tf_op jit(solution)/shard_map/ppermute | solution.py:410
  131.7 0.7 collective-permute-start.21
  132.4 0.0 collective-permute-done.15.refs_2_
  132.4 0.0 collective-permute-done.16.refs_3_
  132.4 3.8 %combine.2 = (bf16[64,1024]{1,0:T(8,128)(2,1)}, bf16[64,1024]{1,0:T(8,128)(2,1)}, bf16[64,1024]{1,0:T(8,128)(2,1)}, bf16[64,1024]{1,0:T(8,128)(2,1)}) custom-call(s32[3]{0:T(128)} %pad_add_fusion.sc_ref, s32[2,512]{1,0:T(2,128)} %bitcast.15, f32[2,512]{1,0:T(2,128)} %bitcast.17, bf16[160,2048]{1,0:T(8,128)(2,1)} %get-tuple-element.33.refs_0_, ...), custom_call_target="tpu_custom_call" | custom-call | flops 1000000000 | bytes 2000000 | tf_op jit(solution)/shard_map/combine/pallas_call | solution.py:367
  136.2 1.1 collective-permute-start.17
  137.3 3.3 %collective-permute-start.18 = (bf16[64,1024]{1,0:T(8,128)(2,1)}, bf16[64,1024]{1,0:T(8,128)(2,1)S(1)}, u32[]{:S(2)}, u32[]{:S(2)}) collective-permute-start(bf16[64,1024]{1,0:T(8,128)(2,1)} %get-tuple-element.40), channel_id=1, source_target_pairs={{0,4},{1,5},{2,6},{3,7},{4,0},{5,1},{6,2},{7,3},{8,12},{9,13},{10,... | collective-permute-start | bytes 393224 | tf_op jit(solution)/shard_map/ppermute | solution.py:412
  140.6 0.0 collective-permute-done.7
  140.6 0.0 collective-permute-start.19
  140.6 1.2 add_convert_fusion
  141.9 0.0 collective-permute-done.21.refs_2_
  141.9 3.7 %combine.3 = (bf16[64,1024]{1,0:T(8,128)(2,1)}, bf16[64,1024]{1,0:T(8,128)(2,1)}, bf16[64,1024]{1,0:T(8,128)(2,1)}, bf16[64,1024]{1,0:T(8,128)(2,1)}) custom-call(s32[3]{0:T(128)} %pad_add_fusion.sc_ref, s32[2,512]{1,0:T(2,128)} %bitcast.16, f32[2,512]{1,0:T(2,128)} %bitcast.18, bf16[160,2048]{1,0:T(8,128)(2,1)} %get-tuple-element.33.refs_0_, ...), custom_call_target="tpu_custom_call" | custom-call | flops 1000000000 | bytes 2000000 | tf_op jit(solution)/shard_map/combine/pallas_call | solution.py:367
  145.6 0.6 collective-permute-start.22
  146.1 3.8 %collective-permute-start.23 = (bf16[64,1024]{1,0:T(8,128)(2,1)}, bf16[64,1024]{1,0:T(8,128)(2,1)S(1)}, u32[]{:S(2)}, u32[]{:S(2)}) collective-permute-start(bf16[64,1024]{1,0:T(8,128)(2,1)} %get-tuple-element.46), channel_id=1, source_target_pairs={{0,4},{1,5},{2,6},{3,7},{4,0},{5,1},{6,2},{7,3},{8,12},{9,13},{10,... | collective-permute-start | bytes 393224 | tf_op jit(solution)/shard_map/ppermute | solution.py:412
  150.0 0.0 collective-permute-start.24
  150.0 1.2 collective-permute-done.18
  151.1 1.0 add_convert_fusion.2
  152.1 8.8 %collective-permute-done.23 = bf16[64,1024]{1,0:T(8,128)(2,1)S(1)} collective-permute-done((bf16[64,1024]{1,0:T(8,128)(2,1)}, bf16[64,1024]{1,0:T(8,128)(2,1)S(1)}, u32[]{:S(2)}, u32[]{:S(2)}) %collective-permute-start.23) | collective-permute-done | bytes 131104 | tf_op jit(solution)/shard_map/ppermute | solution.py:412
  161.0 1.0 add_convert_fusion.1
  162.0 0.7 pad_maximum_fusion
  (31 shorter events, 0.1 us)
Async XLA Ops:
  0.6 86.2 %collective-permute-start.10 = (bf16[1,2048,896]{2,1,0:T(8,128)(2,1)}, bf16[1,2048,896]{2,1,0:T(8,128)(2,1)}, u32[]{:S(2)}, u32[]{:S(2)}) collective-permute-start(bf16[1,2048,896]{2,1,0:T(8,128)(2,1)} %refs_4_.7), channel_id=1, source_target_pairs={{0,1},{1,0},{2,3},{3,2},{4,5},{5,4},{6,7},{7,6},{8,9},{9,8},{10,11... | collective-permute-start | bytes 11010056 | tf_op jit(solution)/shard_map/ppermute | solution.py:411
  1.2 86.4 %collective-permute-start.11 = (bf16[1,896,2048]{2,1,0:T(8,128)(2,1)}, bf16[1,896,2048]{2,1,0:T(8,128)(2,1)}, u32[]{:S(2)}, u32[]{:S(2)}) collective-permute-start(bf16[1,896,2048]{2,1,0:T(8,128)(2,1)} %refs_6_.5), channel_id=1, source_target_pairs={{0,1},{1,0},{2,3},{3,2},{4,5},{5,4},{6,7},{7,6},{8,9},{9,8},{10,11... | collective-permute-start | bytes 11010056 | tf_op jit(solution)/shard_map/ppermute | solution.py:411
  1.3 86.3 %collective-permute-start.9 = (bf16[1,2048,896]{2,1,0:T(8,128)(2,1)}, bf16[1,2048,896]{2,1,0:T(8,128)(2,1)}, u32[]{:S(2)}, u32[]{:S(2)}) collective-permute-start(bf16[1,2048,896]{2,1,0:T(8,128)(2,1)} %refs_2_.3), channel_id=1, source_target_pairs={{0,1},{1,0},{2,3},{3,2},{4,5},{5,4},{6,7},{7,6},{8,9},{9,8},{10,11... | collective-permute-start | bytes 11010056 | tf_op jit(solution)/shard_map/ppermute | solution.py:411
  9.9 5.5 %collective-permute-start = (f32[136,128]{1,0:T(8,128)}, f32[136,128]{1,0:T(8,128)S(1)}, u32[]{:S(2)}, u32[]{:S(2)}) collective-permute-start(f32[136,128]{1,0:T(8,128)} %final_state.1), channel_id=1, source_target_pairs={{0,8},{8,0},{16,24},{24,16},{1,9},{9,1},{17,25},{25,17},{2,10},{10... | collective-permute-start | bytes 208904 | tf_op jit(solution)/shard_map/ppermute | solution.py:410
  12.4 9.9 %collective-permute-start.1 = (f32[136,128]{1,0:T(8,128)}, f32[136,128]{1,0:T(8,128)S(1)}, u32[]{:S(2)}, u32[]{:S(2)}) collective-permute-start(f32[136,128]{1,0:T(8,128)} %final_state.1), channel_id=1, source_target_pairs={{0,16},{8,24},{16,0},{24,8},{1,17},{9,25},{17,1},{25,9},{2,18},{10... | collective-permute-start | bytes 208904 | tf_op jit(solution)/shard_map/ppermute | solution.py:410
  15.4 6.9 %copy-start.13 = (f32[136,128]{1,0:T(8,128)}, f32[136,128]{1,0:T(8,128)S(1)}, u32[]{:S(2)}) copy-start(f32[136,128]{1,0:T(8,128)S(1)} %collective-permute-done.refs_0_) | copy-start | bytes 208900
  15.4 7.0 %collective-permute-start.2 = (f32[136,128]{1,0:T(8,128)}, f32[136,128]{1,0:T(8,128)S(1)}, u32[]{:S(2)}, u32[]{:S(2)}) collective-permute-start(f32[136,128]{1,0:T(8,128)} %final_state.1), channel_id=1, source_target_pairs={{0,24},{8,16},{16,8},{24,0},{1,25},{9,17},{17,9},{25,1},{2,26},{10... | collective-permute-start | bytes 208904 | tf_op jit(solution)/shard_map/ppermute | solution.py:410
  18.1 4.2 %copy-start.7 = (bf16[1024,256]{1,0:T(8,128)(2,1)S(1)}, bf16[1024,256]{1,0:T(8,128)(2,1)}, u32[]{:S(2)}) copy-start(bf16[1024,256]{1,0:T(8,128)(2,1)} %refs_4_.5) | copy-start | bytes 1572868
  22.3 0.6 copy-start.14
  22.3 18.9 %collective-permute-start.6 = (bf16[1024,256]{1,0:T(8,128)(2,1)S(1)}, bf16[1024,256]{1,0:T(8,128)(2,1)S(1)}, u32[]{:S(2)}, u32[]{:S(2)}) collective-permute-start(bf16[1024,256]{1,0:T(8,128)(2,1)S(1)} %copy-done.7), channel_id=1, source_target_pairs={{0,1},{1,0},{2,3},{3,2},{4,5},{5,4},{6,7},{7,6},{8,9},{9,8},{10,11... | collective-permute-start | bytes 1572872 | tf_op jit(solution)/shard_map/ppermute | solution.py:411
  22.4 0.6 copy-start.15
  23.1 43.0 %copy-start.4 = (bf16[160,2048]{1,0:T(8,128)(2,1)S(1)}, bf16[160,2048]{1,0:T(8,128)(2,1)}, u32[]{:S(2)}) copy-start(bf16[160,2048]{1,0:T(8,128)(2,1)} %get-tuple-element.30) | copy-start | bytes 1966084
  23.1 56.5 %copy-start.3 = (bf16[160,2048]{1,0:T(8,128)(2,1)S(1)}, bf16[160,2048]{1,0:T(8,128)(2,1)}, u32[]{:S(2)}) copy-start(bf16[160,2048]{1,0:T(8,128)(2,1)} %get-tuple-element.26) | copy-start | bytes 1966084
  38.6 26.8 %collective-permute-start.4 = (bf16[2048,128]{1,0:T(8,128)(2,1)}, bf16[2048,128]{1,0:T(8,128)(2,1)S(1)}, u32[]{:S(2)}, u32[]{:S(2)}) collective-permute-start(bf16[2048,128]{1,0:T(8,128)(2,1)} %mixer.1.refs_0_), channel_id=1, source_target_pairs={{0,4},{1,5},{2,6},{3,7},{4,0},{5,1},{6,2},{7,3},{8,12},{9,13},{10,... | collective-permute-start | bytes 1572872 | tf_op jit(solution)/shard_map/ppermute | solution.py:412
  41.2 25.4 %copy-start.8 = (bf16[1024,256]{1,0:T(8,128)(2,1)}, bf16[1024,256]{1,0:T(8,128)(2,1)S(1)}, u32[]{:S(2)}) copy-start(bf16[1024,256]{1,0:T(8,128)(2,1)S(1)} %collective-permute-done.6.refs_5_) | copy-start | bytes 1572868
  41.2 24.8 %collective-permute-start.3 = (bf16[2048,128]{1,0:T(8,128)(2,1)}, bf16[2048,128]{1,0:T(8,128)(2,1)S(1)}, u32[]{:S(2)}, u32[]{:S(2)}) collective-permute-start(bf16[2048,128]{1,0:T(8,128)(2,1)} %mixer.1.refs_0_), channel_id=1, source_target_pairs={{0,2},{1,3},{2,0},{3,1},{4,6},{5,7},{6,4},{7,5},{8,10},{9,11},{10,... | collective-permute-start | bytes 1572872 | tf_op jit(solution)/shard_map/ppermute | solution.py:412
  65.4 1.2 copy-start.9
  65.4 13.4 %collective-permute-start.5 = (bf16[2048,128]{1,0:T(8,128)(2,1)S(1)}, bf16[2048,128]{1,0:T(8,128)(2,1)S(1)}, u32[]{:S(2)}, u32[]{:S(2)}) collective-permute-start(bf16[2048,128]{1,0:T(8,128)(2,1)S(1)} %collective-permute-done.4.refs_2_), channel_id=1, source_target_pairs={{0,2},{1,3},{2,0},{3,1},{4,6},{5,7},{6,4},{7,5},{8,10},{9,11},{10,... | collective-permute-start | bytes 1572872 | tf_op jit(solution)/shard_map/ppermute | solution.py:412
  66.1 14.1 %copy-start.10 = (bf16[2048,128]{1,0:T(8,128)(2,1)}, bf16[2048,128]{1,0:T(8,128)(2,1)S(1)}, u32[]{:S(2)}) copy-start(bf16[2048,128]{1,0:T(8,128)(2,1)S(1)} %collective-permute-done.3.refs_1_) | copy-start | bytes 1572868
  66.1 20.6 %collective-permute-start.8 = (bf16[160,2048]{1,0:T(8,128)(2,1)S(1)}, bf16[160,2048]{1,0:T(8,128)(2,1)S(1)}, u32[]{:S(2)}, u32[]{:S(2)}) collective-permute-start(bf16[160,2048]{1,0:T(8,128)(2,1)S(1)} %copy-done.4), channel_id=1, source_target_pairs={{0,24},{8,16},{16,8},{24,0},{1,25},{9,17},{17,9},{25,1},{2,26},{10... | collective-permute-start | bytes 1966088 | tf_op jit(solution)/shard_map/ppermute | solution.py:410
  66.6 20.1 %copy-start.2 = (bf16[160,2048]{1,0:T(8,128)(2,1)S(1)}, bf16[160,2048]{1,0:T(8,128)(2,1)}, u32[]{:S(2)}) copy-start(bf16[160,2048]{1,0:T(8,128)(2,1)} %get-tuple-element.34) | copy-start | bytes 1966084
  78.8 0.8 copy-start.11
  79.6 25.3 %collective-permute-start.12 = (bf16[160,2048]{1,0:T(8,128)(2,1)S(1)}, bf16[160,2048]{1,0:T(8,128)(2,1)}, u32[]{:S(2)}, u32[]{:S(2)}) collective-permute-start(bf16[160,2048]{1,0:T(8,128)(2,1)S(1)} %copy-done.3), channel_id=1, source_target_pairs={{0,8},{8,0},{16,24},{24,16},{1,9},{9,1},{17,25},{25,17},{2,10},{10... | collective-permute-start | bytes 1966088 | tf_op jit(solution)/shard_map/ppermute | solution.py:410
  86.7 0.8 copy-start.5
  86.7 18.2 %collective-permute-start.13 = (bf16[160,2048]{1,0:T(8,128)(2,1)S(1)}, bf16[160,2048]{1,0:T(8,128)(2,1)S(1)}, u32[]{:S(2)}, u32[]{:S(2)}) collective-permute-start(bf16[160,2048]{1,0:T(8,128)(2,1)S(1)} %copy-done.2), channel_id=1, source_target_pairs={{0,16},{8,24},{16,0},{24,8},{1,17},{9,25},{17,1},{25,9},{2,18},{10... | collective-permute-start | bytes 1966088 | tf_op jit(solution)/shard_map/ppermute | solution.py:410
  87.5 53.1 %collective-permute-start.7 = (bf16[2048,256]{1,0:T(8,128)(2,1)}, bf16[2048,256]{1,0:T(8,128)(2,1)S(1)}, u32[]{:S(2)}, u32[]{:S(2)}) collective-permute-start(bf16[2048,256]{1,0:T(8,128)(2,1)} %get-tuple-element.29), channel_id=1, source_target_pairs={{0,1},{1,0},{2,3},{3,2},{4,5},{5,4},{6,7},{7,6},{8,9},{9,8},{10,11... | collective-permute-start | bytes 3145736 | tf_op jit(solution)/shard_map/ppermute | solution.py:411
  102.7 29.7 %collective-permute-start.16 = (bf16[160,2048]{1,0:T(8,128)(2,1)}, bf16[160,2048]{1,0:T(8,128)(2,1)}, u32[]{:S(2)}, u32[]{:S(2)}) collective-permute-start(bf16[160,2048]{1,0:T(8,128)(2,1)} %get-tuple-element.37), channel_id=1, source_target_pairs={{0,24},{8,16},{16,8},{24,0},{1,25},{9,17},{17,9},{25,1},{2,26},{10... | collective-permute-start | bytes 1966088 | tf_op jit(solution)/shard_map/ppermute | solution.py:410
  104.9 0.8 copy-start.6
  120.8 19.8 %copy-start = (f32[2048,256]{1,0:T(8,128)S(1)}, f32[2048,256]{1,0:T(8,128)}, u32[]{:S(2)}) copy-start(f32[2048,256]{1,0:T(8,128)} %get-tuple-element.28) | copy-start | bytes 6291460
  120.8 10.9 %collective-permute-start.14 = (bf16[160,1024]{1,0:T(8,128)(2,1)}, bf16[160,1024]{1,0:T(8,128)(2,1)S(1)}, u32[]{:S(2)}, u32[]{:S(2)}) collective-permute-start(bf16[160,1024]{1,0:T(8,128)(2,1)} %get-tuple-element.35), channel_id=1, source_target_pairs={{0,8},{8,0},{16,24},{24,16},{1,9},{9,1},{17,25},{25,17},{2,10},{10... | collective-permute-start | bytes 983048 | tf_op jit(solution)/shard_map/ppermute | solution.py:410
  121.4 11.0 %collective-permute-start.15 = (bf16[160,1024]{1,0:T(8,128)(2,1)}, bf16[160,1024]{1,0:T(8,128)(2,1)}, u32[]{:S(2)}, u32[]{:S(2)}) collective-permute-start(bf16[160,1024]{1,0:T(8,128)(2,1)} %get-tuple-element.36), channel_id=1, source_target_pairs={{0,16},{8,24},{16,0},{24,8},{1,17},{9,25},{17,1},{25,9},{2,18},{10... | collective-permute-start | bytes 983048 | tf_op jit(solution)/shard_map/ppermute | solution.py:410
  122.1 19.7 %collective-permute-start.20 = (bf16[160,1024]{1,0:T(8,128)(2,1)}, bf16[160,1024]{1,0:T(8,128)(2,1)}, u32[]{:S(2)}, u32[]{:S(2)}) collective-permute-start(bf16[160,1024]{1,0:T(8,128)(2,1)} %get-tuple-element.42), channel_id=1, source_target_pairs={{0,8},{8,0},{16,24},{24,16},{1,9},{9,1},{17,25},{25,17},{2,10},{10... | collective-permute-start | bytes 983048 | tf_op jit(solution)/shard_map/ppermute | solution.py:410
  131.7 0.7 copy-start.12
  131.7 10.2 %collective-permute-start.21 = (bf16[160,1024]{1,0:T(8,128)(2,1)}, bf16[160,1024]{1,0:T(8,128)(2,1)}, u32[]{:S(2)}, u32[]{:S(2)}) collective-permute-start(bf16[160,1024]{1,0:T(8,128)(2,1)} %get-tuple-element.43), channel_id=1, source_target_pairs={{0,16},{8,24},{16,0},{24,8},{1,17},{9,25},{17,1},{25,9},{2,18},{10... | collective-permute-start | bytes 983048 | tf_op jit(solution)/shard_map/ppermute | solution.py:410
  136.2 13.8 %collective-permute-start.17 = (bf16[64,1024]{1,0:T(8,128)(2,1)}, bf16[64,1024]{1,0:T(8,128)(2,1)S(1)}, u32[]{:S(2)}, u32[]{:S(2)}) collective-permute-start(bf16[64,1024]{1,0:T(8,128)(2,1)} %get-tuple-element.39), channel_id=1, source_target_pairs={{0,2},{1,3},{2,0},{3,1},{4,6},{5,7},{6,4},{7,5},{8,10},{9,11},{10,... | collective-permute-start | bytes 393224 | tf_op jit(solution)/shard_map/ppermute | solution.py:412
  137.3 13.8 %collective-permute-start.18 = (bf16[64,1024]{1,0:T(8,128)(2,1)}, bf16[64,1024]{1,0:T(8,128)(2,1)S(1)}, u32[]{:S(2)}, u32[]{:S(2)}) collective-permute-start(bf16[64,1024]{1,0:T(8,128)(2,1)} %get-tuple-element.40), channel_id=1, source_target_pairs={{0,4},{1,5},{2,6},{3,7},{4,0},{5,1},{6,2},{7,3},{8,12},{9,13},{10,... | collective-permute-start | bytes 393224 | tf_op jit(solution)/shard_map/ppermute | solution.py:412
  140.6 10.5 %collective-permute-start.19 = (bf16[64,1024]{1,0:T(8,128)(2,1)}, bf16[64,1024]{1,0:T(8,128)(2,1)}, u32[]{:S(2)}, u32[]{:S(2)}) collective-permute-start(bf16[64,1024]{1,0:T(8,128)(2,1)} %get-tuple-element.41), channel_id=1, source_target_pairs={{0,6},{1,7},{2,4},{3,5},{4,2},{5,3},{6,0},{7,1},{8,14},{9,15},{10,... | collective-permute-start | bytes 393224 | tf_op jit(solution)/shard_map/ppermute | solution.py:412
  140.6 10.5 %copy-start.1 = (bf16[64,1024]{1,0:T(8,128)(2,1)S(1)}, bf16[64,1024]{1,0:T(8,128)(2,1)}, u32[]{:S(2)}) copy-start(bf16[64,1024]{1,0:T(8,128)(2,1)} %get-tuple-element.38) | copy-start | bytes 393220
  145.6 6.5 %collective-permute-start.22 = (bf16[64,1024]{1,0:T(8,128)(2,1)}, bf16[64,1024]{1,0:T(8,128)(2,1)S(1)}, u32[]{:S(2)}, u32[]{:S(2)}) collective-permute-start(bf16[64,1024]{1,0:T(8,128)(2,1)} %get-tuple-element.45), channel_id=1, source_target_pairs={{0,2},{1,3},{2,0},{3,1},{4,6},{5,7},{6,4},{7,5},{8,10},{9,11},{10,... | collective-permute-start | bytes 393224 | tf_op jit(solution)/shard_map/ppermute | solution.py:412
  146.1 14.8 %collective-permute-start.23 = (bf16[64,1024]{1,0:T(8,128)(2,1)}, bf16[64,1024]{1,0:T(8,128)(2,1)S(1)}, u32[]{:S(2)}, u32[]{:S(2)}) collective-permute-start(bf16[64,1024]{1,0:T(8,128)(2,1)} %get-tuple-element.46), channel_id=1, source_target_pairs={{0,4},{1,5},{2,6},{3,7},{4,0},{5,1},{6,2},{7,3},{8,12},{9,13},{10,... | collective-permute-start | bytes 393224 | tf_op jit(solution)/shard_map/ppermute | solution.py:412
  150.0 11.0 %collective-permute-start.24 = (bf16[64,1024]{1,0:T(8,128)(2,1)}, bf16[64,1024]{1,0:T(8,128)(2,1)S(1)}, u32[]{:S(2)}, u32[]{:S(2)}) collective-permute-start(bf16[64,1024]{1,0:T(8,128)(2,1)} %get-tuple-element.47), channel_id=1, source_target_pairs={{0,6},{1,7},{2,4},{3,5},{4,2},{5,3},{6,0},{7,1},{8,14},{9,15},{10,... | collective-permute-start | bytes 393224 | tf_op jit(solution)/shard_map/ppermute | solution.py:412
where the time goes:
time: 163 us
  Pallas kernels  72.1 us (44%)
  waiting for transfers between devices  53.7 us (33%)
  starting transfers between devices  28.5 us (17%)
  other arithmetic  4.5 us (3%)
  local copies, waits for them, and re-layouts  3.04 us (2%)
    ppermute x9, waiting for transfers between devices, on_device(): lax.ppermute(x, 'tp', [(i, i ^ m * CORES) for i in range(tp)])  44.8 us
    pallas_call x2, Pallas kernels, ffn(): pl.pallas_call(functools.partial(ffn_body, count, pieces), grid=(hidden /...  30.1 us
    pallas_call x1, Pallas kernels, mixer(): pl.pallas_call(functools.partial(mixer_body, heads, ep, rows), grid_spec=...  15.6 us
    ppermute x11, starting transfers between devices, on_device(): lax.ppermute(x, 'ep', [(i, i ^ m) for i in range(ep)])  13.7 us
    ppermute x9, starting transfers between devices, on_device(): lax.ppermute(x, 'tp', [(i, i ^ m * CORES) for i in range(tp)])  13.7 us
    ppermute x11, waiting for transfers between devices, on_device(): lax.ppermute(x, 'ep', [(i, i ^ m) for i in range(ep)])  8.92 us
    pallas_call x1, Pallas kernels, final_state(): pl.pallas_call(functools.partial(state_body, heads, rows), grid=(length /...  8.2 us
    pallas_call x2, Pallas kernels, combine(): pl.pallas_call(functools.partial(combine_body, experts, capacity, zn), gr...  7.5 us
  transfers between devices with their start and end apart: 25, of which 6 were waited for; matrix products, arithmetic and copies ran while one was open for 2% of the time, Pallas kernels for 44%

commit v1 on v0

--- a/solution.py
+++ b/solution.py
@@ -13,6 +13,10 @@
 TOPK = 2
 CORES = 2
 PIECES = 2
+STATE_ROWS = 2048
+MIXER_ROWS = 2048
+FFN_VMEM = 36 * 1024 * 1024
+VMEM = 20 * 1024 * 1024
 epsilon = 1e-06
 f32 = jnp.float32
 bf16 = jnp.bfloat16
@@ -28,15 +32,15 @@
 
 
 def sigmoid(x):
-    return 1.0 / (1.0 + jnp.exp(-x))
-
-
-def forget_log(heads, f_ref, gap_ref, extra_ref):
-    key = gap_ref[...] * sigmoid(-f_ref[...].astype(f32))
+    return 0.5 + 0.5 * jnp.tanh(0.5 * x)
+
+
+def forget_log(heads, f, gap, extra):
+    key = gap * sigmoid(-f.astype(f32))
     kw = heads * KEY_DIM
     pick = lax.broadcasted_iota(jnp.int32, (heads, kw), 1) // KEY_DIM
     pick = (pick == lax.broadcasted_iota(jnp.int32, (heads, kw), 0)).astype(bf16)
-    hi, lo = split2(extra_ref[...])
+    hi, lo = split2(extra)
     extra = mm(hi, pick, ((0,), (0,))) + mm(lo, pick, ((0,), (0,)))
     return key, jnp.log(1.0 - key) + extra
 
@@ -56,15 +60,19 @@
         s_ref[...] = jnp.zeros_like(s_ref)
         l_ref[...] = jnp.zeros_like(l_ref)
 
-    key, logf = forget_log(heads, f_ref, gap_ref, extra_ref)
     row = lax.broadcasted_iota(jnp.int32, (rows, rows), 0)
     later = (row < lax.broadcasted_iota(jnp.int32, (rows, rows), 1)).astype(bf16)
-    hi, lo = split2(logf)
-    rest = mm(later, hi) + mm(later, lo)
-    whole = rest[0:1] + logf[0:1]
-    ks = (key * jnp.exp(rest)).astype(bf16)
-    s = s_ref[...] * jnp.exp(whole) + mm(v_ref[...], ks, ((0,), (0,)))
-    l = l_ref[...] + whole
+    s = s_ref[...]
+    l = l_ref[...]
+    for at in range(0, f_ref.shape[0], rows):
+        rs = slice(at, at + rows)
+        key, logf = forget_log(heads, f_ref[rs, :], gap_ref[...], extra_ref[:, rs])
+        hi, lo = split2(logf)
+        rest = mm(later, hi) + mm(later, lo)
+        whole = rest[0:1] + logf[0:1]
+        ks = (key * jnp.exp(rest)).astype(bf16)
+        s = s * jnp.exp(whole) + mm(v_ref[rs, :], ks, ((0,), (0,)))
+        l = l + whole
     s_ref[...] = s
     l_ref[...] = l
 
@@ -81,17 +89,18 @@
     length, kw = f.shape
     heads = kw // KEY_DIM
     vw = heads * VAL_DIM
-    rows = 4 * BLOCK
+    rows = min(length, STATE_ROWS)
     rows_of = lambda w: pl.BlockSpec((rows, w), lambda i: (i, 0))
     whole = lambda r, w: pl.BlockSpec((r, w), lambda i: (0, 0))
     return pl.pallas_call(
-        functools.partial(state_body, heads, rows),
+        functools.partial(state_body, heads, 4 * BLOCK),
         grid=(length // rows,),
         in_specs=[rows_of(kw), rows_of(vw), whole(1, kw), pl.BlockSpec((heads, rows), lambda i: (0, i))],
         out_specs=whole(vw + 8, KEY_DIM),
         out_shape=jax.ShapeDtypeStruct((vw + 8, KEY_DIM), f32),
         scratch_shapes=[pltpu.VMEM((vw, kw), f32), pltpu.VMEM((1, kw), f32)],
         cost_estimate=pl.CostEstimate(flops=4 * 10**9, bytes_accessed=2 * 10**6, transcendentals=10**6),
+        compiler_params=pltpu.CompilerParams(vmem_limit_bytes=VMEM),
         name="final_state",
     )(f, v, gap.reshape(1, kw), extra)
 
@@ -119,45 +128,49 @@
         for h in range(heads):
             s_ref[h * VAL_DIM : (h + 1) * VAL_DIM, h * KEY_DIM : (h + 1) * KEY_DIM] = carried[h]
 
-    q = q_ref[...].astype(f32)
-    q = q * sigmoid(q)
-    key, logf = forget_log(heads, f_ref, gap_ref, extra_ref)
     row = lax.broadcasted_iota(jnp.int32, (rows, rows), 0)
     col = lax.broadcasted_iota(jnp.int32, (rows, rows), 1)
     causal = (row >= col) & (row // BLOCK == col // BLOCK)
     tri = causal.astype(bf16)
-    hi, lo = split2(logf)
-    cum = mm(tri, hi) + mm(tri, lo)
-    v = v_ref[...]
-    finals = [cum[(b + 1) * BLOCK - 1 : (b + 1) * BLOCK] for b in range(blocks)]
-    fin = jnp.concatenate([jnp.broadcast_to(x, (BLOCK, kw)) for x in finals], axis=0)
-    qs = (q * jnp.exp(cum - fin)).astype(bf16)
-    ks = (key * jnp.exp(fin - cum)).astype(bf16)
-    qc = (q * jnp.exp(cum)).astype(bf16)
-    within = []
-    for h in range(heads):
-        ksl = slice(h * KEY_DIM, (h + 1) * KEY_DIM)
-        sc = mm(qs[:, ksl], ks[:, ksl], ((1,), (1,)))
-        sc = jnp.where(causal, sc, 0.0).astype(bf16)
-        within.append(mm(sc, v[:, h * VAL_DIM : (h + 1) * VAL_DIM]))
-    within = jnp.concatenate(within, axis=1)
     same = same_head(heads)
-    s = s_ref[...]
-    across = []
-    for b in range(blocks):
-        rs = slice(b * BLOCK, (b + 1) * BLOCK)
-        across.append(mm(qc[rs], s.astype(bf16), ((1,), (1,))))
-        upd = jnp.where(same, mm(v[rs], ks[rs], ((0,), (0,))), 0.0)
-        s = s * jnp.exp(finals[b]) + upd
-    s_ref[...] = s
-    rec = within + jnp.concatenate(across, axis=0)
     a = lax.broadcasted_iota(jnp.int32, (vw, vw), 0) // VAL_DIM
     b = lax.broadcasted_iota(jnp.int32, (vw, vw), 1) // VAL_DIM
     ones = (a == b).astype(bf16)
-    hi, lo = split2(rec * rec)
-    mean = (mm(hi, ones) + mm(lo, ones)) * (1.0 / VAL_DIM)
-    g = gate_ref[...].astype(f32)
-    mixed_ref[...] = (rec * lax.rsqrt(mean + epsilon) * gain_ref[...] * (g * sigmoid(g))).astype(bf16)
+    s = s_ref[...]
+    for at in range(0, q_ref.shape[0], rows):
+        part = slice(at, at + rows)
+        q = q_ref[part, :].astype(f32)
+        q = q * sigmoid(q)
+        key, logf = forget_log(heads, f_ref[part, :], gap_ref[...], extra_ref[:, part])
+        hi, lo = split2(logf)
+        cum = mm(tri, hi) + mm(tri, lo)
+        v = v_ref[part, :]
+        finals = [cum[(b + 1) * BLOCK - 1 : (b + 1) * BLOCK] for b in range(blocks)]
+        fin = jnp.concatenate([jnp.broadcast_to(x, (BLOCK, kw)) for x in finals], axis=0)
+        qs = (q * jnp.exp(cum - fin)).astype(bf16)
+        ks = (key * jnp.exp(fin - cum)).astype(bf16)
+        qc = (q * jnp.exp(cum)).astype(bf16)
+        within = []
+        for h in range(heads):
+            ksl = slice(h * KEY_DIM, (h + 1) * KEY_DIM)
+            sc = mm(qs[:, ksl], ks[:, ksl], ((1,), (1,)))
+            sc = jnp.where(causal, sc, 0.0).astype(bf16)
+            within.append(mm(sc, v[:, h * VAL_DIM : (h + 1) * VAL_DIM]))
+        within = jnp.concatenate(within, axis=1)
+        across = []
+        for b in range(blocks):
+            rs = slice(b * BLOCK, (b + 1) * BLOCK)
+            across.append(mm(qc[rs], s.astype(bf16), ((1,), (1,))))
+            upd = jnp.where(same, mm(v[rs], ks[rs], ((0,), (0,))), 0.0)
+            s = s * jnp.exp(finals[b]) + upd
+        rec = within + jnp.concatenate(across, axis=0)
+        hi, lo = split2(rec * rec)
+        mean = (mm(hi, ones) + mm(lo, ones)) * (1.0 / VAL_DIM)
+        g = gate_ref[part, :].astype(f32)
+        mixed_ref[part, :] = (
+            rec * lax.rsqrt(mean + epsilon) * gain_ref[...] * (g * sigmoid(g))
+        ).astype(bf16)
+    s_ref[...] = s
 
 
 def mixer(scal, others, q, f, v, gate, gap, extra, gain):
@@ -165,11 +178,11 @@
     heads = kw // KEY_DIM
     vw = heads * VAL_DIM
     ep = len(others) + 1
-    rows = 4 * BLOCK
+    rows = min(length, MIXER_ROWS)
     rows_of = lambda w: pl.BlockSpec((rows, w), lambda i, s: (i, 0))
     whole = lambda r, w: pl.BlockSpec((r, w), lambda i, s: (0, 0))
     return pl.pallas_call(
-        functools.partial(mixer_body, heads, ep, rows),
+        functools.partial(mixer_body, heads, ep, 4 * BLOCK),
         grid_spec=pltpu.PrefetchScalarGridSpec(
             num_scalar_prefetch=1,
             grid=(length // rows,),
@@ -181,6 +194,7 @@
         ),
         out_shape=jax.ShapeDtypeStruct((length, vw), bf16),
         cost_estimate=pl.CostEstimate(flops=12 * 10**9, bytes_accessed=4 * 10**6, transcendentals=10**6),
+        compiler_params=pltpu.CompilerParams(vmem_limit_bytes=VMEM),
         name="mixer",
     )(scal, *others, q, f, v, gate, gap.reshape(1, kw), extra, gain.reshape(1, vw))
 
@@ -204,7 +218,7 @@
 def project(scal, gathered, w, wp):
     length, vw = gathered[0].shape
     zn = len(gathered)
-    rows = min(length, 512)
+    rows = min(length, 1024)
     rows_of = lambda n: pl.BlockSpec((rows, n), lambda i, s: (i, 0))
     whole = pl.BlockSpec(w.shape, lambda i, s: (0, 0))
     width = w.shape[1]
@@ -221,8 +235,29 @@
             jax.ShapeDtypeStruct((length, width), bf16),
         ],
         cost_estimate=pl.CostEstimate(flops=2 * 10**9, bytes_accessed=6 * 10**6, transcendentals=0),
+        compiler_params=pltpu.CompilerParams(vmem_limit_bytes=VMEM),
         name="project",
     )(scal, *gathered, w, wp)
+
+
+def join_body(own_ref, other_ref, out_ref):
+    out_ref[...] = (own_ref[...] + other_ref[...].astype(f32)).astype(bf16)
+
+
+def join(own, other):
+    length, width = own.shape
+    rows = min(length, 1024)
+    spec = pl.BlockSpec((rows, width), lambda i: (i, 0))
+    return pl.pallas_call(
+        join_body,
+        grid=(length // rows,),
+        in_specs=[spec, spec],
+        out_specs=spec,
+        out_shape=jax.ShapeDtypeStruct(own.shape, bf16),
+        cost_estimate=pl.CostEstimate(flops=10**6, bytes_accessed=4 * 10**6, transcendentals=0),
+        compiler_params=pltpu.CompilerParams(vmem_limit_bytes=VMEM),
+        name="join",
+    )(own, other)
 
 
 def own_lanes(x, zn, sub, core):
@@ -283,56 +318,91 @@
         ),
         out_shape=[shape] * experts,
         cost_estimate=pl.CostEstimate(flops=4 * 10**9, bytes_accessed=4 * 10**6, transcendentals=10**3),
+        compiler_params=pltpu.CompilerParams(vmem_limit_bytes=VMEM),
         name="pack",
     )(scal, tokens, idx, gain.reshape(1, width))
 
 
-def ffn_body(count, pieces, *refs):
+def hidden_chunks(hidden):
+    units, unit = (hidden // 128, 128) if hidden % 128 == 0 else (1, hidden)
+    out, step = [], 1
+    while units:
+        take = min(step, units)
+        if units - take < step:
+            take = units
+        out.append(take * unit)
+        units -= take
+        step *= 2
+    return out
+
+
+def ffn_body(count, pieces, chunks, *refs):
     xs = refs[:count]
-    wg, wgp, wu, wup, wd, wdp = refs[count : count + 6]
-    outs = refs[count + 6 : -2]
-    x_ref, acc_ref = refs[-2:]
-    step = pl.program_id(0)
+    sources = refs[count : count + 6]
+    outs = refs[count + 6 : count + 6 + count * pieces]
+    scratch = refs[count + 6 + count * pieces :]
+    x_ref, acc_ref, sems = scratch[0], scratch[1], scratch[2]
+    buffers = scratch[3:]
     per = xs[0].shape[0]
 
-    @pl.when(step == 0)
-    def _():
-        x_ref[...] = jnp.concatenate([x[...] for x in xs], axis=0)
-        acc_ref[...] = jnp.zeros_like(acc_ref)
-
-    x = x_ref[...]
-    g = mm(x, jnp.concatenate([wg[0], wgp[0]], axis=1))
-    u = mm(x, jnp.concatenate([wu[0], wup[0]], axis=1))
-    h = (g * sigmoid(g) * u).astype(bf16)
-    acc_ref[...] += mm(h, jnp.concatenate([wd[0], wdp[0]], axis=0))
-
-    @pl.when(step == pl.num_programs(0) - 1)
-    def _():
-        cols = x_ref.shape[1] // pieces
-        for i in range(count):
-            for p in range(pieces):
-                outs[i * pieces + p][...] = acc_ref[
-                    i * per : (i + 1) * per, p * cols : (p + 1) * cols
-                ].astype(bf16)
+    def copies(c):
+        at = sum(chunks[:c])
+        span = pl.ds(at, chunks[c])
+        for k in range(3):
+            for side in range(2):
+                src = sources[2 * k + side].at[0]
+                src = src.at[span, :] if k == 2 else src.at[:, span]
+                yield pltpu.make_async_copy(src, buffers[3 * c + k].at[side], sems.at[c, 2 * k + side])
+
+    for c in range(len(chunks)):
+        for copy in copies(c):
+            copy.start()
+    x_ref[...] = jnp.concatenate([x[...] for x in xs], axis=0)
+    for c in range(len(chunks)):
+        for copy in copies(c):
+            copy.wait()
+        bg, bu, bd = buffers[3 * c : 3 * c + 3]
+        x = x_ref[...]
+        g = mm(x, jnp.concatenate([bg[0], bg[1]], axis=1))
+        u = mm(x, jnp.concatenate([bu[0], bu[1]], axis=1))
+        h = (g * sigmoid(g) * u).astype(bf16)
+        part = mm(h, jnp.concatenate([bd[0], bd[1]], axis=0))
+        if c == 0 and len(chunks) > 1:
+            acc_ref[...] = part
+        elif c + 1 < len(chunks):
+            acc_ref[...] += part
+        else:
+            total = part if c == 0 else acc_ref[...] + part
+            cols = total.shape[1] // pieces
+            for i in range(count):
+                for p in range(pieces):
+                    piece = total[i * per : (i + 1) * per, p * cols : (p + 1) * cols]
+                    outs[i * pieces + p][...] = piece.astype(bf16)
 
 
 def ffn(xs, weights, pieces):
     count = len(xs)
     per, width = xs[0].shape
     hidden = weights[0].shape[2]
-    chunk = 128 if hidden % 128 == 0 else hidden
-    whole = pl.BlockSpec((per, width), lambda i: (0, 0))
-    out = pl.BlockSpec((per, width // pieces), lambda i: (0, 0))
-    up = pl.BlockSpec((1, width, chunk), lambda i: (0, 0, i))
-    down = pl.BlockSpec((1, chunk, width), lambda i: (0, i, 0))
+    chunks = hidden_chunks(hidden)
+    buffers = []
+    for c in chunks:
+        buffers += [pltpu.VMEM((2, width, c), bf16), pltpu.VMEM((2, width, c), bf16), pltpu.VMEM((2, c, width), bf16)]
+    whole = pl.BlockSpec((per, width), lambda: (0, 0))
+    out = pl.BlockSpec((per, width // pieces), lambda: (0, 0))
     outs = pl.pallas_call(
-        functools.partial(ffn_body, count, pieces),
-        grid=(hidden // chunk,),
-        in_specs=[whole] * count + [up] * 4 + [down] * 2,
+        functools.partial(ffn_body, count, pieces, chunks),
+        in_specs=[whole] * count + [pl.BlockSpec(memory_space=pl.ANY)] * 6,
         out_specs=[out] * (count * pieces),
         out_shape=[jax.ShapeDtypeStruct((per, width // pieces), bf16)] * (count * pieces),
-        scratch_shapes=[pltpu.VMEM((count * per, width), bf16), pltpu.VMEM((count * per, width), f32)],
+        scratch_shapes=[
+            pltpu.VMEM((count * per, width), bf16),
+            pltpu.VMEM((count * per, width), f32),
+            pltpu.SemaphoreType.DMA((len(chunks), 6)),
+        ]
+        + buffers,
         cost_estimate=pl.CostEstimate(flops=8 * 10**9, bytes_accessed=25 * 10**6, transcendentals=10**6),
+        compiler_params=pltpu.CompilerParams(vmem_limit_bytes=FFN_VMEM),
         name="ffn",
     )(*xs, *weights)
     return [outs[i * pieces : (i + 1) * pieces] for i in range(count)]
@@ -379,6 +449,7 @@
         ),
         out_shape=[shape] * zn,
         cost_estimate=pl.CostEstimate(flops=10**9, bytes_accessed=2 * 10**6, transcendentals=10**3),
+        compiler_params=pltpu.CompilerParams(vmem_limit_bytes=VMEM),
         name="combine",
     )(scal, idx, w, *ys)
 
@@ -461,7 +532,7 @@
     back = [[over_ep(late[i][p], m) for i, m in enumerate(order[1:])] for p in range(pieces)]
     own, other = project(scal, gathered, mixer_output_weight, wp)
     other = over_core(other)
-    mixer_output_first = (own + other.astype(f32)).astype(bf16)
+    mixer_output_first = join(own, other)
     outs = []
     for p in range(pieces):
         ys = [y0] + back[p] + [first_back]

time: 163 us -> 141 us (0.87)
  Pallas kernels: 72.1 us -> 41 us
  starting transfers between devices: 28.5 us -> 38.6 us
  other arithmetic: 4.5 us -> 0.94 us
    pallas_call x4 -> x5, Pallas kernels: 53.9 us -> 32.9 us  [the longest x2 20 us: ffn(): pl.pallas_call(functools.partial(ffn_body, count, pieces, chunks), in_spe...]
    ppermute x9, starting transfers between devices: 13.7 us -> 23.9 us  [on_device(): lax.ppermute(x, 'tp', [(i, i ^ m * CORES) for i in range(tp)])]
    ppermute x11, waiting for transfers between devices: 8.92 us -> 15.8 us  [on_device(): lax.ppermute(x, 'ep', [(i, i ^ m) for i in range(ep)])]
    ppermute x9, waiting for transfers between devices: 44.8 us -> 39.5 us  [on_device(): lax.ppermute(x, 'tp', [(i, i ^ m * CORES) for i in range(tp)])]
    pallas_call x2, Pallas kernels: 7.5 us -> 3.13 us  [combine(): pl.pallas_call(functools.partial(combine_body, experts, capacity, zn), gr...]
    pallas_call x1, Pallas kernels: 6.57 us -> 3.22 us  [project(): pl.pallas_call(functools.partial(project_body, zn), grid_spec=pltpu.Prefe...]
    pallas_call x1, Pallas kernels: 4.17 us -> 1.73 us  [pack(): pl.pallas_call(functools.partial(pack_body, experts, capacity), grid_spec...]
    convert_element_type x2, other arithmetic: 1.95 us -> 0.14 us  [on_device(): outs.append(total.astype(bf16))]
  transfers between devices with their start and end apart: 25 -> 25, of which waited for: 6 -> 11; matrix products, arithmetic and copies ran while one was open for 2% -> 0% of each run, Pallas kernels for 44% -> 29%
where the time goes in v1:
time: 141 us
  waiting for transfers between devices  55.3 us (39%)
  Pallas kernels  41 us (29%)
  starting transfers between devices  38.6 us (27%)
  local copies, waits for them, and re-layouts  3.73 us (3%)
    ppermute x9, waiting for transfers between devices, on_device(): lax.ppermute(x, 'tp', [(i, i ^ m * CORES) for i in range(tp)])  39.5 us
    ppermute x9, starting transfers between devices, on_device(): lax.ppermute(x, 'tp', [(i, i ^ m * CORES) for i in range(tp)])  23.9 us
    pallas_call x2, Pallas kernels, ffn(): pl.pallas_call(functools.partial(ffn_body, count, pieces, chunks), in_spe...  20 us
    ppermute x11, waiting for transfers between devices, on_device(): lax.ppermute(x, 'ep', [(i, i ^ m) for i in range(ep)])  15.8 us
    ppermute x11, starting transfers between devices, on_device(): lax.ppermute(x, 'ep', [(i, i ^ m) for i in range(ep)])  13.6 us
    pallas_call x1, Pallas kernels, mixer(): pl.pallas_call(functools.partial(mixer_body, heads, ep, 4 * BLOCK), grid_...  8.44 us
    unnamed x36, local copies, waits for them, and re-layouts  3.73 us
    pallas_call x1, Pallas kernels, final_state(): pl.pallas_call(functools.partial(state_body, heads, 4 * BLOCK), grid=(len...  3.49 us
  transfers between devices with their start and end apart: 25, of which 11 were waited for; matrix products, arithmetic and copies ran while one was open for 0% of the time, Pallas kernels for 29%

profile of v1, /device:TPU:0, one launch (start us, length us, event | category | flops | bytes accessed | tf_op | source)
XLA Modules:
  0.0 140.5 jit_solution(504098248058925987)
XLA Ops:
  0.6 0.6 collective-permute-start.10
  1.2 0.1 collective-permute-start.11
  1.3 0.4 collective-permute-start.9
  1.7 1.2 copy-done.3
  2.9 1.0 copy-done.6
  4.0 0.7 copy-done.10
  4.7 0.7 copy-done.15
  5.4 3.5 %final_state.1 = f32[136,128]{1,0:T(8,128)S(1)} custom-call(bf16[2048,256]{1,0:T(8,128)(2,1)S(1)} %copy-done.3, bf16[2048,128]{1,0:T(8,128)(2,1)S(1)} %copy-done.6, f32[1,256]{1,0:T(1,128)S(1)} %bitcast.19, f32[2,2048]{1,0:T(2,128)S(1)} %bitcast.11), custom_call_target="tpu_custom_call" | custom-call | flops 4000000000 | bytes 2000000 | tf_op jit(solution)/shard_map/final_state/pallas_call | solution.py:95
  8.9 2.6 %collective-permute-start = (f32[136,128]{1,0:T(8,128)S(1)}, f32[136,128]{1,0:T(8,128)S(1)}, u32[]{:S(2)}, u32[]{:S(2)}) collective-permute-start(f32[136,128]{1,0:T(8,128)S(1)} %final_state.1), channel_id=1, source_target_pairs={{0,8},{8,0},{16,24},{24,16},{1,9},{9,1},{17,25},{25,17},{2,10},{10... | collective-permute-start | bytes 208904 | tf_op jit(solution)/shard_map/ppermute | solution.py:481
  11.5 1.5 %collective-permute-start.1 = (f32[136,128]{1,0:T(8,128)S(1)}, f32[136,128]{1,0:T(8,128)S(1)}, u32[]{:S(2)}, u32[]{:S(2)}) collective-permute-start(f32[136,128]{1,0:T(8,128)S(1)} %final_state.1), channel_id=1, source_target_pairs={{0,16},{8,24},{16,0},{24,8},{1,17},{9,25},{17,1},{25,9},{2,18},{10... | collective-permute-start | bytes 208904 | tf_op jit(solution)/shard_map/ppermute | solution.py:481
  13.0 0.1 pad_add_fusion.sc_ref
  13.1 1.2 collective-permute-done.refs_0_
  14.3 2.7 %collective-permute-start.2 = (f32[136,128]{1,0:T(8,128)S(1)}, f32[136,128]{1,0:T(8,128)S(1)}, u32[]{:S(2)}, u32[]{:S(2)}) collective-permute-start(f32[136,128]{1,0:T(8,128)S(1)} %final_state.1), channel_id=1, source_target_pairs={{0,24},{8,16},{16,8},{24,0},{1,25},{9,17},{17,9},{25,1},{2,26},{10... | collective-permute-start | bytes 208904 | tf_op jit(solution)/shard_map/ppermute | solution.py:481
  17.0 0.0 copy-start.4
  17.0 0.0 copy-start.5
  17.0 0.0 copy-start.7
  17.0 0.0 copy-start.8
  17.0 0.0 copy-start.11
  17.0 0.0 copy-start.16
  17.0 0.0 copy-start.17
  17.1 1.7 %pack.1 = (bf16[160,2048]{1,0:T(8,128)(2,1)S(1)}, bf16[160,2048]{1,0:T(8,128)(2,1)S(1)}, bf16[160,2048]{1,0:T(8,128)(2,1)S(1)}, bf16[160,2048]{1,0:T(8,128)(2,1)S(1)}) custom-call(s32[3]{0:T(128)S(1)} %pad_add_fusion.sc_ref, bf16[4,2,64,2048]{3,2,1,0:T(8,128)(2,1)S(1)} %bitcast.10, s32[2,512]{1,0:T(2,128)S(1)} %bitcast.14, f32[1,2048]{1,0:T(1,128)S(1)} %bitcast.13), custom_call_target="tpu_custom_call" | custom-call | flops 4000000000 | bytes 4000000 | tf_op jit(solution)/shard_map/pack/pallas_call | solution.py:307
  18.8 0.0 collective-permute-done.1.refs_1_
  18.8 0.1 collective-permute-start.6
  18.9 0.6 collective-permute-done.2.refs_2_
  19.5 8.4 %mixer.1.refs_0_ = bf16[2048,128]{1,0:T(8,128)(2,1)S(1)} custom-call(s32[3]{0:T(128)S(1)} %pad_add_fusion.sc_ref, f32[136,128]{1,0:T(8,128)S(1)} %collective-permute-done.refs_0_, f32[136,128]{1,0:T(8,128)S(1)} %collective-permute-done.1.refs_1_, f32[136,128]{1,0:T(8,128)S(1)} %collective-permute-done.2.refs_2_, bf16[2048,256]{1,0:T(8,128)(2,1)S(1)} %copy-done.5, ...), custom_call_target="tpu_custom_call" | custom-call | flops 12000000000 | bytes 4000000 | tf_op jit(solution)/shard_map/mixer/pallas_call | solution.py:184
  28.0 2.9 %collective-permute-start.4 = (bf16[2048,128]{1,0:T(8,128)(2,1)S(1)}, bf16[2048,128]{1,0:T(8,128)(2,1)S(1)}, u32[]{:S(2)}, u32[]{:S(2)}) collective-permute-start(bf16[2048,128]{1,0:T(8,128)(2,1)S(1)} %mixer.1.refs_0_), channel_id=1, source_target_pairs={{0,4},{1,5},{2,6},{3,7},{4,0},{5,1},{6,2},{7,3},{8,12},{9,13},{10,... | collective-permute-start | bytes 1572872 | tf_op jit(solution)/shard_map/ppermute | solution.py:483
  30.9 1.6 %collective-permute-start.3 = (bf16[2048,128]{1,0:T(8,128)(2,1)S(1)}, bf16[2048,128]{1,0:T(8,128)(2,1)S(1)}, u32[]{:S(2)}, u32[]{:S(2)}) collective-permute-start(bf16[2048,128]{1,0:T(8,128)(2,1)S(1)} %mixer.1.refs_0_), channel_id=1, source_target_pairs={{0,2},{1,3},{2,0},{3,1},{4,6},{5,7},{6,4},{7,5},{8,10},{9,11},{10,... | collective-permute-start | bytes 1572872 | tf_op jit(solution)/shard_map/ppermute | solution.py:483
  32.4 21.6 %collective-permute-done.4.refs_2_ = bf16[2048,128]{1,0:T(8,128)(2,1)S(1)} collective-permute-done((bf16[2048,128]{1,0:T(8,128)(2,1)S(1)}, bf16[2048,128]{1,0:T(8,128)(2,1)S(1)}, u32[]{:S(2)}, u32[]{:S(2)}) %collective-permute-start.4) | collective-permute-done | bytes 524320 | tf_op jit(solution)/shard_map/ppermute | solution.py:483
  54.0 0.6 collective-permute-start.5
  54.6 0.0 collective-permute-done.3.refs_1_
  54.6 1.2 collective-permute-start.8
  55.8 11.1 %collective-permute-done.5.refs_3_ = bf16[2048,128]{1,0:T(8,128)(2,1)S(1)} collective-permute-done((bf16[2048,128]{1,0:T(8,128)(2,1)S(1)}, bf16[2048,128]{1,0:T(8,128)(2,1)S(1)}, u32[]{:S(2)}, u32[]{:S(2)}) %collective-permute-start.5) | collective-permute-done | bytes 524320 | tf_op jit(solution)/shard_map/ppermute | solution.py:483
  66.9 0.5 collective-permute-start.12
  67.3 3.2 %project.1 = (f32[2048,256]{1,0:T(8,128)S(1)}, bf16[2048,256]{1,0:T(8,128)(2,1)S(1)}) custom-call(s32[3]{0:T(128)S(1)} %pad_add_fusion.sc_ref, bf16[2048,128]{1,0:T(8,128)(2,1)S(1)} %mixer.1.refs_0_, bf16[2048,128]{1,0:T(8,128)(2,1)S(1)} %collective-permute-done.3.refs_1_, bf16[2048,128]{1,0:T(8,128)(2,1)S(1)} %collective-permute-done.4.refs_2_, ...), custom_call_target="tpu_custom_call" | custom-call | flops 2000000000 | bytes 6000000 | tf_op jit(solution)/shard_map/project/pallas_call | solution.py:225
  70.6 2.5 %collective-permute-done.8.refs_0_ = bf16[160,2048]{1,0:T(8,128)(2,1)S(1)} collective-permute-done((bf16[160,2048]{1,0:T(8,128)(2,1)S(1)}, bf16[160,2048]{1,0:T(8,128)(2,1)S(1)}, u32[]{:S(2)}, u32[]{:S(2)}) %collective-permute-start.8) | collective-permute-done | bytes 655392 | tf_op jit(solution)/shard_map/ppermute | solution.py:481
  73.1 0.5 collective-permute-start.13
  73.6 0.0 collective-permute-done.10.refs_5_
  73.6 0.0 collective-permute-start.7
  73.6 0.0 collective-permute-done.11.refs_7_
  73.7 10.0 %ffn.2 = (bf16[160,2048]{1,0:T(8,128)(2,1)S(1)}, bf16[160,2048]{1,0:T(8,128)(2,1)S(1)}) custom-call(bf16[160,2048]{1,0:T(8,128)(2,1)S(1)} %collective-permute-done.8.refs_0_, bf16[160,2048]{1,0:T(8,128)(2,1)S(1)} %get-tuple-element.32.refs_1_, bf16[1,2048,896]{2,1,0:T(8,128)(2,1)S(1)} %copy-done, bf16[1,2048,896]{2,1,0:T(8,128)(2,1)} %collective-permute-done.9.refs_3_, ...), custom_call_target="tpu_custom_call" | custom-call | flops 8000000000 | bytes 25000000 | tf_op jit(solution)/shard_map/ffn/pallas_call | solution.py:393
  83.6 0.0 copy-start.14
  83.6 1.5 %collective-permute-start.16 = (bf16[160,2048]{1,0:T(8,128)(2,1)S(1)}, bf16[160,2048]{1,0:T(8,128)(2,1)S(1)}, u32[]{:S(2)}, u32[]{:S(2)}) collective-permute-start(bf16[160,2048]{1,0:T(8,128)(2,1)S(1)} %get-tuple-element.37), channel_id=1, source_target_pairs={{0,24},{8,16},{16,8},{24,0},{1,25},{9,17},{17,9},{25,1},{2,26},{10... | collective-permute-start | bytes 1966088 | tf_op jit(solution)/shard_map/ppermute | solution.py:481
  85.2 0.0 collective-permute-done.12.refs_0_
  85.2 2.2 %collective-permute-done.13.refs_1_ = bf16[160,2048]{1,0:T(8,128)(2,1)S(1)} collective-permute-done((bf16[160,2048]{1,0:T(8,128)(2,1)S(1)}, bf16[160,2048]{1,0:T(8,128)(2,1)S(1)}, u32[]{:S(2)}, u32[]{:S(2)}) %collective-permute-start.13) | collective-permute-done | bytes 655392 | tf_op jit(solution)/shard_map/ppermute | solution.py:481
  87.4 10.0 %ffn.3 = (bf16[160,1024]{1,0:T(8,128)(2,1)S(1)}, bf16[160,1024]{1,0:T(8,128)(2,1)S(1)}, bf16[160,1024]{1,0:T(8,128)(2,1)S(1)}, bf16[160,1024]{1,0:T(8,128)(2,1)S(1)}) custom-call(bf16[160,2048]{1,0:T(8,128)(2,1)S(1)} %collective-permute-done.12.refs_0_, bf16[160,2048]{1,0:T(8,128)(2,1)S(1)} %collective-permute-done.13.refs_1_, ...), custom_call_target="tpu_custom_call" | custom-call | flops 8000000000 | bytes 25000000 | tf_op jit(solution)/shard_map/ffn/pallas_call | solution.py:393
  97.4 0.6 collective-permute-start.14
  98.0 1.2 collective-permute-start.15
  99.2 0.8 collective-permute-start.20
  100.0 9.3 %collective-permute-done.14.refs_1_ = bf16[160,1024]{1,0:T(8,128)(2,1)S(1)} collective-permute-done((bf16[160,1024]{1,0:T(8,128)(2,1)S(1)}, bf16[160,1024]{1,0:T(8,128)(2,1)S(1)}, u32[]{:S(2)}, u32[]{:S(2)}) %collective-permute-start.14) | collective-permute-done | bytes 327712 | tf_op jit(solution)/shard_map/ppermute | solution.py:481
  109.3 0.5 collective-permute-start.21
  109.8 1.6 %combine.2 = (bf16[64,1024]{1,0:T(8,128)(2,1)S(1)}, bf16[64,1024]{1,0:T(8,128)(2,1)S(1)}, bf16[64,1024]{1,0:T(8,128)(2,1)S(1)}, bf16[64,1024]{1,0:T(8,128)(2,1)S(1)}) custom-call(s32[3]{0:T(128)S(1)} %pad_add_fusion.sc_ref, s32[2,512]{1,0:T(2,128)S(1)} %bitcast.15, f32[2,512]{1,0:T(2,128)S(1)} %bitcast.17, bf16[160,2048]{1,0:T(8,128)(2,1)S(1)} %get-tuple-element.33.refs_0_, ...), custom_call_target="tpu_custom_call" | custom-call | flops 1000000000 | bytes 2000000 | tf_op jit(solution)/shard_map/combine/pallas_call | solution.py:437
  111.4 1.0 collective-permute-start.17
  112.4 13.4 %collective-permute-start.18 = (bf16[64,1024]{1,0:T(8,128)(2,1)S(1)}, bf16[64,1024]{1,0:T(8,128)(2,1)S(1)}, u32[]{:S(2)}, u32[]{:S(2)}) collective-permute-start(bf16[64,1024]{1,0:T(8,128)(2,1)S(1)} %get-tuple-element.40), channel_id=1, source_target_pairs={{0,4},{1,5},{2,6},{3,7},{4,0},{5,1},{6,2},{7,3},{8,12},{9,13},{10,... | collective-permute-start | bytes 393224 | tf_op jit(solution)/shard_map/ppermute | solution.py:483
  125.8 1.1 join.1
  126.8 1.6 %combine.3 = (bf16[64,1024]{1,0:T(8,128)(2,1)S(1)}, bf16[64,1024]{1,0:T(8,128)(2,1)S(1)}, bf16[64,1024]{1,0:T(8,128)(2,1)S(1)}, bf16[64,1024]{1,0:T(8,128)(2,1)S(1)}) custom-call(s32[3]{0:T(128)S(1)} %pad_add_fusion.sc_ref, s32[2,512]{1,0:T(2,128)S(1)} %bitcast.16, f32[2,512]{1,0:T(2,128)S(1)} %bitcast.18, bf16[160,2048]{1,0:T(8,128)(2,1)S(1)} %get-tuple-element.33.refs_0_, ...), custom_call_target="tpu_custom_call" | custom-call | flops 1000000000 | bytes 2000000 | tf_op jit(solution)/shard_map/combine/pallas_call | solution.py:437
  128.4 0.6 collective-permute-start.22
  129.0 3.8 %collective-permute-start.23 = (bf16[64,1024]{1,0:T(8,128)(2,1)S(1)}, bf16[64,1024]{1,0:T(8,128)(2,1)S(1)}, u32[]{:S(2)}, u32[]{:S(2)}) collective-permute-start(bf16[64,1024]{1,0:T(8,128)(2,1)S(1)} %get-tuple-element.46), channel_id=1, source_target_pairs={{0,4},{1,5},{2,6},{3,7},{4,0},{5,1},{6,2},{7,3},{8,12},{9,13},{10,... | collective-permute-start | bytes 393224 | tf_op jit(solution)/shard_map/ppermute | solution.py:483
  132.9 0.4 collective-permute-done.18
  133.3 0.1 add_convert_fusion.1
  133.4 1.2 collective-permute-done.22
  134.5 3.0 %collective-permute-done.23 = bf16[64,1024]{1,0:T(8,128)(2,1)S(1)} collective-permute-done((bf16[64,1024]{1,0:T(8,128)(2,1)S(1)}, bf16[64,1024]{1,0:T(8,128)(2,1)S(1)}, u32[]{:S(2)}, u32[]{:S(2)}) %collective-permute-start.23) | collective-permute-done | bytes 131104 | tf_op jit(solution)/shard_map/ppermute | solution.py:483
  137.5 2.2 %collective-permute-done.24 = bf16[64,1024]{1,0:T(8,128)(2,1)S(1)} collective-permute-done((bf16[64,1024]{1,0:T(8,128)(2,1)S(1)}, bf16[64,1024]{1,0:T(8,128)(2,1)S(1)}, u32[]{:S(2)}, u32[]{:S(2)}) %collective-permute-start.24) | collective-permute-done | bytes 131104 | tf_op jit(solution)/shard_map/ppermute | solution.py:483
  139.7 0.1 add_convert_fusion
  139.8 0.7 pad_maximum_fusion
  (35 shorter events, 0.1 us)
Async XLA Ops:
  0.6 73.0 %collective-permute-start.10 = (bf16[1,2048,896]{2,1,0:T(8,128)(2,1)}, bf16[1,2048,896]{2,1,0:T(8,128)(2,1)}, u32[]{:S(2)}, u32[]{:S(2)}) collective-permute-start(bf16[1,2048,896]{2,1,0:T(8,128)(2,1)} %refs_4_.7), channel_id=1, source_target_pairs={{0,1},{1,0},{2,3},{3,2},{4,5},{5,4},{6,7},{7,6},{8,9},{9,8},{10,11... | collective-permute-start | bytes 11010056 | tf_op jit(solution)/shard_map/ppermute | solution.py:482
  1.2 72.4 %collective-permute-start.11 = (bf16[1,896,2048]{2,1,0:T(8,128)(2,1)}, bf16[1,896,2048]{2,1,0:T(8,128)(2,1)}, u32[]{:S(2)}, u32[]{:S(2)}) collective-permute-start(bf16[1,896,2048]{2,1,0:T(8,128)(2,1)} %refs_6_.5), channel_id=1, source_target_pairs={{0,1},{1,0},{2,3},{3,2},{4,5},{5,4},{6,7},{7,6},{8,9},{9,8},{10,11... | collective-permute-start | bytes 11010056 | tf_op jit(solution)/shard_map/ppermute | solution.py:482
  1.3 72.4 %collective-permute-start.9 = (bf16[1,2048,896]{2,1,0:T(8,128)(2,1)}, bf16[1,2048,896]{2,1,0:T(8,128)(2,1)}, u32[]{:S(2)}, u32[]{:S(2)}) collective-permute-start(bf16[1,2048,896]{2,1,0:T(8,128)(2,1)} %refs_2_.3), channel_id=1, source_target_pairs={{0,1},{1,0},{2,3},{3,2},{4,5},{5,4},{6,7},{7,6},{8,9},{9,8},{10,11... | collective-permute-start | bytes 11010056 | tf_op jit(solution)/shard_map/ppermute | solution.py:482
  1.7 1.2 copy-start.3
  2.9 1.0 copy-start.6
  4.0 0.7 copy-start.10
  4.7 0.7 copy-start.15
  5.4 11.6 %copy-start.2 = (bf16[512,2048]{1,0:T(8,128)(2,1)S(1)}, bf16[512,2048]{1,0:T(8,128)(2,1)}, u32[]{:S(2)}) copy-start(bf16[512,2048]{1,0:T(8,128)(2,1)} %param.23) | copy-start | bytes 6291460
  5.4 11.6 %copy-start.12 = (f32[2048]{0:T(1024)S(1)}, f32[2048]{0:T(1024)}, u32[]{:S(2)}) copy-start(f32[2048]{0:T(1024)} %param.24) | copy-start | bytes 24580
  5.4 11.6 %copy-start.13 = (s32[512,2]{0,1:T(2,128)S(1)}, s32[512,2]{0,1:T(2,128)}, u32[]{:S(2)}) copy-start(s32[512,2]{0,1:T(2,128)} %param.25) | copy-start | bytes 12292
  8.9 5.4 %collective-permute-start = (f32[136,128]{1,0:T(8,128)S(1)}, f32[136,128]{1,0:T(8,128)S(1)}, u32[]{:S(2)}, u32[]{:S(2)}) collective-permute-start(f32[136,128]{1,0:T(8,128)S(1)} %final_state.1), channel_id=1, source_target_pairs={{0,8},{8,0},{16,24},{24,16},{1,9},{9,1},{17,25},{25,17},{2,10},{10... | collective-permute-start | bytes 208904 | tf_op jit(solution)/shard_map/ppermute | solution.py:481
  11.5 7.3 %collective-permute-start.1 = (f32[136,128]{1,0:T(8,128)S(1)}, f32[136,128]{1,0:T(8,128)S(1)}, u32[]{:S(2)}, u32[]{:S(2)}) collective-permute-start(f32[136,128]{1,0:T(8,128)S(1)} %final_state.1), channel_id=1, source_target_pairs={{0,16},{8,24},{16,0},{24,8},{1,17},{9,25},{17,1},{25,9},{2,18},{10... | collective-permute-start | bytes 208904 | tf_op jit(solution)/shard_map/ppermute | solution.py:481
  14.3 5.2 %collective-permute-start.2 = (f32[136,128]{1,0:T(8,128)S(1)}, f32[136,128]{1,0:T(8,128)S(1)}, u32[]{:S(2)}, u32[]{:S(2)}) collective-permute-start(f32[136,128]{1,0:T(8,128)S(1)} %final_state.1), channel_id=1, source_target_pairs={{0,24},{8,16},{16,8},{24,0},{1,25},{9,17},{17,9},{25,1},{2,26},{10... | collective-permute-start | bytes 208904 | tf_op jit(solution)/shard_map/ppermute | solution.py:481
  17.0 1.8 %copy-start.9 = (bf16[1024,256]{1,0:T(8,128)(2,1)S(1)}, bf16[1024,256]{1,0:T(8,128)(2,1)}, u32[]{:S(2)}) copy-start(bf16[1024,256]{1,0:T(8,128)(2,1)} %refs_4_.5) | copy-start | bytes 1572868
  17.0 2.5 %copy-start.4 = (bf16[2048,256]{1,0:T(8,128)(2,1)S(1)}, bf16[2048,256]{1,0:T(8,128)(2,1)}, u32[]{:S(2)}) copy-start(bf16[2048,256]{1,0:T(8,128)(2,1)} %refs_4_.4) | copy-start | bytes 3145732
  17.0 2.5 %copy-start.5 = (bf16[2048,256]{1,0:T(8,128)(2,1)S(1)}, bf16[2048,256]{1,0:T(8,128)(2,1)}, u32[]{:S(2)}) copy-start(bf16[2048,256]{1,0:T(8,128)(2,1)} %refs_3_) | copy-start | bytes 3145732
  17.0 2.5 %copy-start.7 = (bf16[2048,128]{1,0:T(8,128)(2,1)S(1)}, bf16[2048,128]{1,0:T(8,128)(2,1)}, u32[]{:S(2)}) copy-start(bf16[2048,128]{1,0:T(8,128)(2,1)} %refs_5_.1) | copy-start | bytes 1572868
  17.0 2.5 %copy-start.8 = (bf16[2048,128]{1,0:T(8,128)(2,1)S(1)}, bf16[2048,128]{1,0:T(8,128)(2,1)}, u32[]{:S(2)}) copy-start(bf16[2048,128]{1,0:T(8,128)(2,1)} %refs_6_.3) | copy-start | bytes 1572868
  17.0 2.5 %copy-start.11 = (f32[2048,2]{0,1:T(2,128)S(1)}, f32[2048,2]{0,1:T(2,128)}, u32[]{:S(2)}) copy-start(f32[2048,2]{0,1:T(2,128)} %param.20) | copy-start | bytes 49156
  17.0 2.5 %copy-start.16 = (f32[256]{0:T(256)S(1)}, f32[256]{0:T(256)}, u32[]{:S(2)}) copy-start(f32[256]{0:T(256)} %param.19) | copy-start | bytes 3076
  17.0 2.5 %copy-start.17 = (f32[128]{0:T(128)S(1)}, f32[128]{0:T(128)}, u32[]{:S(2)}) copy-start(f32[128]{0:T(128)} %param.21) | copy-start | bytes 1540
  18.8 12.1 %collective-permute-start.6 = (bf16[1024,256]{1,0:T(8,128)(2,1)S(1)}, bf16[1024,256]{1,0:T(8,128)(2,1)S(1)}, u32[]{:S(2)}, u32[]{:S(2)}) collective-permute-start(bf16[1024,256]{1,0:T(8,128)(2,1)S(1)} %copy-done.9), channel_id=1, source_target_pairs={{0,1},{1,0},{2,3},{3,2},{4,5},{5,4},{6,7},{7,6},{8,9},{9,8},{10,11... | collective-permute-start | bytes 1572872 | tf_op jit(solution)/shard_map/ppermute | solution.py:482
  28.0 26.1 %collective-permute-start.4 = (bf16[2048,128]{1,0:T(8,128)(2,1)S(1)}, bf16[2048,128]{1,0:T(8,128)(2,1)S(1)}, u32[]{:S(2)}, u32[]{:S(2)}) collective-permute-start(bf16[2048,128]{1,0:T(8,128)(2,1)S(1)} %mixer.1.refs_0_), channel_id=1, source_target_pairs={{0,4},{1,5},{2,6},{3,7},{4,0},{5,1},{6,2},{7,3},{8,12},{9,13},{10,... | collective-permute-start | bytes 1572872 | tf_op jit(solution)/shard_map/ppermute | solution.py:483
  30.9 23.7 %collective-permute-start.3 = (bf16[2048,128]{1,0:T(8,128)(2,1)S(1)}, bf16[2048,128]{1,0:T(8,128)(2,1)S(1)}, u32[]{:S(2)}, u32[]{:S(2)}) collective-permute-start(bf16[2048,128]{1,0:T(8,128)(2,1)S(1)} %mixer.1.refs_0_), channel_id=1, source_target_pairs={{0,2},{1,3},{2,0},{3,1},{4,6},{5,7},{6,4},{7,5},{8,10},{9,11},{10,... | collective-permute-start | bytes 1572872 | tf_op jit(solution)/shard_map/ppermute | solution.py:483
  54.0 12.9 %collective-permute-start.5 = (bf16[2048,128]{1,0:T(8,128)(2,1)S(1)}, bf16[2048,128]{1,0:T(8,128)(2,1)S(1)}, u32[]{:S(2)}, u32[]{:S(2)}) collective-permute-start(bf16[2048,128]{1,0:T(8,128)(2,1)S(1)} %collective-permute-done.4.refs_2_), channel_id=1, source_target_pairs={{0,2},{1,3},{2,0},{3,1},{4,6},{5,7},{6,4},{7,5},{8,10},{9,11},{10,... | collective-permute-start | bytes 1572872 | tf_op jit(solution)/shard_map/ppermute | solution.py:483
  54.6 18.5 %collective-permute-start.8 = (bf16[160,2048]{1,0:T(8,128)(2,1)S(1)}, bf16[160,2048]{1,0:T(8,128)(2,1)S(1)}, u32[]{:S(2)}, u32[]{:S(2)}) collective-permute-start(bf16[160,2048]{1,0:T(8,128)(2,1)S(1)} %get-tuple-element.30), channel_id=1, source_target_pairs={{0,24},{8,16},{16,8},{24,0},{1,25},{9,17},{17,9},{25,1},{2,26},{10... | collective-permute-start | bytes 1966088 | tf_op jit(solution)/shard_map/ppermute | solution.py:481
  55.8 17.8 %copy-start = (bf16[1,2048,896]{2,1,0:T(8,128)(2,1)S(1)}, bf16[1,2048,896]{2,1,0:T(8,128)(2,1)}, u32[]{:S(2)}) copy-start(bf16[1,2048,896]{2,1,0:T(8,128)(2,1)} %refs_2_.3) | copy-start | bytes 11010052
  55.8 17.9 %copy-start.1 = (bf16[1,2048,896]{2,1,0:T(8,128)(2,1)S(1)}, bf16[1,2048,896]{2,1,0:T(8,128)(2,1)}, u32[]{:S(2)}) copy-start(bf16[1,2048,896]{2,1,0:T(8,128)(2,1)} %refs_4_.7) | copy-start | bytes 11010052
  66.9 18.3 %collective-permute-start.12 = (bf16[160,2048]{1,0:T(8,128)(2,1)S(1)}, bf16[160,2048]{1,0:T(8,128)(2,1)S(1)}, u32[]{:S(2)}, u32[]{:S(2)}) collective-permute-start(bf16[160,2048]{1,0:T(8,128)(2,1)S(1)} %get-tuple-element.26), channel_id=1, source_target_pairs={{0,8},{8,0},{16,24},{24,16},{1,9},{9,1},{17,25},{25,17},{2,10},{10... | collective-permute-start | bytes 1966088 | tf_op jit(solution)/shard_map/ppermute | solution.py:481
  73.1 14.3 %collective-permute-start.13 = (bf16[160,2048]{1,0:T(8,128)(2,1)S(1)}, bf16[160,2048]{1,0:T(8,128)(2,1)S(1)}, u32[]{:S(2)}, u32[]{:S(2)}) collective-permute-start(bf16[160,2048]{1,0:T(8,128)(2,1)S(1)} %get-tuple-element.34), channel_id=1, source_target_pairs={{0,16},{8,24},{16,0},{24,8},{1,17},{9,25},{17,1},{25,9},{2,18},{10... | collective-permute-start | bytes 1966088 | tf_op jit(solution)/shard_map/ppermute | solution.py:481
  73.6 52.2 %collective-permute-start.7 = (bf16[2048,256]{1,0:T(8,128)(2,1)S(1)}, bf16[2048,256]{1,0:T(8,128)(2,1)S(1)}, u32[]{:S(2)}, u32[]{:S(2)}) collective-permute-start(bf16[2048,256]{1,0:T(8,128)(2,1)S(1)} %get-tuple-element.29), channel_id=1, source_target_pairs={{0,1},{1,0},{2,3},{3,2},{4,5},{5,4},{6,7},{7,6},{8,9},{9,8},{10,11... | collective-permute-start | bytes 3145736 | tf_op jit(solution)/shard_map/ppermute | solution.py:482
  83.6 26.2 %copy-start.14 = (f32[512,2]{0,1:T(2,128)S(1)}, f32[512,2]{0,1:T(2,128)}, u32[]{:S(2)}) copy-start(f32[512,2]{0,1:T(2,128)} %param.26) | copy-start | bytes 12292
  83.6 26.2 %collective-permute-start.16 = (bf16[160,2048]{1,0:T(8,128)(2,1)S(1)}, bf16[160,2048]{1,0:T(8,128)(2,1)S(1)}, u32[]{:S(2)}, u32[]{:S(2)}) collective-permute-start(bf16[160,2048]{1,0:T(8,128)(2,1)S(1)} %get-tuple-element.37), channel_id=1, source_target_pairs={{0,24},{8,16},{16,8},{24,0},{1,25},{9,17},{17,9},{25,1},{2,26},{10... | collective-permute-start | bytes 1966088 | tf_op jit(solution)/shard_map/ppermute | solution.py:481
  97.4 11.9 %collective-permute-start.14 = (bf16[160,1024]{1,0:T(8,128)(2,1)S(1)}, bf16[160,1024]{1,0:T(8,128)(2,1)S(1)}, u32[]{:S(2)}, u32[]{:S(2)}) collective-permute-start(bf16[160,1024]{1,0:T(8,128)(2,1)S(1)} %get-tuple-element.35), channel_id=1, source_target_pairs={{0,8},{8,0},{16,24},{24,16},{1,9},{9,1},{17,25},{25,17},{2,10},{10... | collective-permute-start | bytes 983048 | tf_op jit(solution)/shard_map/ppermute | solution.py:481
  98.0 11.8 %collective-permute-start.15 = (bf16[160,1024]{1,0:T(8,128)(2,1)S(1)}, bf16[160,1024]{1,0:T(8,128)(2,1)S(1)}, u32[]{:S(2)}, u32[]{:S(2)}) collective-permute-start(bf16[160,1024]{1,0:T(8,128)(2,1)S(1)} %get-tuple-element.36), channel_id=1, source_target_pairs={{0,16},{8,24},{16,0},{24,8},{1,17},{9,25},{17,1},{25,9},{2,18},{10... | collective-permute-start | bytes 983048 | tf_op jit(solution)/shard_map/ppermute | solution.py:481
  99.2 27.6 %collective-permute-start.20 = (bf16[160,1024]{1,0:T(8,128)(2,1)S(1)}, bf16[160,1024]{1,0:T(8,128)(2,1)S(1)}, u32[]{:S(2)}, u32[]{:S(2)}) collective-permute-start(bf16[160,1024]{1,0:T(8,128)(2,1)S(1)} %get-tuple-element.42), channel_id=1, source_target_pairs={{0,8},{8,0},{16,24},{24,16},{1,9},{9,1},{17,25},{25,17},{2,10},{10... | collective-permute-start | bytes 983048 | tf_op jit(solution)/shard_map/ppermute | solution.py:481
  109.3 17.5 %collective-permute-start.21 = (bf16[160,1024]{1,0:T(8,128)(2,1)S(1)}, bf16[160,1024]{1,0:T(8,128)(2,1)S(1)}, u32[]{:S(2)}, u32[]{:S(2)}) collective-permute-start(bf16[160,1024]{1,0:T(8,128)(2,1)S(1)} %get-tuple-element.43), channel_id=1, source_target_pairs={{0,16},{8,24},{16,0},{24,8},{1,17},{9,25},{17,1},{25,9},{2,18},{10... | collective-permute-start | bytes 983048 | tf_op jit(solution)/shard_map/ppermute | solution.py:481
  111.4 21.4 %collective-permute-start.17 = (bf16[64,1024]{1,0:T(8,128)(2,1)S(1)}, bf16[64,1024]{1,0:T(8,128)(2,1)S(1)}, u32[]{:S(2)}, u32[]{:S(2)}) collective-permute-start(bf16[64,1024]{1,0:T(8,128)(2,1)S(1)} %get-tuple-element.39), channel_id=1, source_target_pairs={{0,2},{1,3},{2,0},{3,1},{4,6},{5,7},{6,4},{7,5},{8,10},{9,11},{10,... | collective-permute-start | bytes 393224 | tf_op jit(solution)/shard_map/ppermute | solution.py:483
  112.4 20.9 %collective-permute-start.18 = (bf16[64,1024]{1,0:T(8,128)(2,1)S(1)}, bf16[64,1024]{1,0:T(8,128)(2,1)S(1)}, u32[]{:S(2)}, u32[]{:S(2)}) collective-permute-start(bf16[64,1024]{1,0:T(8,128)(2,1)S(1)} %get-tuple-element.40), channel_id=1, source_target_pairs={{0,4},{1,5},{2,6},{3,7},{4,0},{5,1},{6,2},{7,3},{8,12},{9,13},{10,... | collective-permute-start | bytes 393224 | tf_op jit(solution)/shard_map/ppermute | solution.py:483
  125.8 7.5 %collective-permute-start.19 = (bf16[64,1024]{1,0:T(8,128)(2,1)S(1)}, bf16[64,1024]{1,0:T(8,128)(2,1)S(1)}, u32[]{:S(2)}, u32[]{:S(2)}) collective-permute-start(bf16[64,1024]{1,0:T(8,128)(2,1)S(1)} %get-tuple-element.41), channel_id=1, source_target_pairs={{0,6},{1,7},{2,4},{3,5},{4,2},{5,3},{6,0},{7,1},{8,14},{9,15},{10,... | collective-permute-start | bytes 393224 | tf_op jit(solution)/shard_map/ppermute | solution.py:483
  128.4 6.1 %collective-permute-start.22 = (bf16[64,1024]{1,0:T(8,128)(2,1)S(1)}, bf16[64,1024]{1,0:T(8,128)(2,1)S(1)}, u32[]{:S(2)}, u32[]{:S(2)}) collective-permute-start(bf16[64,1024]{1,0:T(8,128)(2,1)S(1)} %get-tuple-element.45), channel_id=1, source_target_pairs={{0,2},{1,3},{2,0},{3,1},{4,6},{5,7},{6,4},{7,5},{8,10},{9,11},{10,... | collective-permute-start | bytes 393224 | tf_op jit(solution)/shard_map/ppermute | solution.py:483
  129.0 8.5 %collective-permute-start.23 = (bf16[64,1024]{1,0:T(8,128)(2,1)S(1)}, bf16[64,1024]{1,0:T(8,128)(2,1)S(1)}, u32[]{:S(2)}, u32[]{:S(2)}) collective-permute-start(bf16[64,1024]{1,0:T(8,128)(2,1)S(1)} %get-tuple-element.46), channel_id=1, source_target_pairs={{0,4},{1,5},{2,6},{3,7},{4,0},{5,1},{6,2},{7,3},{8,12},{9,13},{10,... | collective-permute-start | bytes 393224 | tf_op jit(solution)/shard_map/ppermute | solution.py:483
  132.9 6.9 %collective-permute-start.24 = (bf16[64,1024]{1,0:T(8,128)(2,1)S(1)}, bf16[64,1024]{1,0:T(8,128)(2,1)S(1)}, u32[]{:S(2)}, u32[]{:S(2)}) collective-permute-start(bf16[64,1024]{1,0:T(8,128)(2,1)S(1)} %get-tuple-element.47), channel_id=1, source_target_pairs={{0,6},{1,7},{2,4},{3,5},{4,2},{5,3},{6,0},{7,1},{8,14},{9,15},{10,... | collective-permute-start | bytes 393224 | tf_op jit(solution)/shard_map/ppermute | solution.py:483

commit v2 on v1

--- a/solution.py
+++ b/solution.py
@@ -12,8 +12,7 @@
 BLOCK = 64
 TOPK = 2
 CORES = 2
-PIECES = 2
-STATE_ROWS = 2048
+PIECES = (2, 3, 3)
 MIXER_ROWS = 2048
 FFN_VMEM = 36 * 1024 * 1024
 VMEM = 20 * 1024 * 1024
@@ -51,20 +50,31 @@
     return vh == lax.broadcasted_iota(jnp.int32, shape, 1) // KEY_DIM
 
 
-def state_body(heads, rows, f_ref, v_ref, gap_ref, extra_ref, st_ref, s_ref, l_ref):
-    step = pl.program_id(0)
+def state_body(heads, rows, f_hbm, v_hbm, gap_hbm, extra_hbm, st_ref, f_ref, v_ref, gap_ref, extra_ref, sems):
     vw = heads * VAL_DIM
-
-    @pl.when(step == 0)
-    def _():
-        s_ref[...] = jnp.zeros_like(s_ref)
-        l_ref[...] = jnp.zeros_like(l_ref)
-
+    kw = heads * KEY_DIM
+    length = f_ref.shape[0]
+    half = max(rows, length // 2)
+    copies = [
+        pltpu.make_async_copy(gap_hbm, gap_ref, sems.at[0]),
+        pltpu.make_async_copy(extra_hbm, extra_ref, sems.at[1]),
+    ]
+    for n, at in enumerate(range(0, length, half)):
+        span = pl.ds(at, half)
+        copies.append(pltpu.make_async_copy(f_hbm.at[span], f_ref.at[span], sems.at[2 + 2 * n]))
+        copies.append(pltpu.make_async_copy(v_hbm.at[span], v_ref.at[span], sems.at[3 + 2 * n]))
+    for copy in copies:
+        copy.start()
     row = lax.broadcasted_iota(jnp.int32, (rows, rows), 0)
     later = (row < lax.broadcasted_iota(jnp.int32, (rows, rows), 1)).astype(bf16)
-    s = s_ref[...]
-    l = l_ref[...]
-    for at in range(0, f_ref.shape[0], rows):
+    s = jnp.zeros((vw, kw), f32)
+    l = jnp.zeros((1, kw), f32)
+    copies[0].wait()
+    copies[1].wait()
+    for at in range(0, length, rows):
+        if at % half == 0:
+            copies[2 + 2 * (at // half)].wait()
+            copies[3 + 2 * (at // half)].wait()
         rs = slice(at, at + rows)
         key, logf = forget_log(heads, f_ref[rs, :], gap_ref[...], extra_ref[:, rs])
         hi, lo = split2(logf)
@@ -73,34 +83,30 @@
         ks = (key * jnp.exp(rest)).astype(bf16)
         s = s * jnp.exp(whole) + mm(v_ref[rs, :], ks, ((0,), (0,)))
         l = l + whole
-    s_ref[...] = s
-    l_ref[...] = l
-
-    @pl.when(step == pl.num_programs(0) - 1)
-    def _():
-        for h in range(heads):
-            st_ref[h * VAL_DIM : (h + 1) * VAL_DIM, :] = s[
-                h * VAL_DIM : (h + 1) * VAL_DIM, h * KEY_DIM : (h + 1) * KEY_DIM
-            ]
-            st_ref[vw + h : vw + h + 1, :] = l[:, h * KEY_DIM : (h + 1) * KEY_DIM]
+    for h in range(heads):
+        st_ref[h * VAL_DIM : (h + 1) * VAL_DIM, :] = s[
+            h * VAL_DIM : (h + 1) * VAL_DIM, h * KEY_DIM : (h + 1) * KEY_DIM
+        ]
+        st_ref[vw + h : vw + h + 1, :] = l[:, h * KEY_DIM : (h + 1) * KEY_DIM]
 
 
 def final_state(f, v, gap, extra):
     length, kw = f.shape
     heads = kw // KEY_DIM
     vw = heads * VAL_DIM
-    rows = min(length, STATE_ROWS)
-    rows_of = lambda w: pl.BlockSpec((rows, w), lambda i: (i, 0))
-    whole = lambda r, w: pl.BlockSpec((r, w), lambda i: (0, 0))
     return pl.pallas_call(
         functools.partial(state_body, heads, 4 * BLOCK),
-        grid=(length // rows,),
-        in_specs=[rows_of(kw), rows_of(vw), whole(1, kw), pl.BlockSpec((heads, rows), lambda i: (0, i))],
-        out_specs=whole(vw + 8, KEY_DIM),
+        in_specs=[pl.BlockSpec(memory_space=pltpu.HBM)] * 4,
+        out_specs=pl.BlockSpec((vw + 8, KEY_DIM), lambda: (0, 0)),
         out_shape=jax.ShapeDtypeStruct((vw + 8, KEY_DIM), f32),
-        scratch_shapes=[pltpu.VMEM((vw, kw), f32), pltpu.VMEM((1, kw), f32)],
+        scratch_shapes=[
+            pltpu.VMEM((length, kw), bf16),
+            pltpu.VMEM((length, vw), bf16),
+            pltpu.VMEM((1, kw), f32),
+            pltpu.VMEM(extra.shape, f32),
+            pltpu.SemaphoreType.DMA((6,)),
+        ],
         cost_estimate=pl.CostEstimate(flops=4 * 10**9, bytes_accessed=2 * 10**6, transcendentals=10**6),
-        compiler_params=pltpu.CompilerParams(vmem_limit_bytes=VMEM),
         name="final_state",
     )(f, v, gap.reshape(1, kw), extra)
 
@@ -339,8 +345,8 @@
 def ffn_body(count, pieces, chunks, *refs):
     xs = refs[:count]
     sources = refs[count : count + 6]
-    outs = refs[count + 6 : count + 6 + count * pieces]
-    scratch = refs[count + 6 + count * pieces :]
+    outs = refs[count + 6 : count + 6 + count * len(pieces)]
+    scratch = refs[count + 6 + count * len(pieces) :]
     x_ref, acc_ref, sems = scratch[0], scratch[1], scratch[2]
     buffers = scratch[3:]
     per = xs[0].shape[0]
@@ -373,11 +379,9 @@
             acc_ref[...] += part
         else:
             total = part if c == 0 else acc_ref[...] + part
-            cols = total.shape[1] // pieces
             for i in range(count):
-                for p in range(pieces):
-                    piece = total[i * per : (i + 1) * per, p * cols : (p + 1) * cols]
-                    outs[i * pieces + p][...] = piece.astype(bf16)
+                for p, (left, right) in enumerate(pieces):
+                    outs[i * len(pieces) + p][...] = total[i * per : (i + 1) * per, left:right].astype(bf16)
 
 
 def ffn(xs, weights, pieces):
@@ -389,12 +393,12 @@
     for c in chunks:
         buffers += [pltpu.VMEM((2, width, c), bf16), pltpu.VMEM((2, width, c), bf16), pltpu.VMEM((2, c, width), bf16)]
     whole = pl.BlockSpec((per, width), lambda: (0, 0))
-    out = pl.BlockSpec((per, width // pieces), lambda: (0, 0))
+    widths = [right - left for left, right in pieces]
     outs = pl.pallas_call(
         functools.partial(ffn_body, count, pieces, chunks),
         in_specs=[whole] * count + [pl.BlockSpec(memory_space=pl.ANY)] * 6,
-        out_specs=[out] * (count * pieces),
-        out_shape=[jax.ShapeDtypeStruct((per, width // pieces), bf16)] * (count * pieces),
+        out_specs=[pl.BlockSpec((per, w), lambda: (0, 0)) for w in widths] * count,
+        out_shape=[jax.ShapeDtypeStruct((per, w), bf16) for w in widths] * count,
         scratch_shapes=[
             pltpu.VMEM((count * per, width), bf16),
             pltpu.VMEM((count * per, width), f32),
@@ -405,10 +409,11 @@
         compiler_params=pltpu.CompilerParams(vmem_limit_bytes=FFN_VMEM),
         name="ffn",
     )(*xs, *weights)
-    return [outs[i * pieces : (i + 1) * pieces] for i in range(count)]
-
-
-def combine_body(experts, capacity, zn, sc_ref, idx_ref, w_ref, *refs):
+    n = len(pieces)
+    return [outs[i * n : (i + 1) * n] for i in range(count)]
+
+
+def combine_body(experts, capacity, zn, lefts, cols, sc_ref, idx_ref, w_ref, *refs):
     ys = refs[:experts]
     outs = refs[experts : experts + zn]
     acc_ref = refs[-1]
@@ -422,29 +427,25 @@
     for m in range(experts):
         c = jnp.where(t[0] == line + m * per, w[0:1], 0.0)
         c = c + jnp.where(t[1] == line + m * per, w[1:2], 0.0)
-        part = mm(c.astype(bf16), ys[m][...], ((0,), (0,)))
+        y = ys[m][:, lefts[m] : lefts[m] + cols]
+        part = mm(c.astype(bf16), y, ((0,), (0,)))
         acc = part if acc is None else acc + part
     acc_ref[...] = acc.reshape(zn, sub, acc.shape[1]).astype(bf16)
     for m in range(zn):
         outs[m][...] = acc_ref[sc_ref[2] ^ m]
 
 
-def combine(scal, idx, w, ys, piece, pieces, zn, sub, capacity):
+def combine(scal, idx, w, ys, lefts, cols, zn, sub, capacity):
     experts = len(ys)
-    per = zn * capacity
-    cols = ys[0].shape[1] // pieces if ys[0].shape[1] == max(y.shape[1] for y in ys) else ys[0].shape[1]
     shape = jax.ShapeDtypeStruct((sub, cols), bf16)
+    whole = lambda shape: pl.BlockSpec(shape, lambda i, s: (0, 0))
     return pl.pallas_call(
-        functools.partial(combine_body, experts, capacity, zn),
+        functools.partial(combine_body, experts, capacity, zn, lefts, cols),
         grid_spec=pltpu.PrefetchScalarGridSpec(
             num_scalar_prefetch=1,
             grid=(1,),
-            in_specs=[pl.BlockSpec(idx.shape, lambda i, s: (0, 0))] * 2
-            + [
-                pl.BlockSpec((per, cols), (lambda i, s: (0, piece)) if y.shape[1] != cols else (lambda i, s: (0, 0)))
-                for y in ys
-            ],
-            out_specs=[pl.BlockSpec(shape.shape, lambda i, s: (0, 0))] * zn,
+            in_specs=[whole(idx.shape)] * 2 + [whole(y.shape) for y in ys],
+            out_specs=[whole(shape.shape)] * zn,
             scratch_shapes=[pltpu.VMEM((zn, sub, cols), bf16)],
         ),
         out_shape=[shape] * zn,
@@ -452,6 +453,15 @@
         compiler_params=pltpu.CompilerParams(vmem_limit_bytes=VMEM),
         name="combine",
     )(scal, idx, w, *ys)
+
+
+def columns(width, shares):
+    units, out, left = width // 128, [], 0
+    for p in range(len(shares)):
+        right = units * sum(shares[: p + 1]) // sum(shares) * 128
+        out.append((left, right))
+        left = right
+    return out
 
 
 def on_device(
@@ -487,7 +497,8 @@
     rows, width = second_batch_tokens.shape
     sub = rows // tp
     capacity = max(2, sub * TOPK * 5 // (4 * experts))
-    pieces = PIECES
+    cuts = columns(width, PIECES)
+    pieces = len(cuts)
     extra = extra_log_forget.T
     idx = chosen_expert_index.T
     wts = chosen_expert_weight.T
@@ -526,8 +537,8 @@
         gathered.append(over_z(gathered[m - 1] if chained else mixed, 1 if chained else m))
 
     x0, _ = tie((arrived[0], mixed))
-    (y1,), (y0,) = ffn([arrived[ep - 1], x0], weights, 1)
-    late = ffn([arrived[m] for m in order[1:]], weights, pieces)
+    (y1,), (y0,) = ffn([arrived[ep - 1], x0], weights, [(0, width)])
+    late = ffn([arrived[m] for m in order[1:]], weights, cuts)
     first_back = over_ep(y1, ep - 1)
     back = [[over_ep(late[i][p], m) for i, m in enumerate(order[1:])] for p in range(pieces)]
     own, other = project(scal, gathered, mixer_output_weight, wp)
@@ -536,7 +547,9 @@
     outs = []
     for p in range(pieces):
         ys = [y0] + back[p] + [first_back]
-        parts = combine(scal, idx, wts, ys, p, pieces, zn, sub, capacity)
+        left, right = cuts[p]
+        lefts = [left] + [0] * (ep - 2) + [left]
+        parts = combine(scal, idx, wts, ys, lefts, right - left, zn, sub, capacity)
         total = parts[0].astype(f32)
         for m in range(1, zn):
             total = total + over_z(parts[m], m).astype(f32)

time: 141 us -> 142 us (level)
  starting transfers between devices: 38.6 us -> 46.3 us
  waiting for transfers between devices: 55.3 us -> 49.7 us
  local copies, waits for them, and re-layouts: 3.73 us -> 0.07 us
  Pallas kernels: 41 us -> 44.3 us
    ppermute x11 -> x13, waiting for transfers between devices: 15.8 us -> 11.2 us  [on_device(): lax.ppermute(x, 'ep', [(i, i ^ m) for i in range(ep)])]
    ppermute x9 -> x12, starting transfers between devices: 23.9 us -> 28.3 us  [on_device(): lax.ppermute(x, 'tp', [(i, i ^ m * CORES) for i in range(tp)])]
    unnamed x36 -> x28, local copies, waits for them, and re-layouts: 3.73 us -> 0.07 us
    pallas_call x3 -> x4, Pallas kernels: 6.61 us -> 9.89 us  [the longest x1 5.82 us: final_state(): pl.pallas_call(functools.partial(state_body, heads, 4 * BLOCK), in_specs=...]
    ppermute x11 -> x13, starting transfers between devices: 13.6 us -> 16.9 us  [on_device(): lax.ppermute(x, 'ep', [(i, i ^ m) for i in range(ep)])]
    ppermute x9 -> x12, waiting for transfers between devices: 39.5 us -> 38.5 us  [on_device(): lax.ppermute(x, 'tp', [(i, i ^ m * CORES) for i in range(tp)])]
  transfers between devices with their start and end apart: 25 -> 30, of which waited for: 11 -> 10; matrix products, arithmetic and copies ran while one was open for 0% -> 0% of each run, Pallas kernels for 29% -> 31%
where the time goes in v2:
time: 142 us
  waiting for transfers between devices  49.7 us (35%)
  starting transfers between devices  46.3 us (33%)
  Pallas kernels  44.3 us (31%)
    ppermute x12, waiting for transfers between devices, on_device(): lax.ppermute(x, 'tp', [(i, i ^ m * CORES) for i in range(tp)])  38.5 us
    ppermute x12, starting transfers between devices, on_device(): lax.ppermute(x, 'tp', [(i, i ^ m * CORES) for i in range(tp)])  28.3 us
    pallas_call x2, Pallas kernels, ffn(): pl.pallas_call(functools.partial(ffn_body, count, pieces, chunks), in_spe...  20 us
    ppermute x13, starting transfers between devices, on_device(): lax.ppermute(x, 'ep', [(i, i ^ m) for i in range(ep)])  16.9 us
    ppermute x13, waiting for transfers between devices, on_device(): lax.ppermute(x, 'ep', [(i, i ^ m) for i in range(ep)])  11.2 us
    pallas_call x1, Pallas kernels, mixer(): pl.pallas_call(functools.partial(mixer_body, heads, ep, 4 * BLOCK), grid_...  8.46 us
    pallas_call x1, Pallas kernels, final_state(): pl.pallas_call(functools.partial(state_body, heads, 4 * BLOCK), in_specs=...  5.82 us
    pallas_call x3, Pallas kernels, combine(): pl.pallas_call(functools.partial(combine_body, experts, capacity, zn, lef...  4.07 us
  transfers between devices with their start and end apart: 30, of which 10 were waited for; matrix products, arithmetic and copies ran while one was open for 0% of the time, Pallas kernels for 31%

profile of v2, /device:TPU:0, one launch (start us, length us, event | category | flops | bytes accessed | tf_op | source)
XLA Modules:
  0.0 142.3 jit_solution(7074666557642607695)
XLA Ops:
  0.6 0.6 collective-permute-start.10
  1.2 0.1 collective-permute-start.11
  1.3 0.4 collective-permute-start.9
  1.7 5.8 %final_state.1 = f32[136,128]{1,0:T(8,128)} custom-call(bf16[2048,256]{1,0:T(8,128)(2,1)} %refs_4_.4, bf16[2048,128]{1,0:T(8,128)(2,1)} %refs_5_.1, f32[1,256]{1,0:T(1,128)} %bitcast.21, f32[2,2048]{1,0:T(2,128)} %bitcast.11), custom_call_target="tpu_custom_call" | custom-call | flops 4000000000 | bytes 2000000 | tf_op jit(solution)/shard_map/final_state/pallas_call | solution.py:97
  7.5 2.6 %collective-permute-start = (f32[136,128]{1,0:T(8,128)}, f32[136,128]{1,0:T(8,128)S(1)}, u32[]{:S(2)}, u32[]{:S(2)}) collective-permute-start(f32[136,128]{1,0:T(8,128)} %final_state.1), channel_id=1, source_target_pairs={{0,8},{8,0},{16,24},{24,16},{1,9},{9,1},{17,25},{25,17},{2,10},{10... | collective-permute-start | bytes 208904 | tf_op jit(solution)/shard_map/ppermute | solution.py:491
  10.2 1.5 %collective-permute-start.1 = (f32[136,128]{1,0:T(8,128)}, f32[136,128]{1,0:T(8,128)S(1)}, u32[]{:S(2)}, u32[]{:S(2)}) collective-permute-start(f32[136,128]{1,0:T(8,128)} %final_state.1), channel_id=1, source_target_pairs={{0,16},{8,24},{16,0},{24,8},{1,17},{9,25},{17,1},{25,9},{2,18},{10... | collective-permute-start | bytes 208904 | tf_op jit(solution)/shard_map/ppermute | solution.py:491
  11.7 0.1 pad_add_fusion.sc_ref
  11.8 1.4 collective-permute-done.refs_0_
  13.1 2.7 %collective-permute-start.2 = (f32[136,128]{1,0:T(8,128)}, f32[136,128]{1,0:T(8,128)S(1)}, u32[]{:S(2)}, u32[]{:S(2)}) collective-permute-start(f32[136,128]{1,0:T(8,128)} %final_state.1), channel_id=1, source_target_pairs={{0,24},{8,16},{16,8},{24,0},{1,25},{9,17},{17,9},{25,1},{2,26},{10... | collective-permute-start | bytes 208904 | tf_op jit(solution)/shard_map/ppermute | solution.py:491
  15.8 0.0 copy-start.3
  15.9 0.0 copy-start.4
  15.9 0.0 copy-start.5
  15.9 0.0 copy-start.6
  15.9 0.0 copy-start.8
  15.9 0.0 copy-start.12
  15.9 0.0 copy-start.13
  15.9 1.7 %pack.1 = (bf16[160,2048]{1,0:T(8,128)(2,1)S(1)}, bf16[160,2048]{1,0:T(8,128)(2,1)S(1)}, bf16[160,2048]{1,0:T(8,128)(2,1)S(1)}, bf16[160,2048]{1,0:T(8,128)(2,1)S(1)}) custom-call(s32[3]{0:T(128)S(1)} %pad_add_fusion.sc_ref, bf16[4,2,64,2048]{3,2,1,0:T(8,128)(2,1)S(1)} %bitcast.10, s32[2,512]{1,0:T(2,128)S(1)} %bitcast.14, f32[1,2048]{1,0:T(1,128)S(1)} %bitcast.13), custom_call_target="tpu_custom_call" | custom-call | flops 4000000000 | bytes 4000000 | tf_op jit(solution)/shard_map/pack/pallas_call | solution.py:313
  17.7 0.1 collective-permute-start.6
  17.8 0.8 collective-permute-done.2.refs_2_
  18.6 8.5 %mixer.1.refs_0_ = bf16[2048,128]{1,0:T(8,128)(2,1)S(1)} custom-call(s32[3]{0:T(128)S(1)} %pad_add_fusion.sc_ref, f32[136,128]{1,0:T(8,128)S(1)} %collective-permute-done.refs_0_, f32[136,128]{1,0:T(8,128)S(1)} %collective-permute-done.1.refs_1_, f32[136,128]{1,0:T(8,128)S(1)} %collective-permute-done.2.refs_2_, bf16[2048,256]{1,0:T(8,128)(2,1)S(1)} %copy-done.4, ...), custom_call_target="tpu_custom_call" | custom-call | flops 12000000000 | bytes 4000000 | tf_op jit(solution)/shard_map/mixer/pallas_call | solution.py:190
  27.1 2.9 %collective-permute-start.4 = (bf16[2048,128]{1,0:T(8,128)(2,1)S(1)}, bf16[2048,128]{1,0:T(8,128)(2,1)S(1)}, u32[]{:S(2)}, u32[]{:S(2)}) collective-permute-start(bf16[2048,128]{1,0:T(8,128)(2,1)S(1)} %mixer.1.refs_0_), channel_id=1, source_target_pairs={{0,4},{1,5},{2,6},{3,7},{4,0},{5,1},{6,2},{7,3},{8,12},{9,13},{10,... | collective-permute-start | bytes 1572872 | tf_op jit(solution)/shard_map/ppermute | solution.py:493
  30.0 1.6 %collective-permute-start.3 = (bf16[2048,128]{1,0:T(8,128)(2,1)S(1)}, bf16[2048,128]{1,0:T(8,128)(2,1)S(1)}, u32[]{:S(2)}, u32[]{:S(2)}) collective-permute-start(bf16[2048,128]{1,0:T(8,128)(2,1)S(1)} %mixer.1.refs_0_), channel_id=1, source_target_pairs={{0,2},{1,3},{2,0},{3,1},{4,6},{5,7},{6,4},{7,5},{8,10},{9,11},{10,... | collective-permute-start | bytes 1572872 | tf_op jit(solution)/shard_map/ppermute | solution.py:493
  31.6 21.4 %collective-permute-done.4.refs_2_ = bf16[2048,128]{1,0:T(8,128)(2,1)S(1)} collective-permute-done((bf16[2048,128]{1,0:T(8,128)(2,1)S(1)}, bf16[2048,128]{1,0:T(8,128)(2,1)S(1)}, u32[]{:S(2)}, u32[]{:S(2)}) %collective-permute-start.4) | collective-permute-done | bytes 524320 | tf_op jit(solution)/shard_map/ppermute | solution.py:493
  52.9 0.6 collective-permute-start.5
  53.5 0.0 collective-permute-done.3.refs_1_
  53.5 1.4 collective-permute-start.8
  54.9 10.8 %collective-permute-done.5.refs_3_ = bf16[2048,128]{1,0:T(8,128)(2,1)S(1)} collective-permute-done((bf16[2048,128]{1,0:T(8,128)(2,1)S(1)}, bf16[2048,128]{1,0:T(8,128)(2,1)S(1)}, u32[]{:S(2)}, u32[]{:S(2)}) %collective-permute-start.5) | collective-permute-done | bytes 524320 | tf_op jit(solution)/shard_map/ppermute | solution.py:493
  65.7 0.5 collective-permute-start.12
  66.2 3.2 %project.1 = (f32[2048,256]{1,0:T(8,128)S(1)}, bf16[2048,256]{1,0:T(8,128)(2,1)S(1)}) custom-call(s32[3]{0:T(128)S(1)} %pad_add_fusion.sc_ref, bf16[2048,128]{1,0:T(8,128)(2,1)S(1)} %mixer.1.refs_0_, bf16[2048,128]{1,0:T(8,128)(2,1)S(1)} %collective-permute-done.3.refs_1_, bf16[2048,128]{1,0:T(8,128)(2,1)S(1)} %collective-permute-done.4.refs_2_, ...), custom_call_target="tpu_custom_call" | custom-call | flops 2000000000 | bytes 6000000 | tf_op jit(solution)/shard_map/project/pallas_call | solution.py:231
  69.5 2.5 %collective-permute-done.8.refs_0_ = bf16[160,2048]{1,0:T(8,128)(2,1)S(1)} collective-permute-done((bf16[160,2048]{1,0:T(8,128)(2,1)S(1)}, bf16[160,2048]{1,0:T(8,128)(2,1)S(1)}, u32[]{:S(2)}, u32[]{:S(2)}) %collective-permute-start.8) | collective-permute-done | bytes 655392 | tf_op jit(solution)/shard_map/ppermute | solution.py:491
  72.0 0.5 collective-permute-start.13
  72.5 0.0 collective-permute-done.10.refs_5_
  72.5 0.0 collective-permute-start.7
  72.5 0.0 collective-permute-done.11.refs_7_
  72.6 10.0 %ffn.2 = (bf16[160,2048]{1,0:T(8,128)(2,1)S(1)}, bf16[160,2048]{1,0:T(8,128)(2,1)S(1)}) custom-call(bf16[160,2048]{1,0:T(8,128)(2,1)S(1)} %collective-permute-done.8.refs_0_, bf16[160,2048]{1,0:T(8,128)(2,1)S(1)} %get-tuple-element.38.refs_1_, bf16[1,2048,896]{2,1,0:T(8,128)(2,1)S(1)} %copy-done, bf16[1,2048,896]{2,1,0:T(8,128)(2,1)} %collective-permute-done.9.refs_3_, ...), custom_call_target="tpu_custom_call" | custom-call | flops 8000000000 | bytes 25000000 | tf_op jit(solution)/shard_map/ffn/pallas_call | solution.py:397
  82.5 1.6 %collective-permute-start.16 = (bf16[160,2048]{1,0:T(8,128)(2,1)S(1)}, bf16[160,2048]{1,0:T(8,128)(2,1)S(1)}, u32[]{:S(2)}, u32[]{:S(2)}) collective-permute-start(bf16[160,2048]{1,0:T(8,128)(2,1)S(1)} %get-tuple-element.43), channel_id=1, source_target_pairs={{0,24},{8,16},{16,8},{24,0},{1,25},{9,17},{17,9},{25,1},{2,26},{10... | collective-permute-start | bytes 1966088 | tf_op jit(solution)/shard_map/ppermute | solution.py:491
  84.1 2.2 %collective-permute-done.13.refs_1_ = bf16[160,2048]{1,0:T(8,128)(2,1)S(1)} collective-permute-done((bf16[160,2048]{1,0:T(8,128)(2,1)S(1)}, bf16[160,2048]{1,0:T(8,128)(2,1)S(1)}, u32[]{:S(2)}, u32[]{:S(2)}) %collective-permute-start.13) | collective-permute-done | bytes 655392 | tf_op jit(solution)/shard_map/ppermute | solution.py:491
  86.3 10.0 %ffn.3 = (bf16[160,512]{1,0:T(8,128)(2,1)S(1)}, bf16[160,768]{1,0:T(8,128)(2,1)S(1)}, bf16[160,768]{1,0:T(8,128)(2,1)S(1)}, bf16[160,512]{1,0:T(8,128)(2,1)S(1)}...) custom-call(bf16[160,2048]{1,0:T(8,128)(2,1)S(1)} %collective-permute-done.12.refs_0_, ...), custom_call_target="tpu_custom_call" | custom-call | flops 8000000000 | bytes 25000000 | tf_op jit(solution)/shard_map/ffn/pallas_call | solution.py:397
  96.3 0.0 copy-start.11
  96.3 0.6 collective-permute-start.14
  96.9 1.4 collective-permute-start.15
  98.3 0.6 collective-permute-start.20
  98.9 1.5 %collective-permute-start.21 = (bf16[160,768]{1,0:T(8,128)(2,1)S(1)}, bf16[160,768]{1,0:T(8,128)(2,1)S(1)}, u32[]{:S(2)}, u32[]{:S(2)}) collective-permute-start(bf16[160,768]{1,0:T(8,128)(2,1)S(1)} %get-tuple-element.49), channel_id=1, source_target_pairs={{0,16},{8,24},{16,0},{24,8},{1,17},{9,25},{17,1},{25,9},{2,18},{10... | collective-permute-start | bytes 737288 | tf_op jit(solution)/shard_map/ppermute | solution.py:491
  100.4 4.3 %collective-permute-done.14.refs_1_ = bf16[160,512]{1,0:T(8,128)(2,1)S(1)} collective-permute-done((bf16[160,512]{1,0:T(8,128)(2,1)S(1)}, bf16[160,512]{1,0:T(8,128)(2,1)S(1)}, u32[]{:S(2)}, u32[]{:S(2)}) %collective-permute-start.14) | collective-permute-done | bytes 163872 | tf_op jit(solution)/shard_map/ppermute | solution.py:491
  104.7 0.5 collective-permute-start.25
  105.2 1.4 collective-permute-start.26
  106.7 1.1 join.1
  107.7 1.3 combine.3
  109.0 1.2 collective-permute-start.17
  110.2 13.0 %collective-permute-start.18 = (bf16[64,512]{1,0:T(8,128)(2,1)S(1)}, bf16[64,512]{1,0:T(8,128)(2,1)S(1)}, u32[]{:S(2)}, u32[]{:S(2)}) collective-permute-start(bf16[64,512]{1,0:T(8,128)(2,1)S(1)} %get-tuple-element.46), channel_id=1, source_target_pairs={{0,4},{1,5},{2,6},{3,7},{4,0},{5,1},{6,2},{7,3},{8,12},{9,13},{10,... | collective-permute-start | bytes 196616 | tf_op jit(solution)/shard_map/ppermute | solution.py:493
  123.2 1.4 combine.4
  124.6 0.7 collective-permute-start.22
  125.3 3.8 %collective-permute-start.23 = (bf16[64,768]{1,0:T(8,128)(2,1)S(1)}, bf16[64,768]{1,0:T(8,128)(2,1)S(1)}, u32[]{:S(2)}, u32[]{:S(2)}) collective-permute-start(bf16[64,768]{1,0:T(8,128)(2,1)S(1)} %get-tuple-element.52), channel_id=1, source_target_pairs={{0,4},{1,5},{2,6},{3,7},{4,0},{5,1},{6,2},{7,3},{8,12},{9,13},{10,... | collective-permute-start | bytes 294920 | tf_op jit(solution)/shard_map/ppermute | solution.py:493
  129.1 1.4 combine.5
  130.5 0.1 collective-permute-start.24
  130.6 0.5 collective-permute-start.27
  131.2 3.8 %collective-permute-start.28 = (bf16[64,768]{1,0:T(8,128)(2,1)S(1)}, bf16[64,768]{1,0:T(8,128)(2,1)S(1)}, u32[]{:S(2)}, u32[]{:S(2)}) collective-permute-start(bf16[64,768]{1,0:T(8,128)(2,1)S(1)} %get-tuple-element.58), channel_id=1, source_target_pairs={{0,4},{1,5},{2,6},{3,7},{4,0},{5,1},{6,2},{7,3},{8,12},{9,13},{10,... | collective-permute-start | bytes 294920 | tf_op jit(solution)/shard_map/ppermute | solution.py:493
  135.0 0.1 collective-permute-start.29
  135.2 1.9 %collective-permute-done.24 = bf16[64,768]{1,0:T(8,128)(2,1)S(1)} collective-permute-done((bf16[64,768]{1,0:T(8,128)(2,1)S(1)}, bf16[64,768]{1,0:T(8,128)(2,1)S(1)}, u32[]{:S(2)}, u32[]{:S(2)}) %collective-permute-start.24) | collective-permute-done | bytes 98336 | tf_op jit(solution)/shard_map/ppermute | solution.py:493
  137.0 0.1 add_convert_fusion.1
  137.1 0.9 collective-permute-done.28
  138.0 3.5 %collective-permute-done.29 = bf16[64,768]{1,0:T(8,128)(2,1)S(1)} collective-permute-done((bf16[64,768]{1,0:T(8,128)(2,1)S(1)}, bf16[64,768]{1,0:T(8,128)(2,1)S(1)}, u32[]{:S(2)}, u32[]{:S(2)}) %collective-permute-start.29) | collective-permute-done | bytes 98336 | tf_op jit(solution)/shard_map/ppermute | solution.py:493
  141.5 0.1 add_convert_fusion
  141.6 0.7 pad_maximum_fusion
  (39 shorter events, 0.1 us)
Async XLA Ops:
  0.6 71.9 %collective-permute-start.10 = (bf16[1,2048,896]{2,1,0:T(8,128)(2,1)}, bf16[1,2048,896]{2,1,0:T(8,128)(2,1)}, u32[]{:S(2)}, u32[]{:S(2)}) collective-permute-start(bf16[1,2048,896]{2,1,0:T(8,128)(2,1)} %refs_4_.7), channel_id=1, source_target_pairs={{0,1},{1,0},{2,3},{3,2},{4,5},{5,4},{6,7},{7,6},{8,9},{9,8},{10,11... | collective-permute-start | bytes 11010056 | tf_op jit(solution)/shard_map/ppermute | solution.py:492
  1.2 71.3 %collective-permute-start.11 = (bf16[1,896,2048]{2,1,0:T(8,128)(2,1)}, bf16[1,896,2048]{2,1,0:T(8,128)(2,1)}, u32[]{:S(2)}, u32[]{:S(2)}) collective-permute-start(bf16[1,896,2048]{2,1,0:T(8,128)(2,1)} %refs_6_.5), channel_id=1, source_target_pairs={{0,1},{1,0},{2,3},{3,2},{4,5},{5,4},{6,7},{7,6},{8,9},{9,8},{10,11... | collective-permute-start | bytes 11010056 | tf_op jit(solution)/shard_map/ppermute | solution.py:492
  1.3 71.3 %collective-permute-start.9 = (bf16[1,2048,896]{2,1,0:T(8,128)(2,1)}, bf16[1,2048,896]{2,1,0:T(8,128)(2,1)}, u32[]{:S(2)}, u32[]{:S(2)}) collective-permute-start(bf16[1,2048,896]{2,1,0:T(8,128)(2,1)} %refs_2_.3), channel_id=1, source_target_pairs={{0,1},{1,0},{2,3},{3,2},{4,5},{5,4},{6,7},{7,6},{8,9},{9,8},{10,11... | collective-permute-start | bytes 11010056 | tf_op jit(solution)/shard_map/ppermute | solution.py:492
  1.7 14.1 %copy-start.2 = (bf16[512,2048]{1,0:T(8,128)(2,1)S(1)}, bf16[512,2048]{1,0:T(8,128)(2,1)}, u32[]{:S(2)}) copy-start(bf16[512,2048]{1,0:T(8,128)(2,1)} %param.23) | copy-start | bytes 6291460
  1.7 14.1 %copy-start.9 = (f32[2048]{0:T(1024)S(1)}, f32[2048]{0:T(1024)}, u32[]{:S(2)}) copy-start(f32[2048]{0:T(1024)} %param.24) | copy-start | bytes 24580
  1.7 14.1 %copy-start.10 = (s32[512,2]{0,1:T(2,128)S(1)}, s32[512,2]{0,1:T(2,128)}, u32[]{:S(2)}) copy-start(s32[512,2]{0,1:T(2,128)} %param.25) | copy-start | bytes 12292
  7.5 5.6 %collective-permute-start = (f32[136,128]{1,0:T(8,128)}, f32[136,128]{1,0:T(8,128)S(1)}, u32[]{:S(2)}, u32[]{:S(2)}) collective-permute-start(f32[136,128]{1,0:T(8,128)} %final_state.1), channel_id=1, source_target_pairs={{0,8},{8,0},{16,24},{24,16},{1,9},{9,1},{17,25},{25,17},{2,10},{10... | collective-permute-start | bytes 208904 | tf_op jit(solution)/shard_map/ppermute | solution.py:491
  10.2 7.5 %collective-permute-start.1 = (f32[136,128]{1,0:T(8,128)}, f32[136,128]{1,0:T(8,128)S(1)}, u32[]{:S(2)}, u32[]{:S(2)}) collective-permute-start(f32[136,128]{1,0:T(8,128)} %final_state.1), channel_id=1, source_target_pairs={{0,16},{8,24},{16,0},{24,8},{1,17},{9,25},{17,1},{25,9},{2,18},{10... | collective-permute-start | bytes 208904 | tf_op jit(solution)/shard_map/ppermute | solution.py:491
  13.1 5.4 %collective-permute-start.2 = (f32[136,128]{1,0:T(8,128)}, f32[136,128]{1,0:T(8,128)S(1)}, u32[]{:S(2)}, u32[]{:S(2)}) collective-permute-start(f32[136,128]{1,0:T(8,128)} %final_state.1), channel_id=1, source_target_pairs={{0,24},{8,16},{16,8},{24,0},{1,25},{9,17},{17,9},{25,1},{2,26},{10... | collective-permute-start | bytes 208904 | tf_op jit(solution)/shard_map/ppermute | solution.py:491
  15.8 1.8 %copy-start.7 = (bf16[1024,256]{1,0:T(8,128)(2,1)S(1)}, bf16[1024,256]{1,0:T(8,128)(2,1)}, u32[]{:S(2)}) copy-start(bf16[1024,256]{1,0:T(8,128)(2,1)} %refs_4_.5) | copy-start | bytes 1572868
  15.8 2.7 %copy-start.3 = (bf16[2048,256]{1,0:T(8,128)(2,1)S(1)}, bf16[2048,256]{1,0:T(8,128)(2,1)}, u32[]{:S(2)}) copy-start(bf16[2048,256]{1,0:T(8,128)(2,1)} %refs_4_.4) | copy-start | bytes 3145732
  15.9 2.7 %copy-start.4 = (bf16[2048,256]{1,0:T(8,128)(2,1)S(1)}, bf16[2048,256]{1,0:T(8,128)(2,1)}, u32[]{:S(2)}) copy-start(bf16[2048,256]{1,0:T(8,128)(2,1)} %refs_3_) | copy-start | bytes 3145732
  15.9 2.7 %copy-start.5 = (bf16[2048,128]{1,0:T(8,128)(2,1)S(1)}, bf16[2048,128]{1,0:T(8,128)(2,1)}, u32[]{:S(2)}) copy-start(bf16[2048,128]{1,0:T(8,128)(2,1)} %refs_5_.1) | copy-start | bytes 1572868
  15.9 2.7 %copy-start.6 = (bf16[2048,128]{1,0:T(8,128)(2,1)S(1)}, bf16[2048,128]{1,0:T(8,128)(2,1)}, u32[]{:S(2)}) copy-start(bf16[2048,128]{1,0:T(8,128)(2,1)} %refs_6_.3) | copy-start | bytes 1572868
  15.9 2.7 %copy-start.8 = (f32[2048,2]{0,1:T(2,128)S(1)}, f32[2048,2]{0,1:T(2,128)}, u32[]{:S(2)}) copy-start(f32[2048,2]{0,1:T(2,128)} %param.20) | copy-start | bytes 49156
  15.9 2.7 %copy-start.12 = (f32[256]{0:T(256)S(1)}, f32[256]{0:T(256)}, u32[]{:S(2)}) copy-start(f32[256]{0:T(256)} %param.19) | copy-start | bytes 3076
  15.9 2.7 %copy-start.13 = (f32[128]{0:T(128)S(1)}, f32[128]{0:T(128)}, u32[]{:S(2)}) copy-start(f32[128]{0:T(128)} %param.21) | copy-start | bytes 1540
  17.7 12.3 %collective-permute-start.6 = (bf16[1024,256]{1,0:T(8,128)(2,1)S(1)}, bf16[1024,256]{1,0:T(8,128)(2,1)S(1)}, u32[]{:S(2)}, u32[]{:S(2)}) collective-permute-start(bf16[1024,256]{1,0:T(8,128)(2,1)S(1)} %copy-done.7), channel_id=1, source_target_pairs={{0,1},{1,0},{2,3},{3,2},{4,5},{5,4},{6,7},{7,6},{8,9},{9,8},{10,11... | collective-permute-start | bytes 1572872 | tf_op jit(solution)/shard_map/ppermute | solution.py:492
  27.1 25.9 %collective-permute-start.4 = (bf16[2048,128]{1,0:T(8,128)(2,1)S(1)}, bf16[2048,128]{1,0:T(8,128)(2,1)S(1)}, u32[]{:S(2)}, u32[]{:S(2)}) collective-permute-start(bf16[2048,128]{1,0:T(8,128)(2,1)S(1)} %mixer.1.refs_0_), channel_id=1, source_target_pairs={{0,4},{1,5},{2,6},{3,7},{4,0},{5,1},{6,2},{7,3},{8,12},{9,13},{10,... | collective-permute-start | bytes 1572872 | tf_op jit(solution)/shard_map/ppermute | solution.py:493
  30.0 23.5 %collective-permute-start.3 = (bf16[2048,128]{1,0:T(8,128)(2,1)S(1)}, bf16[2048,128]{1,0:T(8,128)(2,1)S(1)}, u32[]{:S(2)}, u32[]{:S(2)}) collective-permute-start(bf16[2048,128]{1,0:T(8,128)(2,1)S(1)} %mixer.1.refs_0_), channel_id=1, source_target_pairs={{0,2},{1,3},{2,0},{3,1},{4,6},{5,7},{6,4},{7,5},{8,10},{9,11},{10,... | collective-permute-start | bytes 1572872 | tf_op jit(solution)/shard_map/ppermute | solution.py:493
  52.9 12.8 %collective-permute-start.5 = (bf16[2048,128]{1,0:T(8,128)(2,1)S(1)}, bf16[2048,128]{1,0:T(8,128)(2,1)S(1)}, u32[]{:S(2)}, u32[]{:S(2)}) collective-permute-start(bf16[2048,128]{1,0:T(8,128)(2,1)S(1)} %collective-permute-done.4.refs_2_), channel_id=1, source_target_pairs={{0,2},{1,3},{2,0},{3,1},{4,6},{5,7},{6,4},{7,5},{8,10},{9,11},{10,... | collective-permute-start | bytes 1572872 | tf_op jit(solution)/shard_map/ppermute | solution.py:493
  53.5 18.5 %collective-permute-start.8 = (bf16[160,2048]{1,0:T(8,128)(2,1)S(1)}, bf16[160,2048]{1,0:T(8,128)(2,1)S(1)}, u32[]{:S(2)}, u32[]{:S(2)}) collective-permute-start(bf16[160,2048]{1,0:T(8,128)(2,1)S(1)} %get-tuple-element.36), channel_id=1, source_target_pairs={{0,24},{8,16},{16,8},{24,0},{1,25},{9,17},{17,9},{25,1},{2,26},{10... | collective-permute-start | bytes 1966088 | tf_op jit(solution)/shard_map/ppermute | solution.py:491
  54.9 17.6 %copy-start = (bf16[1,2048,896]{2,1,0:T(8,128)(2,1)S(1)}, bf16[1,2048,896]{2,1,0:T(8,128)(2,1)}, u32[]{:S(2)}) copy-start(bf16[1,2048,896]{2,1,0:T(8,128)(2,1)} %refs_2_.3) | copy-start | bytes 11010052
  54.9 17.6 %copy-start.1 = (bf16[1,2048,896]{2,1,0:T(8,128)(2,1)S(1)}, bf16[1,2048,896]{2,1,0:T(8,128)(2,1)}, u32[]{:S(2)}) copy-start(bf16[1,2048,896]{2,1,0:T(8,128)(2,1)} %refs_4_.7) | copy-start | bytes 11010052
  65.7 18.4 %collective-permute-start.12 = (bf16[160,2048]{1,0:T(8,128)(2,1)S(1)}, bf16[160,2048]{1,0:T(8,128)(2,1)S(1)}, u32[]{:S(2)}, u32[]{:S(2)}) collective-permute-start(bf16[160,2048]{1,0:T(8,128)(2,1)S(1)} %get-tuple-element.32), channel_id=1, source_target_pairs={{0,8},{8,0},{16,24},{24,16},{1,9},{9,1},{17,25},{25,17},{2,10},{10... | collective-permute-start | bytes 1966088 | tf_op jit(solution)/shard_map/ppermute | solution.py:491
  72.0 14.3 %collective-permute-start.13 = (bf16[160,2048]{1,0:T(8,128)(2,1)S(1)}, bf16[160,2048]{1,0:T(8,128)(2,1)S(1)}, u32[]{:S(2)}, u32[]{:S(2)}) collective-permute-start(bf16[160,2048]{1,0:T(8,128)(2,1)S(1)} %get-tuple-element.40), channel_id=1, source_target_pairs={{0,16},{8,24},{16,0},{24,8},{1,17},{9,25},{17,1},{25,9},{2,18},{10... | collective-permute-start | bytes 1966088 | tf_op jit(solution)/shard_map/ppermute | solution.py:491
  72.5 26.4 %collective-permute-start.7 = (bf16[2048,256]{1,0:T(8,128)(2,1)S(1)}, bf16[2048,256]{1,0:T(8,128)(2,1)S(1)}, u32[]{:S(2)}, u32[]{:S(2)}) collective-permute-start(bf16[2048,256]{1,0:T(8,128)(2,1)S(1)} %get-tuple-element.35), channel_id=1, source_target_pairs={{0,1},{1,0},{2,3},{3,2},{4,5},{5,4},{6,7},{7,6},{8,9},{9,8},{10,11... | collective-permute-start | bytes 3145736 | tf_op jit(solution)/shard_map/ppermute | solution.py:492
  82.5 25.2 %collective-permute-start.16 = (bf16[160,2048]{1,0:T(8,128)(2,1)S(1)}, bf16[160,2048]{1,0:T(8,128)(2,1)S(1)}, u32[]{:S(2)}, u32[]{:S(2)}) collective-permute-start(bf16[160,2048]{1,0:T(8,128)(2,1)S(1)} %get-tuple-element.43), channel_id=1, source_target_pairs={{0,24},{8,16},{16,8},{24,0},{1,25},{9,17},{17,9},{25,1},{2,26},{10... | collective-permute-start | bytes 1966088 | tf_op jit(solution)/shard_map/ppermute | solution.py:491
  96.3 11.4 %copy-start.11 = (f32[512,2]{0,1:T(2,128)S(1)}, f32[512,2]{0,1:T(2,128)}, u32[]{:S(2)}) copy-start(f32[512,2]{0,1:T(2,128)} %param.26) | copy-start | bytes 12292
  96.3 8.4 %collective-permute-start.14 = (bf16[160,512]{1,0:T(8,128)(2,1)S(1)}, bf16[160,512]{1,0:T(8,128)(2,1)S(1)}, u32[]{:S(2)}, u32[]{:S(2)}) collective-permute-start(bf16[160,512]{1,0:T(8,128)(2,1)S(1)} %get-tuple-element.41), channel_id=1, source_target_pairs={{0,8},{8,0},{16,24},{24,16},{1,9},{9,1},{17,25},{25,17},{2,10},{10... | collective-permute-start | bytes 491528 | tf_op jit(solution)/shard_map/ppermute | solution.py:491
  96.9 8.3 %collective-permute-start.15 = (bf16[160,512]{1,0:T(8,128)(2,1)S(1)}, bf16[160,512]{1,0:T(8,128)(2,1)S(1)}, u32[]{:S(2)}, u32[]{:S(2)}) collective-permute-start(bf16[160,512]{1,0:T(8,128)(2,1)S(1)} %get-tuple-element.42), channel_id=1, source_target_pairs={{0,16},{8,24},{16,0},{24,8},{1,17},{9,25},{17,1},{25,9},{2,18},{10... | collective-permute-start | bytes 491528 | tf_op jit(solution)/shard_map/ppermute | solution.py:491
  98.3 11.9 %collective-permute-start.20 = (bf16[160,768]{1,0:T(8,128)(2,1)S(1)}, bf16[160,768]{1,0:T(8,128)(2,1)S(1)}, u32[]{:S(2)}, u32[]{:S(2)}) collective-permute-start(bf16[160,768]{1,0:T(8,128)(2,1)S(1)} %get-tuple-element.48), channel_id=1, source_target_pairs={{0,8},{8,0},{16,24},{24,16},{1,9},{9,1},{17,25},{25,17},{2,10},{10... | collective-permute-start | bytes 737288 | tf_op jit(solution)/shard_map/ppermute | solution.py:491
  98.9 24.3 %collective-permute-start.21 = (bf16[160,768]{1,0:T(8,128)(2,1)S(1)}, bf16[160,768]{1,0:T(8,128)(2,1)S(1)}, u32[]{:S(2)}, u32[]{:S(2)}) collective-permute-start(bf16[160,768]{1,0:T(8,128)(2,1)S(1)} %get-tuple-element.49), channel_id=1, source_target_pairs={{0,16},{8,24},{16,0},{24,8},{1,17},{9,25},{17,1},{25,9},{2,18},{10... | collective-permute-start | bytes 737288 | tf_op jit(solution)/shard_map/ppermute | solution.py:491
  104.7 19.9 %collective-permute-start.25 = (bf16[160,768]{1,0:T(8,128)(2,1)S(1)}, bf16[160,768]{1,0:T(8,128)(2,1)S(1)}, u32[]{:S(2)}, u32[]{:S(2)}) collective-permute-start(bf16[160,768]{1,0:T(8,128)(2,1)S(1)} %get-tuple-element.54), channel_id=1, source_target_pairs={{0,8},{8,0},{16,24},{24,16},{1,9},{9,1},{17,25},{25,17},{2,10},{10... | collective-permute-start | bytes 737288 | tf_op jit(solution)/shard_map/ppermute | solution.py:491
  105.2 20.1 %collective-permute-start.26 = (bf16[160,768]{1,0:T(8,128)(2,1)S(1)}, bf16[160,768]{1,0:T(8,128)(2,1)S(1)}, u32[]{:S(2)}, u32[]{:S(2)}) collective-permute-start(bf16[160,768]{1,0:T(8,128)(2,1)S(1)} %get-tuple-element.55), channel_id=1, source_target_pairs={{0,16},{8,24},{16,0},{24,8},{1,17},{9,25},{17,1},{25,9},{2,18},{10... | collective-permute-start | bytes 737288 | tf_op jit(solution)/shard_map/ppermute | solution.py:491
  109.0 21.5 %collective-permute-start.17 = (bf16[64,512]{1,0:T(8,128)(2,1)S(1)}, bf16[64,512]{1,0:T(8,128)(2,1)S(1)}, u32[]{:S(2)}, u32[]{:S(2)}) collective-permute-start(bf16[64,512]{1,0:T(8,128)(2,1)S(1)} %get-tuple-element.45), channel_id=1, source_target_pairs={{0,2},{1,3},{2,0},{3,1},{4,6},{5,7},{6,4},{7,5},{8,10},{9,11},{10,... | collective-permute-start | bytes 196616 | tf_op jit(solution)/shard_map/ppermute | solution.py:493
  110.2 20.4 %collective-permute-start.18 = (bf16[64,512]{1,0:T(8,128)(2,1)S(1)}, bf16[64,512]{1,0:T(8,128)(2,1)S(1)}, u32[]{:S(2)}, u32[]{:S(2)}) collective-permute-start(bf16[64,512]{1,0:T(8,128)(2,1)S(1)} %get-tuple-element.46), channel_id=1, source_target_pairs={{0,4},{1,5},{2,6},{3,7},{4,0},{5,1},{6,2},{7,3},{8,12},{9,13},{10,... | collective-permute-start | bytes 196616 | tf_op jit(solution)/shard_map/ppermute | solution.py:493
  123.2 7.9 %collective-permute-start.19 = (bf16[64,512]{1,0:T(8,128)(2,1)S(1)}, bf16[64,512]{1,0:T(8,128)(2,1)S(1)}, u32[]{:S(2)}, u32[]{:S(2)}) collective-permute-start(bf16[64,512]{1,0:T(8,128)(2,1)S(1)} %get-tuple-element.47), channel_id=1, source_target_pairs={{0,6},{1,7},{2,4},{3,5},{4,2},{5,3},{6,0},{7,1},{8,14},{9,15},{10,... | collective-permute-start | bytes 196616 | tf_op jit(solution)/shard_map/ppermute | solution.py:493
  124.6 10.4 %collective-permute-start.22 = (bf16[64,768]{1,0:T(8,128)(2,1)S(1)}, bf16[64,768]{1,0:T(8,128)(2,1)S(1)}, u32[]{:S(2)}, u32[]{:S(2)}) collective-permute-start(bf16[64,768]{1,0:T(8,128)(2,1)S(1)} %get-tuple-element.51), channel_id=1, source_target_pairs={{0,2},{1,3},{2,0},{3,1},{4,6},{5,7},{6,4},{7,5},{8,10},{9,11},{10,... | collective-permute-start | bytes 294920 | tf_op jit(solution)/shard_map/ppermute | solution.py:493
  125.3 9.8 %collective-permute-start.23 = (bf16[64,768]{1,0:T(8,128)(2,1)S(1)}, bf16[64,768]{1,0:T(8,128)(2,1)S(1)}, u32[]{:S(2)}, u32[]{:S(2)}) collective-permute-start(bf16[64,768]{1,0:T(8,128)(2,1)S(1)} %get-tuple-element.52), channel_id=1, source_target_pairs={{0,4},{1,5},{2,6},{3,7},{4,0},{5,1},{6,2},{7,3},{8,12},{9,13},{10,... | collective-permute-start | bytes 294920 | tf_op jit(solution)/shard_map/ppermute | solution.py:493
  130.5 6.5 %collective-permute-start.24 = (bf16[64,768]{1,0:T(8,128)(2,1)S(1)}, bf16[64,768]{1,0:T(8,128)(2,1)S(1)}, u32[]{:S(2)}, u32[]{:S(2)}) collective-permute-start(bf16[64,768]{1,0:T(8,128)(2,1)S(1)} %get-tuple-element.53), channel_id=1, source_target_pairs={{0,6},{1,7},{2,4},{3,5},{4,2},{5,3},{6,0},{7,1},{8,14},{9,15},{10,... | collective-permute-start | bytes 294920 | tf_op jit(solution)/shard_map/ppermute | solution.py:493
  130.6 6.5 %collective-permute-start.27 = (bf16[64,768]{1,0:T(8,128)(2,1)S(1)}, bf16[64,768]{1,0:T(8,128)(2,1)S(1)}, u32[]{:S(2)}, u32[]{:S(2)}) collective-permute-start(bf16[64,768]{1,0:T(8,128)(2,1)S(1)} %get-tuple-element.57), channel_id=1, source_target_pairs={{0,2},{1,3},{2,0},{3,1},{4,6},{5,7},{6,4},{7,5},{8,10},{9,11},{10,... | collective-permute-start | bytes 294920 | tf_op jit(solution)/shard_map/ppermute | solution.py:493
  131.2 6.9 %collective-permute-start.28 = (bf16[64,768]{1,0:T(8,128)(2,1)S(1)}, bf16[64,768]{1,0:T(8,128)(2,1)S(1)}, u32[]{:S(2)}, u32[]{:S(2)}) collective-permute-start(bf16[64,768]{1,0:T(8,128)(2,1)S(1)} %get-tuple-element.58), channel_id=1, source_target_pairs={{0,4},{1,5},{2,6},{3,7},{4,0},{5,1},{6,2},{7,3},{8,12},{9,13},{10,... | collective-permute-start | bytes 294920 | tf_op jit(solution)/shard_map/ppermute | solution.py:493
  135.0 6.5 %collective-permute-start.29 = (bf16[64,768]{1,0:T(8,128)(2,1)S(1)}, bf16[64,768]{1,0:T(8,128)(2,1)S(1)}, u32[]{:S(2)}, u32[]{:S(2)}) collective-permute-start(bf16[64,768]{1,0:T(8,128)(2,1)S(1)} %get-tuple-element.59), channel_id=1, source_target_pairs={{0,6},{1,7},{2,4},{3,5},{4,2},{5,3},{6,0},{7,1},{8,14},{9,15},{10,... | collective-permute-start | bytes 294920 | tf_op jit(solution)/shard_map/ppermute | solution.py:493

commit v3 on v2

--- a/solution.py
+++ b/solution.py
@@ -13,6 +13,7 @@
 TOPK = 2
 CORES = 2
 PIECES = (2, 3, 3)
+STATE_GROUP = 4
 MIXER_ROWS = 2048
 FFN_VMEM = 36 * 1024 * 1024
 VMEM = 20 * 1024 * 1024
@@ -69,6 +70,7 @@
     later = (row < lax.broadcasted_iota(jnp.int32, (rows, rows), 1)).astype(bf16)
     s = jnp.zeros((vw, kw), f32)
     l = jnp.zeros((1, kw), f32)
+    parts = []
     copies[0].wait()
     copies[1].wait()
     for at in range(0, length, rows):
@@ -78,11 +80,15 @@
         rs = slice(at, at + rows)
         key, logf = forget_log(heads, f_ref[rs, :], gap_ref[...], extra_ref[:, rs])
         hi, lo = split2(logf)
-        rest = mm(later, hi) + mm(later, lo)
-        whole = rest[0:1] + logf[0:1]
-        ks = (key * jnp.exp(rest)).astype(bf16)
-        s = s * jnp.exp(whole) + mm(v_ref[rs, :], ks, ((0,), (0,)))
-        l = l + whole
+        parts.append((rs, key, logf[0:1], mm(later, hi) + mm(later, lo)))
+        if len(parts) < STATE_GROUP and at + rows < length:
+            continue
+        for rs, key, first, rest in parts:
+            whole = rest[0:1] + first
+            ks = (key * jnp.exp(rest)).astype(bf16)
+            s = s * jnp.exp(whole) + mm(v_ref[rs, :], ks, ((0,), (0,)))
+            l = l + whole
+        parts = []
     for h in range(heads):
         st_ref[h * VAL_DIM : (h + 1) * VAL_DIM, :] = s[
             h * VAL_DIM : (h + 1) * VAL_DIM, h * KEY_DIM : (h + 1) * KEY_DIM

time: 142 us -> 141 us (level)
  no operation moved by 1% of the time
where the time goes in v3:
time: 141 us
  waiting for transfers between devices  49.5 us (35%)
  starting transfers between devices  46.5 us (33%)
  Pallas kernels  43 us (30%)
    ppermute x12, waiting for transfers between devices, on_device(): lax.ppermute(x, 'tp', [(i, i ^ m * CORES) for i in range(tp)])  38.3 us
    ppermute x12, starting transfers between devices, on_device(): lax.ppermute(x, 'tp', [(i, i ^ m * CORES) for i in range(tp)])  28.5 us
    pallas_call x2, Pallas kernels, ffn(): pl.pallas_call(functools.partial(ffn_body, count, pieces, chunks), in_spe...  20 us
    ppermute x13, starting transfers between devices, on_device(): lax.ppermute(x, 'ep', [(i, i ^ m) for i in range(ep)])  16.9 us
    ppermute x13, waiting for transfers between devices, on_device(): lax.ppermute(x, 'ep', [(i, i ^ m) for i in range(ep)])  11.2 us
    pallas_call x1, Pallas kernels, mixer(): pl.pallas_call(functools.partial(mixer_body, heads, ep, 4 * BLOCK), grid_...  8.47 us
    pallas_call x1, Pallas kernels, final_state(): pl.pallas_call(functools.partial(state_body, heads, 4 * BLOCK), in_specs=...  4.51 us
    pallas_call x3, Pallas kernels, combine(): pl.pallas_call(functools.partial(combine_body, experts, capacity, zn, lef...  4.07 us
  transfers between devices with their start and end apart: 30, of which 10 were waited for; matrix products, arithmetic and copies ran while one was open for 0% of the time, Pallas kernels for 31%

profile of v3, /device:TPU:0, one launch (start us, length us, event | category | flops | bytes accessed | tf_op | source)
XLA Modules:
  0.0 141.0 jit_solution(5317225898179896297)
XLA Ops:
  0.6 0.6 collective-permute-start.10
  1.2 0.1 collective-permute-start.11
  1.3 0.4 collective-permute-start.9
  1.7 4.5 %final_state.1 = f32[136,128]{1,0:T(8,128)} custom-call(bf16[2048,256]{1,0:T(8,128)(2,1)} %refs_4_.4, bf16[2048,128]{1,0:T(8,128)(2,1)} %refs_5_.1, f32[1,256]{1,0:T(1,128)} %bitcast.21, f32[2,2048]{1,0:T(2,128)} %bitcast.11), custom_call_target="tpu_custom_call" | custom-call | flops 4000000000 | bytes 2000000 | tf_op jit(solution)/shard_map/final_state/pallas_call | solution.py:103
  6.2 2.6 %collective-permute-start = (f32[136,128]{1,0:T(8,128)}, f32[136,128]{1,0:T(8,128)S(1)}, u32[]{:S(2)}, u32[]{:S(2)}) collective-permute-start(f32[136,128]{1,0:T(8,128)} %final_state.1), channel_id=1, source_target_pairs={{0,8},{8,0},{16,24},{24,16},{1,9},{9,1},{17,25},{25,17},{2,10},{10... | collective-permute-start | bytes 208904 | tf_op jit(solution)/shard_map/ppermute | solution.py:497
  8.8 1.5 %collective-permute-start.1 = (f32[136,128]{1,0:T(8,128)}, f32[136,128]{1,0:T(8,128)S(1)}, u32[]{:S(2)}, u32[]{:S(2)}) collective-permute-start(f32[136,128]{1,0:T(8,128)} %final_state.1), channel_id=1, source_target_pairs={{0,16},{8,24},{16,0},{24,8},{1,17},{9,25},{17,1},{25,9},{2,18},{10... | collective-permute-start | bytes 208904 | tf_op jit(solution)/shard_map/ppermute | solution.py:497
  10.4 0.1 pad_add_fusion.sc_ref
  10.4 1.4 collective-permute-done.refs_0_
  11.8 2.7 %collective-permute-start.2 = (f32[136,128]{1,0:T(8,128)}, f32[136,128]{1,0:T(8,128)S(1)}, u32[]{:S(2)}, u32[]{:S(2)}) collective-permute-start(f32[136,128]{1,0:T(8,128)} %final_state.1), channel_id=1, source_target_pairs={{0,24},{8,16},{16,8},{24,0},{1,25},{9,17},{17,9},{25,1},{2,26},{10... | collective-permute-start | bytes 208904 | tf_op jit(solution)/shard_map/ppermute | solution.py:497
  14.5 0.0 copy-start.3
  14.6 0.0 copy-start.4
  14.6 0.0 copy-start.5
  14.6 0.0 copy-start.6
  14.6 0.0 copy-start.8
  14.6 0.0 copy-start.12
  14.6 0.0 copy-start.13
  14.6 1.7 %pack.1 = (bf16[160,2048]{1,0:T(8,128)(2,1)S(1)}, bf16[160,2048]{1,0:T(8,128)(2,1)S(1)}, bf16[160,2048]{1,0:T(8,128)(2,1)S(1)}, bf16[160,2048]{1,0:T(8,128)(2,1)S(1)}) custom-call(s32[3]{0:T(128)S(1)} %pad_add_fusion.sc_ref, bf16[4,2,64,2048]{3,2,1,0:T(8,128)(2,1)S(1)} %bitcast.10, s32[2,512]{1,0:T(2,128)S(1)} %bitcast.14, f32[1,2048]{1,0:T(1,128)S(1)} %bitcast.13), custom_call_target="tpu_custom_call" | custom-call | flops 4000000000 | bytes 4000000 | tf_op jit(solution)/shard_map/pack/pallas_call | solution.py:319
  16.4 0.0 collective-permute-done.1.refs_1_
  16.4 0.1 collective-permute-start.6
  16.5 0.8 collective-permute-done.2.refs_2_
  17.3 8.5 %mixer.1.refs_0_ = bf16[2048,128]{1,0:T(8,128)(2,1)S(1)} custom-call(s32[3]{0:T(128)S(1)} %pad_add_fusion.sc_ref, f32[136,128]{1,0:T(8,128)S(1)} %collective-permute-done.refs_0_, f32[136,128]{1,0:T(8,128)S(1)} %collective-permute-done.1.refs_1_, f32[136,128]{1,0:T(8,128)S(1)} %collective-permute-done.2.refs_2_, bf16[2048,256]{1,0:T(8,128)(2,1)S(1)} %copy-done.4, ...), custom_call_target="tpu_custom_call" | custom-call | flops 12000000000 | bytes 4000000 | tf_op jit(solution)/shard_map/mixer/pallas_call | solution.py:196
  25.8 2.9 %collective-permute-start.4 = (bf16[2048,128]{1,0:T(8,128)(2,1)S(1)}, bf16[2048,128]{1,0:T(8,128)(2,1)S(1)}, u32[]{:S(2)}, u32[]{:S(2)}) collective-permute-start(bf16[2048,128]{1,0:T(8,128)(2,1)S(1)} %mixer.1.refs_0_), channel_id=1, source_target_pairs={{0,4},{1,5},{2,6},{3,7},{4,0},{5,1},{6,2},{7,3},{8,12},{9,13},{10,... | collective-permute-start | bytes 1572872 | tf_op jit(solution)/shard_map/ppermute | solution.py:499
  28.7 1.6 %collective-permute-start.3 = (bf16[2048,128]{1,0:T(8,128)(2,1)S(1)}, bf16[2048,128]{1,0:T(8,128)(2,1)S(1)}, u32[]{:S(2)}, u32[]{:S(2)}) collective-permute-start(bf16[2048,128]{1,0:T(8,128)(2,1)S(1)} %mixer.1.refs_0_), channel_id=1, source_target_pairs={{0,2},{1,3},{2,0},{3,1},{4,6},{5,7},{6,4},{7,5},{8,10},{9,11},{10,... | collective-permute-start | bytes 1572872 | tf_op jit(solution)/shard_map/ppermute | solution.py:499
  30.3 21.4 %collective-permute-done.4.refs_2_ = bf16[2048,128]{1,0:T(8,128)(2,1)S(1)} collective-permute-done((bf16[2048,128]{1,0:T(8,128)(2,1)S(1)}, bf16[2048,128]{1,0:T(8,128)(2,1)S(1)}, u32[]{:S(2)}, u32[]{:S(2)}) %collective-permute-start.4) | collective-permute-done | bytes 524320 | tf_op jit(solution)/shard_map/ppermute | solution.py:499
  51.6 0.6 collective-permute-start.5
  52.2 0.0 collective-permute-done.3.refs_1_
  52.2 1.4 collective-permute-start.8
  53.6 10.8 %collective-permute-done.5.refs_3_ = bf16[2048,128]{1,0:T(8,128)(2,1)S(1)} collective-permute-done((bf16[2048,128]{1,0:T(8,128)(2,1)S(1)}, bf16[2048,128]{1,0:T(8,128)(2,1)S(1)}, u32[]{:S(2)}, u32[]{:S(2)}) %collective-permute-start.5) | collective-permute-done | bytes 524320 | tf_op jit(solution)/shard_map/ppermute | solution.py:499
  64.4 0.5 collective-permute-start.12
  64.9 3.2 %project.1 = (f32[2048,256]{1,0:T(8,128)S(1)}, bf16[2048,256]{1,0:T(8,128)(2,1)S(1)}) custom-call(s32[3]{0:T(128)S(1)} %pad_add_fusion.sc_ref, bf16[2048,128]{1,0:T(8,128)(2,1)S(1)} %mixer.1.refs_0_, bf16[2048,128]{1,0:T(8,128)(2,1)S(1)} %collective-permute-done.3.refs_1_, bf16[2048,128]{1,0:T(8,128)(2,1)S(1)} %collective-permute-done.4.refs_2_, ...), custom_call_target="tpu_custom_call" | custom-call | flops 2000000000 | bytes 6000000 | tf_op jit(solution)/shard_map/project/pallas_call | solution.py:237
  68.2 2.5 %collective-permute-done.8.refs_0_ = bf16[160,2048]{1,0:T(8,128)(2,1)S(1)} collective-permute-done((bf16[160,2048]{1,0:T(8,128)(2,1)S(1)}, bf16[160,2048]{1,0:T(8,128)(2,1)S(1)}, u32[]{:S(2)}, u32[]{:S(2)}) %collective-permute-start.8) | collective-permute-done | bytes 655392 | tf_op jit(solution)/shard_map/ppermute | solution.py:497
  70.7 0.5 collective-permute-start.13
  71.2 0.0 collective-permute-done.10.refs_5_
  71.2 0.0 collective-permute-start.7
  71.2 10.0 %ffn.2 = (bf16[160,2048]{1,0:T(8,128)(2,1)S(1)}, bf16[160,2048]{1,0:T(8,128)(2,1)S(1)}) custom-call(bf16[160,2048]{1,0:T(8,128)(2,1)S(1)} %collective-permute-done.8.refs_0_, bf16[160,2048]{1,0:T(8,128)(2,1)S(1)} %get-tuple-element.38.refs_1_, bf16[1,2048,896]{2,1,0:T(8,128)(2,1)S(1)} %copy-done, bf16[1,2048,896]{2,1,0:T(8,128)(2,1)} %collective-permute-done.9.refs_3_, ...), custom_call_target="tpu_custom_call" | custom-call | flops 8000000000 | bytes 25000000 | tf_op jit(solution)/shard_map/ffn/pallas_call | solution.py:403
  81.2 1.6 %collective-permute-start.16 = (bf16[160,2048]{1,0:T(8,128)(2,1)S(1)}, bf16[160,2048]{1,0:T(8,128)(2,1)S(1)}, u32[]{:S(2)}, u32[]{:S(2)}) collective-permute-start(bf16[160,2048]{1,0:T(8,128)(2,1)S(1)} %get-tuple-element.43), channel_id=1, source_target_pairs={{0,24},{8,16},{16,8},{24,0},{1,25},{9,17},{17,9},{25,1},{2,26},{10... | collective-permute-start | bytes 1966088 | tf_op jit(solution)/shard_map/ppermute | solution.py:497
  82.8 2.2 %collective-permute-done.13.refs_1_ = bf16[160,2048]{1,0:T(8,128)(2,1)S(1)} collective-permute-done((bf16[160,2048]{1,0:T(8,128)(2,1)S(1)}, bf16[160,2048]{1,0:T(8,128)(2,1)S(1)}, u32[]{:S(2)}, u32[]{:S(2)}) %collective-permute-start.13) | collective-permute-done | bytes 655392 | tf_op jit(solution)/shard_map/ppermute | solution.py:497
  85.0 10.0 %ffn.3 = (bf16[160,512]{1,0:T(8,128)(2,1)S(1)}, bf16[160,768]{1,0:T(8,128)(2,1)S(1)}, bf16[160,768]{1,0:T(8,128)(2,1)S(1)}, bf16[160,512]{1,0:T(8,128)(2,1)S(1)}...) custom-call(bf16[160,2048]{1,0:T(8,128)(2,1)S(1)} %collective-permute-done.12.refs_0_, ...), custom_call_target="tpu_custom_call" | custom-call | flops 8000000000 | bytes 25000000 | tf_op jit(solution)/shard_map/ffn/pallas_call | solution.py:403
  95.0 0.0 copy-start.11
  95.0 0.6 collective-permute-start.14
  95.6 1.4 %collective-permute-start.15 = (bf16[160,512]{1,0:T(8,128)(2,1)S(1)}, bf16[160,512]{1,0:T(8,128)(2,1)S(1)}, u32[]{:S(2)}, u32[]{:S(2)}) collective-permute-start(bf16[160,512]{1,0:T(8,128)(2,1)S(1)} %get-tuple-element.42), channel_id=1, source_target_pairs={{0,16},{8,24},{16,0},{24,8},{1,17},{9,25},{17,1},{25,9},{2,18},{10... | collective-permute-start | bytes 491528 | tf_op jit(solution)/shard_map/ppermute | solution.py:497
  97.0 0.6 collective-permute-start.20
  97.6 1.5 %collective-permute-start.21 = (bf16[160,768]{1,0:T(8,128)(2,1)S(1)}, bf16[160,768]{1,0:T(8,128)(2,1)S(1)}, u32[]{:S(2)}, u32[]{:S(2)}) collective-permute-start(bf16[160,768]{1,0:T(8,128)(2,1)S(1)} %get-tuple-element.49), channel_id=1, source_target_pairs={{0,16},{8,24},{16,0},{24,8},{1,17},{9,25},{17,1},{25,9},{2,18},{10... | collective-permute-start | bytes 737288 | tf_op jit(solution)/shard_map/ppermute | solution.py:497
  99.1 4.3 %collective-permute-done.14.refs_1_ = bf16[160,512]{1,0:T(8,128)(2,1)S(1)} collective-permute-done((bf16[160,512]{1,0:T(8,128)(2,1)S(1)}, bf16[160,512]{1,0:T(8,128)(2,1)S(1)}, u32[]{:S(2)}, u32[]{:S(2)}) %collective-permute-start.14) | collective-permute-done | bytes 163872 | tf_op jit(solution)/shard_map/ppermute | solution.py:497
  103.4 0.5 collective-permute-start.25
  103.9 1.4 %collective-permute-start.26 = (bf16[160,768]{1,0:T(8,128)(2,1)S(1)}, bf16[160,768]{1,0:T(8,128)(2,1)S(1)}, u32[]{:S(2)}, u32[]{:S(2)}) collective-permute-start(bf16[160,768]{1,0:T(8,128)(2,1)S(1)} %get-tuple-element.55), channel_id=1, source_target_pairs={{0,16},{8,24},{16,0},{24,8},{1,17},{9,25},{17,1},{25,9},{2,18},{10... | collective-permute-start | bytes 737288 | tf_op jit(solution)/shard_map/ppermute | solution.py:497
  105.4 1.1 join.1
  106.4 1.3 combine.3
  107.7 1.2 collective-permute-start.17
  108.9 13.0 %collective-permute-start.18 = (bf16[64,512]{1,0:T(8,128)(2,1)S(1)}, bf16[64,512]{1,0:T(8,128)(2,1)S(1)}, u32[]{:S(2)}, u32[]{:S(2)}) collective-permute-start(bf16[64,512]{1,0:T(8,128)(2,1)S(1)} %get-tuple-element.46), channel_id=1, source_target_pairs={{0,4},{1,5},{2,6},{3,7},{4,0},{5,1},{6,2},{7,3},{8,12},{9,13},{10,... | collective-permute-start | bytes 196616 | tf_op jit(solution)/shard_map/ppermute | solution.py:499
  121.9 1.4 combine.4
  123.3 0.7 collective-permute-start.22
  124.0 3.8 %collective-permute-start.23 = (bf16[64,768]{1,0:T(8,128)(2,1)S(1)}, bf16[64,768]{1,0:T(8,128)(2,1)S(1)}, u32[]{:S(2)}, u32[]{:S(2)}) collective-permute-start(bf16[64,768]{1,0:T(8,128)(2,1)S(1)} %get-tuple-element.52), channel_id=1, source_target_pairs={{0,4},{1,5},{2,6},{3,7},{4,0},{5,1},{6,2},{7,3},{8,12},{9,13},{10,... | collective-permute-start | bytes 294920 | tf_op jit(solution)/shard_map/ppermute | solution.py:499
  127.8 1.4 combine.5
  129.2 0.1 collective-permute-start.24
  129.3 0.5 collective-permute-start.27
  129.8 3.8 %collective-permute-start.28 = (bf16[64,768]{1,0:T(8,128)(2,1)S(1)}, bf16[64,768]{1,0:T(8,128)(2,1)S(1)}, u32[]{:S(2)}, u32[]{:S(2)}) collective-permute-start(bf16[64,768]{1,0:T(8,128)(2,1)S(1)} %get-tuple-element.58), channel_id=1, source_target_pairs={{0,4},{1,5},{2,6},{3,7},{4,0},{5,1},{6,2},{7,3},{8,12},{9,13},{10,... | collective-permute-start | bytes 294920 | tf_op jit(solution)/shard_map/ppermute | solution.py:499
  133.7 0.3 collective-permute-start.29
  134.0 1.7 %collective-permute-done.24 = bf16[64,768]{1,0:T(8,128)(2,1)S(1)} collective-permute-done((bf16[64,768]{1,0:T(8,128)(2,1)S(1)}, bf16[64,768]{1,0:T(8,128)(2,1)S(1)}, u32[]{:S(2)}, u32[]{:S(2)}) %collective-permute-start.24) | collective-permute-done | bytes 98336 | tf_op jit(solution)/shard_map/ppermute | solution.py:499
  135.7 0.1 add_convert_fusion.1
  135.8 0.9 collective-permute-done.28
  136.7 3.5 %collective-permute-done.29 = bf16[64,768]{1,0:T(8,128)(2,1)S(1)} collective-permute-done((bf16[64,768]{1,0:T(8,128)(2,1)S(1)}, bf16[64,768]{1,0:T(8,128)(2,1)S(1)}, u32[]{:S(2)}, u32[]{:S(2)}) %collective-permute-start.29) | collective-permute-done | bytes 98336 | tf_op jit(solution)/shard_map/ppermute | solution.py:499
  140.2 0.1 add_convert_fusion
  140.2 0.7 pad_maximum_fusion
  (39 shorter events, 0.1 us)
Async XLA Ops:
  0.6 70.6 %collective-permute-start.10 = (bf16[1,2048,896]{2,1,0:T(8,128)(2,1)}, bf16[1,2048,896]{2,1,0:T(8,128)(2,1)}, u32[]{:S(2)}, u32[]{:S(2)}) collective-permute-start(bf16[1,2048,896]{2,1,0:T(8,128)(2,1)} %refs_4_.7), channel_id=1, source_target_pairs={{0,1},{1,0},{2,3},{3,2},{4,5},{5,4},{6,7},{7,6},{8,9},{9,8},{10,11... | collective-permute-start | bytes 11010056 | tf_op jit(solution)/shard_map/ppermute | solution.py:498
  1.2 70.0 %collective-permute-start.11 = (bf16[1,896,2048]{2,1,0:T(8,128)(2,1)}, bf16[1,896,2048]{2,1,0:T(8,128)(2,1)}, u32[]{:S(2)}, u32[]{:S(2)}) collective-permute-start(bf16[1,896,2048]{2,1,0:T(8,128)(2,1)} %refs_6_.5), channel_id=1, source_target_pairs={{0,1},{1,0},{2,3},{3,2},{4,5},{5,4},{6,7},{7,6},{8,9},{9,8},{10,11... | collective-permute-start | bytes 11010056 | tf_op jit(solution)/shard_map/ppermute | solution.py:498
  1.3 70.0 %collective-permute-start.9 = (bf16[1,2048,896]{2,1,0:T(8,128)(2,1)}, bf16[1,2048,896]{2,1,0:T(8,128)(2,1)}, u32[]{:S(2)}, u32[]{:S(2)}) collective-permute-start(bf16[1,2048,896]{2,1,0:T(8,128)(2,1)} %refs_2_.3), channel_id=1, source_target_pairs={{0,1},{1,0},{2,3},{3,2},{4,5},{5,4},{6,7},{7,6},{8,9},{9,8},{10,11... | collective-permute-start | bytes 11010056 | tf_op jit(solution)/shard_map/ppermute | solution.py:498
  1.7 12.8 %copy-start.2 = (bf16[512,2048]{1,0:T(8,128)(2,1)S(1)}, bf16[512,2048]{1,0:T(8,128)(2,1)}, u32[]{:S(2)}) copy-start(bf16[512,2048]{1,0:T(8,128)(2,1)} %param.23) | copy-start | bytes 6291460
  1.7 12.8 %copy-start.9 = (f32[2048]{0:T(1024)S(1)}, f32[2048]{0:T(1024)}, u32[]{:S(2)}) copy-start(f32[2048]{0:T(1024)} %param.24) | copy-start | bytes 24580
  1.7 12.8 %copy-start.10 = (s32[512,2]{0,1:T(2,128)S(1)}, s32[512,2]{0,1:T(2,128)}, u32[]{:S(2)}) copy-start(s32[512,2]{0,1:T(2,128)} %param.25) | copy-start | bytes 12292
  6.2 5.6 %collective-permute-start = (f32[136,128]{1,0:T(8,128)}, f32[136,128]{1,0:T(8,128)S(1)}, u32[]{:S(2)}, u32[]{:S(2)}) collective-permute-start(f32[136,128]{1,0:T(8,128)} %final_state.1), channel_id=1, source_target_pairs={{0,8},{8,0},{16,24},{24,16},{1,9},{9,1},{17,25},{25,17},{2,10},{10... | collective-permute-start | bytes 208904 | tf_op jit(solution)/shard_map/ppermute | solution.py:497
  8.8 7.5 %collective-permute-start.1 = (f32[136,128]{1,0:T(8,128)}, f32[136,128]{1,0:T(8,128)S(1)}, u32[]{:S(2)}, u32[]{:S(2)}) collective-permute-start(f32[136,128]{1,0:T(8,128)} %final_state.1), channel_id=1, source_target_pairs={{0,16},{8,24},{16,0},{24,8},{1,17},{9,25},{17,1},{25,9},{2,18},{10... | collective-permute-start | bytes 208904 | tf_op jit(solution)/shard_map/ppermute | solution.py:497
  11.8 5.4 %collective-permute-start.2 = (f32[136,128]{1,0:T(8,128)}, f32[136,128]{1,0:T(8,128)S(1)}, u32[]{:S(2)}, u32[]{:S(2)}) collective-permute-start(f32[136,128]{1,0:T(8,128)} %final_state.1), channel_id=1, source_target_pairs={{0,24},{8,16},{16,8},{24,0},{1,25},{9,17},{17,9},{25,1},{2,26},{10... | collective-permute-start | bytes 208904 | tf_op jit(solution)/shard_map/ppermute | solution.py:497
  14.5 1.8 %copy-start.7 = (bf16[1024,256]{1,0:T(8,128)(2,1)S(1)}, bf16[1024,256]{1,0:T(8,128)(2,1)}, u32[]{:S(2)}) copy-start(bf16[1024,256]{1,0:T(8,128)(2,1)} %refs_4_.5) | copy-start | bytes 1572868
  14.5 2.7 %copy-start.3 = (bf16[2048,256]{1,0:T(8,128)(2,1)S(1)}, bf16[2048,256]{1,0:T(8,128)(2,1)}, u32[]{:S(2)}) copy-start(bf16[2048,256]{1,0:T(8,128)(2,1)} %refs_4_.4) | copy-start | bytes 3145732
  14.6 2.7 %copy-start.4 = (bf16[2048,256]{1,0:T(8,128)(2,1)S(1)}, bf16[2048,256]{1,0:T(8,128)(2,1)}, u32[]{:S(2)}) copy-start(bf16[2048,256]{1,0:T(8,128)(2,1)} %refs_3_) | copy-start | bytes 3145732
  14.6 2.7 %copy-start.5 = (bf16[2048,128]{1,0:T(8,128)(2,1)S(1)}, bf16[2048,128]{1,0:T(8,128)(2,1)}, u32[]{:S(2)}) copy-start(bf16[2048,128]{1,0:T(8,128)(2,1)} %refs_5_.1) | copy-start | bytes 1572868
  14.6 2.7 %copy-start.6 = (bf16[2048,128]{1,0:T(8,128)(2,1)S(1)}, bf16[2048,128]{1,0:T(8,128)(2,1)}, u32[]{:S(2)}) copy-start(bf16[2048,128]{1,0:T(8,128)(2,1)} %refs_6_.3) | copy-start | bytes 1572868
  14.6 2.7 %copy-start.8 = (f32[2048,2]{0,1:T(2,128)S(1)}, f32[2048,2]{0,1:T(2,128)}, u32[]{:S(2)}) copy-start(f32[2048,2]{0,1:T(2,128)} %param.20) | copy-start | bytes 49156
  14.6 2.7 %copy-start.12 = (f32[256]{0:T(256)S(1)}, f32[256]{0:T(256)}, u32[]{:S(2)}) copy-start(f32[256]{0:T(256)} %param.19) | copy-start | bytes 3076
  14.6 2.7 %copy-start.13 = (f32[128]{0:T(128)S(1)}, f32[128]{0:T(128)}, u32[]{:S(2)}) copy-start(f32[128]{0:T(128)} %param.21) | copy-start | bytes 1540
  16.4 12.3 %collective-permute-start.6 = (bf16[1024,256]{1,0:T(8,128)(2,1)S(1)}, bf16[1024,256]{1,0:T(8,128)(2,1)S(1)}, u32[]{:S(2)}, u32[]{:S(2)}) collective-permute-start(bf16[1024,256]{1,0:T(8,128)(2,1)S(1)} %copy-done.7), channel_id=1, source_target_pairs={{0,1},{1,0},{2,3},{3,2},{4,5},{5,4},{6,7},{7,6},{8,9},{9,8},{10,11... | collective-permute-start | bytes 1572872 | tf_op jit(solution)/shard_map/ppermute | solution.py:498
  25.8 25.8 %collective-permute-start.4 = (bf16[2048,128]{1,0:T(8,128)(2,1)S(1)}, bf16[2048,128]{1,0:T(8,128)(2,1)S(1)}, u32[]{:S(2)}, u32[]{:S(2)}) collective-permute-start(bf16[2048,128]{1,0:T(8,128)(2,1)S(1)} %mixer.1.refs_0_), channel_id=1, source_target_pairs={{0,4},{1,5},{2,6},{3,7},{4,0},{5,1},{6,2},{7,3},{8,12},{9,13},{10,... | collective-permute-start | bytes 1572872 | tf_op jit(solution)/shard_map/ppermute | solution.py:499
  28.7 23.5 %collective-permute-start.3 = (bf16[2048,128]{1,0:T(8,128)(2,1)S(1)}, bf16[2048,128]{1,0:T(8,128)(2,1)S(1)}, u32[]{:S(2)}, u32[]{:S(2)}) collective-permute-start(bf16[2048,128]{1,0:T(8,128)(2,1)S(1)} %mixer.1.refs_0_), channel_id=1, source_target_pairs={{0,2},{1,3},{2,0},{3,1},{4,6},{5,7},{6,4},{7,5},{8,10},{9,11},{10,... | collective-permute-start | bytes 1572872 | tf_op jit(solution)/shard_map/ppermute | solution.py:499
  51.6 12.8 %collective-permute-start.5 = (bf16[2048,128]{1,0:T(8,128)(2,1)S(1)}, bf16[2048,128]{1,0:T(8,128)(2,1)S(1)}, u32[]{:S(2)}, u32[]{:S(2)}) collective-permute-start(bf16[2048,128]{1,0:T(8,128)(2,1)S(1)} %collective-permute-done.4.refs_2_), channel_id=1, source_target_pairs={{0,2},{1,3},{2,0},{3,1},{4,6},{5,7},{6,4},{7,5},{8,10},{9,11},{10,... | collective-permute-start | bytes 1572872 | tf_op jit(solution)/shard_map/ppermute | solution.py:499
  52.2 18.5 %collective-permute-start.8 = (bf16[160,2048]{1,0:T(8,128)(2,1)S(1)}, bf16[160,2048]{1,0:T(8,128)(2,1)S(1)}, u32[]{:S(2)}, u32[]{:S(2)}) collective-permute-start(bf16[160,2048]{1,0:T(8,128)(2,1)S(1)} %get-tuple-element.36), channel_id=1, source_target_pairs={{0,24},{8,16},{16,8},{24,0},{1,25},{9,17},{17,9},{25,1},{2,26},{10... | collective-permute-start | bytes 1966088 | tf_op jit(solution)/shard_map/ppermute | solution.py:497
  53.6 17.6 %copy-start = (bf16[1,2048,896]{2,1,0:T(8,128)(2,1)S(1)}, bf16[1,2048,896]{2,1,0:T(8,128)(2,1)}, u32[]{:S(2)}) copy-start(bf16[1,2048,896]{2,1,0:T(8,128)(2,1)} %refs_2_.3) | copy-start | bytes 11010052
  53.6 17.6 %copy-start.1 = (bf16[1,2048,896]{2,1,0:T(8,128)(2,1)S(1)}, bf16[1,2048,896]{2,1,0:T(8,128)(2,1)}, u32[]{:S(2)}) copy-start(bf16[1,2048,896]{2,1,0:T(8,128)(2,1)} %refs_4_.7) | copy-start | bytes 11010052
  64.4 18.4 %collective-permute-start.12 = (bf16[160,2048]{1,0:T(8,128)(2,1)S(1)}, bf16[160,2048]{1,0:T(8,128)(2,1)S(1)}, u32[]{:S(2)}, u32[]{:S(2)}) collective-permute-start(bf16[160,2048]{1,0:T(8,128)(2,1)S(1)} %get-tuple-element.32), channel_id=1, source_target_pairs={{0,8},{8,0},{16,24},{24,16},{1,9},{9,1},{17,25},{25,17},{2,10},{10... | collective-permute-start | bytes 1966088 | tf_op jit(solution)/shard_map/ppermute | solution.py:497
  70.7 14.3 %collective-permute-start.13 = (bf16[160,2048]{1,0:T(8,128)(2,1)S(1)}, bf16[160,2048]{1,0:T(8,128)(2,1)S(1)}, u32[]{:S(2)}, u32[]{:S(2)}) collective-permute-start(bf16[160,2048]{1,0:T(8,128)(2,1)S(1)} %get-tuple-element.40), channel_id=1, source_target_pairs={{0,16},{8,24},{16,0},{24,8},{1,17},{9,25},{17,1},{25,9},{2,18},{10... | collective-permute-start | bytes 1966088 | tf_op jit(solution)/shard_map/ppermute | solution.py:497
  71.2 26.4 %collective-permute-start.7 = (bf16[2048,256]{1,0:T(8,128)(2,1)S(1)}, bf16[2048,256]{1,0:T(8,128)(2,1)S(1)}, u32[]{:S(2)}, u32[]{:S(2)}) collective-permute-start(bf16[2048,256]{1,0:T(8,128)(2,1)S(1)} %get-tuple-element.35), channel_id=1, source_target_pairs={{0,1},{1,0},{2,3},{3,2},{4,5},{5,4},{6,7},{7,6},{8,9},{9,8},{10,11... | collective-permute-start | bytes 3145736 | tf_op jit(solution)/shard_map/ppermute | solution.py:498
  81.2 25.2 %collective-permute-start.16 = (bf16[160,2048]{1,0:T(8,128)(2,1)S(1)}, bf16[160,2048]{1,0:T(8,128)(2,1)S(1)}, u32[]{:S(2)}, u32[]{:S(2)}) collective-permute-start(bf16[160,2048]{1,0:T(8,128)(2,1)S(1)} %get-tuple-element.43), channel_id=1, source_target_pairs={{0,24},{8,16},{16,8},{24,0},{1,25},{9,17},{17,9},{25,1},{2,26},{10... | collective-permute-start | bytes 1966088 | tf_op jit(solution)/shard_map/ppermute | solution.py:497
  95.0 11.4 %copy-start.11 = (f32[512,2]{0,1:T(2,128)S(1)}, f32[512,2]{0,1:T(2,128)}, u32[]{:S(2)}) copy-start(f32[512,2]{0,1:T(2,128)} %param.26) | copy-start | bytes 12292
  95.0 8.4 %collective-permute-start.14 = (bf16[160,512]{1,0:T(8,128)(2,1)S(1)}, bf16[160,512]{1,0:T(8,128)(2,1)S(1)}, u32[]{:S(2)}, u32[]{:S(2)}) collective-permute-start(bf16[160,512]{1,0:T(8,128)(2,1)S(1)} %get-tuple-element.41), channel_id=1, source_target_pairs={{0,8},{8,0},{16,24},{24,16},{1,9},{9,1},{17,25},{25,17},{2,10},{10... | collective-permute-start | bytes 491528 | tf_op jit(solution)/shard_map/ppermute | solution.py:497
  95.6 8.3 %collective-permute-start.15 = (bf16[160,512]{1,0:T(8,128)(2,1)S(1)}, bf16[160,512]{1,0:T(8,128)(2,1)S(1)}, u32[]{:S(2)}, u32[]{:S(2)}) collective-permute-start(bf16[160,512]{1,0:T(8,128)(2,1)S(1)} %get-tuple-element.42), channel_id=1, source_target_pairs={{0,16},{8,24},{16,0},{24,8},{1,17},{9,25},{17,1},{25,9},{2,18},{10... | collective-permute-start | bytes 491528 | tf_op jit(solution)/shard_map/ppermute | solution.py:497
  97.0 11.9 %collective-permute-start.20 = (bf16[160,768]{1,0:T(8,128)(2,1)S(1)}, bf16[160,768]{1,0:T(8,128)(2,1)S(1)}, u32[]{:S(2)}, u32[]{:S(2)}) collective-permute-start(bf16[160,768]{1,0:T(8,128)(2,1)S(1)} %get-tuple-element.48), channel_id=1, source_target_pairs={{0,8},{8,0},{16,24},{24,16},{1,9},{9,1},{17,25},{25,17},{2,10},{10... | collective-permute-start | bytes 737288 | tf_op jit(solution)/shard_map/ppermute | solution.py:497
  97.6 24.3 %collective-permute-start.21 = (bf16[160,768]{1,0:T(8,128)(2,1)S(1)}, bf16[160,768]{1,0:T(8,128)(2,1)S(1)}, u32[]{:S(2)}, u32[]{:S(2)}) collective-permute-start(bf16[160,768]{1,0:T(8,128)(2,1)S(1)} %get-tuple-element.49), channel_id=1, source_target_pairs={{0,16},{8,24},{16,0},{24,8},{1,17},{9,25},{17,1},{25,9},{2,18},{10... | collective-permute-start | bytes 737288 | tf_op jit(solution)/shard_map/ppermute | solution.py:497
  103.4 19.9 %collective-permute-start.25 = (bf16[160,768]{1,0:T(8,128)(2,1)S(1)}, bf16[160,768]{1,0:T(8,128)(2,1)S(1)}, u32[]{:S(2)}, u32[]{:S(2)}) collective-permute-start(bf16[160,768]{1,0:T(8,128)(2,1)S(1)} %get-tuple-element.54), channel_id=1, source_target_pairs={{0,8},{8,0},{16,24},{24,16},{1,9},{9,1},{17,25},{25,17},{2,10},{10... | collective-permute-start | bytes 737288 | tf_op jit(solution)/shard_map/ppermute | solution.py:497
  103.9 20.1 %collective-permute-start.26 = (bf16[160,768]{1,0:T(8,128)(2,1)S(1)}, bf16[160,768]{1,0:T(8,128)(2,1)S(1)}, u32[]{:S(2)}, u32[]{:S(2)}) collective-permute-start(bf16[160,768]{1,0:T(8,128)(2,1)S(1)} %get-tuple-element.55), channel_id=1, source_target_pairs={{0,16},{8,24},{16,0},{24,8},{1,17},{9,25},{17,1},{25,9},{2,18},{10... | collective-permute-start | bytes 737288 | tf_op jit(solution)/shard_map/ppermute | solution.py:497
  107.7 21.5 %collective-permute-start.17 = (bf16[64,512]{1,0:T(8,128)(2,1)S(1)}, bf16[64,512]{1,0:T(8,128)(2,1)S(1)}, u32[]{:S(2)}, u32[]{:S(2)}) collective-permute-start(bf16[64,512]{1,0:T(8,128)(2,1)S(1)} %get-tuple-element.45), channel_id=1, source_target_pairs={{0,2},{1,3},{2,0},{3,1},{4,6},{5,7},{6,4},{7,5},{8,10},{9,11},{10,... | collective-permute-start | bytes 196616 | tf_op jit(solution)/shard_map/ppermute | solution.py:499
  108.9 20.3 %collective-permute-start.18 = (bf16[64,512]{1,0:T(8,128)(2,1)S(1)}, bf16[64,512]{1,0:T(8,128)(2,1)S(1)}, u32[]{:S(2)}, u32[]{:S(2)}) collective-permute-start(bf16[64,512]{1,0:T(8,128)(2,1)S(1)} %get-tuple-element.46), channel_id=1, source_target_pairs={{0,4},{1,5},{2,6},{3,7},{4,0},{5,1},{6,2},{7,3},{8,12},{9,13},{10,... | collective-permute-start | bytes 196616 | tf_op jit(solution)/shard_map/ppermute | solution.py:499
  121.9 7.9 %collective-permute-start.19 = (bf16[64,512]{1,0:T(8,128)(2,1)S(1)}, bf16[64,512]{1,0:T(8,128)(2,1)S(1)}, u32[]{:S(2)}, u32[]{:S(2)}) collective-permute-start(bf16[64,512]{1,0:T(8,128)(2,1)S(1)} %get-tuple-element.47), channel_id=1, source_target_pairs={{0,6},{1,7},{2,4},{3,5},{4,2},{5,3},{6,0},{7,1},{8,14},{9,15},{10,... | collective-permute-start | bytes 196616 | tf_op jit(solution)/shard_map/ppermute | solution.py:499
  123.3 10.4 %collective-permute-start.22 = (bf16[64,768]{1,0:T(8,128)(2,1)S(1)}, bf16[64,768]{1,0:T(8,128)(2,1)S(1)}, u32[]{:S(2)}, u32[]{:S(2)}) collective-permute-start(bf16[64,768]{1,0:T(8,128)(2,1)S(1)} %get-tuple-element.51), channel_id=1, source_target_pairs={{0,2},{1,3},{2,0},{3,1},{4,6},{5,7},{6,4},{7,5},{8,10},{9,11},{10,... | collective-permute-start | bytes 294920 | tf_op jit(solution)/shard_map/ppermute | solution.py:499
  124.0 10.0 %collective-permute-start.23 = (bf16[64,768]{1,0:T(8,128)(2,1)S(1)}, bf16[64,768]{1,0:T(8,128)(2,1)S(1)}, u32[]{:S(2)}, u32[]{:S(2)}) collective-permute-start(bf16[64,768]{1,0:T(8,128)(2,1)S(1)} %get-tuple-element.52), channel_id=1, source_target_pairs={{0,4},{1,5},{2,6},{3,7},{4,0},{5,1},{6,2},{7,3},{8,12},{9,13},{10,... | collective-permute-start | bytes 294920 | tf_op jit(solution)/shard_map/ppermute | solution.py:499
  129.2 6.5 %collective-permute-start.24 = (bf16[64,768]{1,0:T(8,128)(2,1)S(1)}, bf16[64,768]{1,0:T(8,128)(2,1)S(1)}, u32[]{:S(2)}, u32[]{:S(2)}) collective-permute-start(bf16[64,768]{1,0:T(8,128)(2,1)S(1)} %get-tuple-element.53), channel_id=1, source_target_pairs={{0,6},{1,7},{2,4},{3,5},{4,2},{5,3},{6,0},{7,1},{8,14},{9,15},{10,... | collective-permute-start | bytes 294920 | tf_op jit(solution)/shard_map/ppermute | solution.py:499
  129.3 6.5 %collective-permute-start.27 = (bf16[64,768]{1,0:T(8,128)(2,1)S(1)}, bf16[64,768]{1,0:T(8,128)(2,1)S(1)}, u32[]{:S(2)}, u32[]{:S(2)}) collective-permute-start(bf16[64,768]{1,0:T(8,128)(2,1)S(1)} %get-tuple-element.57), channel_id=1, source_target_pairs={{0,2},{1,3},{2,0},{3,1},{4,6},{5,7},{6,4},{7,5},{8,10},{9,11},{10,... | collective-permute-start | bytes 294920 | tf_op jit(solution)/shard_map/ppermute | solution.py:499
  129.8 6.9 %collective-permute-start.28 = (bf16[64,768]{1,0:T(8,128)(2,1)S(1)}, bf16[64,768]{1,0:T(8,128)(2,1)S(1)}, u32[]{:S(2)}, u32[]{:S(2)}) collective-permute-start(bf16[64,768]{1,0:T(8,128)(2,1)S(1)} %get-tuple-element.58), channel_id=1, source_target_pairs={{0,4},{1,5},{2,6},{3,7},{4,0},{5,1},{6,2},{7,3},{8,12},{9,13},{10,... | collective-permute-start | bytes 294920 | tf_op jit(solution)/shard_map/ppermute | solution.py:499
  133.7 6.5 %collective-permute-start.29 = (bf16[64,768]{1,0:T(8,128)(2,1)S(1)}, bf16[64,768]{1,0:T(8,128)(2,1)S(1)}, u32[]{:S(2)}, u32[]{:S(2)}) collective-permute-start(bf16[64,768]{1,0:T(8,128)(2,1)S(1)} %get-tuple-element.59), channel_id=1, source_target_pairs={{0,6},{1,7},{2,4},{3,5},{4,2},{5,3},{6,0},{7,1},{8,14},{9,15},{10,... | collective-permute-start | bytes 294920 | tf_op jit(solution)/shard_map/ppermute | solution.py:499
